TPU v7x, 256 devices: a whole 4x4x8 slice. The times are simulated.
256 devices in a mesh: ep: 128 (over z, y, x), tp: 2 (over core).
Axes of the slice: x: 4, y: 4, z: 8, core: 2. Of those that a mesh axis runs over, the one named last changes fastest.
Arguments:
- tokens: bfloat16 [16384, 2048], P('ep'), may hold values from -24 to 24
- cotangent: bfloat16 [16384, 2048], P('ep'), may hold values from -0.625 to 0.625
- routes: int32 [16384, 2], P('ep'), may hold values from 0 to 127, as said below
- router_group: bfloat16 [2048, 4], replicated, may hold values from -0.125 to 0.125
- router_expert: bfloat16 [2048, 128], replicated, may hold values from -0.125 to 0.125
- gate_proj: bfloat16 [128, 2048, 512], P('ep', None, 'tp'), may hold values from -0.125 to 0.125
- up_proj: bfloat16 [128, 2048, 512], P('ep', None, 'tp'), may hold values from -0.125 to 0.125
- down_proj: bfloat16 [128, 512, 2048], P('ep', 'tp'), may hold values from -0.25 to 0.25
Outputs:
- token_grad: bfloat16 [16384, 2048], P('ep', 'tp')
- gate_grad: bfloat16 [128, 2048, 512], P('ep', None, 'tp')
- up_grad: bfloat16 [128, 2048, 512], P('ep', None, 'tp')
- down_grad: bfloat16 [128, 512, 2048], P('ep', 'tp')
- gate_rows: float32 [128, 2048], P('ep')
- up_rows: float32 [128, 2048], P('ep')
- down_rows: float32 [128, 512], P('ep', 'tp')
- router_expert_grad: float32 [2048, 128], P(('ep', 'tp'))
- router_group_grad: float32 [2048, 4], P(('ep', 'tp'))
- router_rows: float32 [2048], P(('ep', 'tp'))
Inputs may be any that keep to these rules, and one draw needn't show every extreme that they name: `routes`: the 2 entries of a row are different experts of one group: their quotients by 32 are equal. Among the rows of one device no expert is named more than 4 times, and the experts of one group, the same for all devices, are each named exactly 4 times by the rows of every device.
All inputs are finite; a program needn't handle non-finite values.
Results may differ from a plain program's by a relative error of at most 0.014.
Values may be sent and summed in bfloat16 or wider, within the bound.
No kernel may reach another device: no remote copies, remote signals or barrier semaphores. Data moves between devices by JAX's collectives and lax.ppermute only.
A program may use at most 64 MiB of HBM per device.

v0:
```python
import jax
import jax.numpy as jnp
from jax import lax
from jax.experimental import pallas as pl
from jax.experimental.pallas import tpu as pltpu
from jax.sharding import PartitionSpec as P

BF = jnp.bfloat16
F32 = jnp.float32
GROUP_LANE = 32
U_LANE = 40
LOW_LANE = 64
EXTRA = 128


def mm(a, b):
    return lax.dot_general(a, b, (((1,), (0,)), ((), ())), preferred_element_type=F32)


def nt(a, b):
    return lax.dot_general(a, b, (((1,), (1,)), ((), ())), preferred_element_type=F32)


def tn(a, b):
    return lax.dot_general(a, b, (((0,), (0,)), ((), ())), preferred_element_type=F32)


def iota(shape, dim):
    return lax.broadcasted_iota(jnp.int32, shape, dim)


def call(kernel, name, flops, outs, scalars, arrays):
    smem = pl.BlockSpec(memory_space=pltpu.SMEM)
    vmem = pl.BlockSpec(memory_space=pltpu.VMEM)
    return pl.pallas_call(
        kernel,
        name=name,
        out_shape=[jax.ShapeDtypeStruct(shape, dtype) for shape, dtype in outs],
        in_specs=[smem] * len(scalars) + [vmem] * len(arrays),
        out_specs=[vmem] * len(outs),
        cost_estimate=pl.CostEstimate(flops=flops, bytes_accessed=4 << 20, transcendentals=0),
        compiler_params=pltpu.CompilerParams(vmem_limit_bytes=56 << 20),
    )(*scalars, *arrays)


def ones_where(mask):
    return jnp.where(mask, 1.0, 0.0).astype(BF)


def pre_kernel(tp_ref, rt_ref, tok_ref, cot_ref, rgt_ref, rex_ref, send_ref, aux_ref):
    tp = tp_ref[0]
    tok, dm = tok_ref.shape
    experts = rex_ref.shape[1]
    groups = rgt_ref.shape[0]
    gw = experts // groups
    width = dm // 4
    r0, r1 = rt_ref[0:1, :], rt_ref[1:2, :]
    group_exp = jnp.exp(nt(rgt_ref[...], tok_ref[...]))
    group_prob = group_exp / jnp.sum(group_exp, axis=0, keepdims=True)
    logits = jnp.transpose(mm(tok_ref[...], rex_ref[...]))
    ei = iota((experts, tok), 0)
    l0 = jnp.sum(jnp.where(ei == r0, logits, 0.0), axis=0, keepdims=True)
    l1 = jnp.sum(jnp.where(ei == r1, logits, 0.0), axis=0, keepdims=True)
    x0, x1 = jnp.exp(l0), jnp.exp(l1)
    p0, p1 = x0 / (x0 + x1), x1 / (x0 + x1)
    chosen = r0 // gw
    gi = iota((groups, tok), 0)
    picked = jnp.sum(jnp.where(gi == chosen, group_prob, 0.0), axis=0, keepdims=True)
    w0 = (picked * p0).astype(BF).astype(F32)
    w1 = (picked * p1).astype(BF).astype(F32)
    li = iota((EXTRA, tok), 0) & (LOW_LANE - 1)
    diff = jnp.where(li == r0 - chosen * gw, 1.0, 0.0) - jnp.where(li == r1 - chosen * gw, 1.0, 0.0)
    group_side = jnp.where(li == GROUP_LANE + chosen, 1.0, 0.0)
    for j in range(groups):
        group_side = group_side - jnp.where(li == GROUP_LANE + j, group_prob[j : j + 1, :], 0.0)
    z0 = (p1 * diff + group_side).astype(BF)
    z1 = (group_side - p0 * diff).astype(BF)
    row = iota((EXTRA, tok), 0)
    aux = jnp.where(row == 0, p0, jnp.where(row == 1, p1, 0.0))
    for j in range(groups):
        aux = jnp.where(row == 2 + j, group_prob[j : j + 1, :], aux)
    aux_ref[...] = jnp.transpose(aux)
    before = ones_where(iota((tok, tok), 0) < iota((tok, tok), 1))
    blk = 128

    def step(b, carry):
        sub = iota((blk, tok), 0) & 7
        expert = b * 16 + (iota((blk, tok), 0) >> 3)
        hit0 = r0 == expert
        hit1 = r1 == expert
        rank = mm(ones_where(hit0 | hit1), before)
        match = rank == (2 * tp + (sub & 1)).astype(F32)
        one0 = jnp.where(hit0 & match, 1.0, 0.0)
        one1 = jnp.where(hit1 & match, 1.0, 0.0)
        one = one0 + one1
        scale = one0 * w0 + one1 * w1
        rows = pl.ds(pl.multiple_of(b * blk, blk), blk)
        got_tok, got_cot = None, None
        for c in range(4):
            here = (sub >> 1) == c
            cols = slice(c * width, (c + 1) * width)
            a = mm(jnp.where(here, one, 0.0).astype(BF), tok_ref[:, cols])
            d = mm(jnp.where(here, scale, 0.0).astype(BF), cot_ref[:, cols])
            got_tok = a if c == 0 else got_tok + a
            got_cot = d if c == 0 else got_cot + d
        send_ref[rows, 0:width] = got_tok.astype(BF)
        send_ref[rows, width : 2 * width] = got_cot.astype(BF)
        head = (sub >> 1) == 0
        side = nt(jnp.where(head, one0, 0.0).astype(BF), z0) + nt(jnp.where(head, one1, 0.0).astype(BF), z1)
        send_ref[rows, 2 * width :] = side.astype(BF)
        return carry

    lax.fori_loop(0, experts * 8 // blk, step, 0)


def expert_kernel(
    tp_ref, got_ref, gate_ref, up_ref, down_ref,
    x_ref, sc_ref, z_ref, gd_ref, ud_ref, hid_ref, u_ref, mine_ref, theirs_ref,
):
    tp = tp_ref[0]
    dm = gate_ref.shape[0]
    width, half = dm // 4, dm // 2
    o, i = iota((128, 128), 0), iota((128, 128), 1)
    perm = ones_where(i == ((o & 31) >> 1) * 8 + (o >> 5) * 2 + (o & 1))
    for b in range(got_ref.shape[0] // 128):
        block = slice(b * 128, (b + 1) * 128)
        rows = slice(b * 32, (b + 1) * 32)
        y = mm(perm, got_ref[block, 0 : 2 * width]).astype(BF)
        for c in range(4):
            cols = slice(c * width, (c + 1) * width)
            x_ref[rows, cols] = y[c * 32 : (c + 1) * 32, 0:width]
            sc_ref[rows, cols] = y[c * 32 : (c + 1) * 32, width:]
        z_ref[rows, :] = mm(perm[0:32], got_ref[block, 2 * width :]).astype(BF)
    gp = mm(x_ref[...], gate_ref[...])
    upre = mm(x_ref[...], up_ref[...])
    pulled = nt(sc_ref[...], down_ref[...])
    sig = 1.0 / (1.0 + jnp.exp(-gp))
    act = gp * sig
    hid = (act * upre).astype(BF)
    hid_ref[...] = hid
    u = jnp.sum(pulled * hid.astype(F32), axis=1, keepdims=True)
    gd = (pulled * (upre * sig * (1.0 + gp * (1.0 - sig)))).astype(BF)
    ud = (pulled * act).astype(BF)
    gd_ref[...] = gd
    ud_ref[...] = ud
    n = x_ref.shape[0]
    u_ref[...] = jnp.broadcast_to(u, (n, EXTRA))
    high = u.astype(BF).astype(F32)
    lane = iota((n, EXTRA), 1)
    theirs_ref[:, half:] = jnp.where(lane == 0, high, jnp.where(lane == 1, u - high, 0.0)).astype(BF)
    far = pl.ds(pl.multiple_of((1 - tp) * half, half), half)
    theirs_ref[:, 0:half] = (nt(gd, gate_ref[far, :]) + nt(ud, up_ref[far, :])).astype(BF)
    near = pl.ds(pl.multiple_of(tp * half, half), half)
    mine_ref[...] = (nt(gd, gate_ref[near, :]) + nt(ud, up_ref[near, :])).astype(BF)


def pack_kernel(tp_ref, *refs):
    tp = tp_ref[0]
    mine, came, us, zs, xs = refs[0:2], refs[2:4], refs[4:6], refs[6:8], refs[8:10]
    ret_ref, y0_ref, y1_ref, ul_ref = refs[10:14]
    n, half = mine[0].shape
    width = half // 2
    lane = iota((n, EXTRA), 1)
    for p, y_ref in ((0, y0_ref), (1, y1_ref)):
        u = us[p][...] + came[p][:, half : half + 1].astype(F32) + came[p][:, half + 1 : half + 2].astype(F32)
        y_ref[...] = (u * zs[p][...].astype(F32)).astype(BF)
        ul_ref[p * n : (p + 1) * n, :] = jnp.where(lane == U_LANE, u, 0.0).astype(BF)
    o, i = iota((128, 128), 0), iota((128, 128), 1)
    perm = ones_where(i == ((o >> 2) & 1) * 64 + ((o >> 1) & 1) * 32 + (o >> 3) * 2 + (o & 1))
    wide = iota((128, EXTRA), 1) < LOW_LANE
    for b in range(n // 32):
        rows = slice(b * 32, (b + 1) * 32)
        out = slice(b * 128, (b + 1) * 128)
        sums = [(mine[p][rows, :].astype(F32) + came[p][rows, 0:half].astype(F32)).astype(BF) for p in range(2)]
        stack = jnp.concatenate(
            [sums[0][:, 0:width], sums[1][:, 0:width], sums[0][:, width:], sums[1][:, width:]], axis=0
        )
        ret_ref[out, 0:width] = mm(perm, stack).astype(BF)
        ulane = jnp.concatenate([ul_ref[rows, :], ul_ref[n + b * 32 : n + (b + 1) * 32, :]], axis=0)
        base = mm(perm[:, 0:64], ulane)
        pieces = []
        for h in range(2):
            cols = slice(b * 256 + h * 128, b * 256 + (h + 1) * 128)
            rc = tn(xs[0][:, cols], y0_ref[...]) + tn(xs[1][:, cols], y1_ref[...])
            rc = rc.reshape(8, 16, EXTRA)
            pieces.append(jnp.where(tp == 0, rc[:, 0:8, :], rc[:, 8:16, :]).reshape(64, EXTRA))
        rc = jnp.concatenate(pieces, axis=0)
        high = rc.astype(BF).astype(F32)
        ret_ref[out, width:] = (base + jnp.where(wide, high, rc - high)).astype(BF)


def home_kernel(tp_ref, routes_ref, aux_ref, rg_ref, rex_ref, sel_ref, q_ref, h_ref):
    tp = tp_ref[0]
    tok = routes_ref.shape[0]
    half = q_ref.shape[1]
    groups = rg_ref.shape[0]
    experts = rex_ref.shape[1]
    gw = experts // groups
    r0, r1 = routes_ref[:, 0:1], routes_ref[:, 1:2]
    n = experts * 8
    col = iota((tok, n), 1)
    hit0 = r0 == (col >> 3)
    hit1 = r1 == (col >> 3)
    earlier = ones_where(iota((tok, tok), 1) < iota((tok, tok), 0))
    rank = mm(earlier, ones_where(hit0 | hit1))
    match = rank == ((2 * tp + (col & 3)) & 3).astype(F32)
    lower = (col & 4) == 0
    one0 = jnp.where(hit0 & match, 1.0, 0.0)
    one1 = jnp.where(hit1 & match, 1.0, 0.0)
    sel_ref[0] = jnp.where(lower, one0, 0.0).astype(BF)
    sel_ref[1] = jnp.where(lower, one1, 0.0).astype(BF)
    sel_ref[2] = jnp.where(lower, one0 + one1, 0.0).astype(BF)
    sel_ref[3] = jnp.where(lower, 0.0, one0 + one1).astype(BF)
    ei = iota((tok, experts), 1)
    pick = (jnp.where(ei == r0, 1.0, 0.0) - jnp.where(ei == r1, 1.0, 0.0)).astype(BF)
    near = pl.ds(pl.multiple_of(tp * half, half), half)
    q_ref[...] = nt(pick, rex_ref[near, :])
    h = None
    for j in range(groups):
        side = jnp.where(r0 // gw == j, 1.0, 0.0) - aux_ref[:, 2 + j : 3 + j]
        term = side * rg_ref[pl.ds(j, 1), near].astype(F32)
        h = term if j == 0 else h + term
    h_ref[...] = h


def final_kernel(back_ref, sel_ref, aux_ref, q_ref, h_ref, tg_ref, rex_ref, rg_ref, rows_ref):
    width = back_ref.shape[1] - EXTRA
    experts = rex_ref.shape[1]
    groups = rg_ref.shape[1]
    gw = experts // groups
    extra = back_ref[:, width:]
    u0 = mm(sel_ref[0], extra)[:, U_LANE : U_LANE + 1]
    u1 = mm(sel_ref[1], extra)[:, U_LANE : U_LANE + 1]
    lean = aux_ref[:, 1:2] * u0 - aux_ref[:, 0:1] * u1
    both = u0 + u1
    for c in range(2):
        cols = slice(c * width, (c + 1) * width)
        part = mm(sel_ref[2 + c], back_ref[:, 0:width])
        tg_ref[:, cols] = (part + (both * h_ref[:, cols] + lean * q_ref[:, cols])).astype(BF)
    sums = jnp.sum(extra.astype(F32).reshape(groups, gw, 8, EXTRA), axis=1)
    rg = None
    square = None
    for g in range(groups):
        s = sums[g]
        rex = s[:, 0:gw] + s[:, LOW_LANE : LOW_LANE + gw]
        grp = s[:, GROUP_LANE : GROUP_LANE + groups] + s[:, LOW_LANE + GROUP_LANE : LOW_LANE + GROUP_LANE + groups]
        rex_ref[:, g * gw : (g + 1) * gw] = rex
        rg = grp if g == 0 else rg + grp
        sq = jnp.sum(rex * rex, axis=1, keepdims=True)
        square = sq if g == 0 else square + sq
    rg_ref[...] = rg
    rows_ref[...] = square + jnp.sum(rg * rg, axis=1, keepdims=True)


def body(tokens, cotangent, routes, router_group, router_expert, gate_proj, up_proj, down_proj):
    tok, dm = tokens.shape
    experts = router_expert.shape[1]
    groups = router_group.shape[1]
    width, half = dm // 4, dm // 2
    ff = gate_proj.shape[2]
    n = experts * 2
    tp = lax.axis_index("tp").reshape(1)
    swap = [(0, 1), (1, 0)]
    rgt = router_group.T
    gate, up, down = gate_proj[0], up_proj[0], down_proj[0]

    def exchange(x):
        m = x.shape[1]
        y = lax.all_to_all(x.reshape(experts, 8, m), "ep", split_axis=0, concat_axis=0, tiled=True)
        return y.reshape(experts * 8, m)

    def partner(x):
        return lax.ppermute(x, "tp", swap)

    send, aux = call(
        pre_kernel, "pre", 1 << 30,
        [((experts * 8, 2 * width + EXTRA), BF), ((tok, EXTRA), F32)],
        [tp], [routes.T, tokens, cotangent, rgt, router_expert],
    )
    got = exchange(send)
    other = partner(got)
    x, sc, z, gd, ud, hid, u, mine, theirs = [list(v) for v in zip(*[
        call(
            expert_kernel, "expert", 3 << 30,
            [((n, dm), BF), ((n, dm), BF), ((n, EXTRA), BF), ((n, ff), BF), ((n, ff), BF), ((n, ff), BF),
             ((n, EXTRA), F32), ((n, half), BF), ((n, half + EXTRA), BF)],
            [tp], [g, gate, up, down],
        )
        for g in (got, other)
    ])]
    came = [partner(theirs[1]), partner(theirs[0])]
    ret = call_pack(tp, mine, came, u, z, x, experts, width)
    back = exchange(ret)
    sel, q, h = call(
        home_kernel, "home", 1 << 29,
        [((4, tok, experts * 8), BF), ((tok, half), F32), ((tok, half), F32)],
        [tp], [routes, aux, rgt, router_expert],
    )
    gate_total = tn(x[0], gd[0]) + tn(x[1], gd[1])
    up_total = tn(x[0], ud[0]) + tn(x[1], ud[1])
    down_total = tn(hid[0], sc[0]) + tn(hid[1], sc[1])
    sq = jnp.stack([jnp.sum(gate_total * gate_total, axis=1), jnp.sum(up_total * up_total, axis=1)])
    sq = sq + partner(sq)
    down_sq = jnp.sum(down_total * down_total, axis=1)
    token_grad, rex_grad, rg_grad, rows = call(
        final_kernel, "final", 1 << 29,
        [((tok, half), BF), ((8, experts), F32), ((8, groups), F32), ((8, 1), F32)],
        [], [back, sel, aux, q, h],
    )
    return (
        token_grad,
        gate_total.astype(BF)[None],
        up_total.astype(BF)[None],
        down_total.astype(BF)[None],
        sq[0:1],
        sq[1:2],
        down_sq[None],
        rex_grad,
        rg_grad,
        rows[:, 0],
    )


def call_pack(tp, mine, came, u, z, x, experts, width):
    n = mine[0].shape[0]
    vmem = pl.BlockSpec(memory_space=pltpu.VMEM)
    return pl.pallas_call(
        pack_kernel,
        name="pack",
        out_shape=jax.ShapeDtypeStruct((experts * 8, width + EXTRA), BF),
        in_specs=[pl.BlockSpec(memory_space=pltpu.SMEM)] + [vmem] * 10,
        out_specs=vmem,
        scratch_shapes=[pltpu.VMEM((n, EXTRA), BF), pltpu.VMEM((n, EXTRA), BF), pltpu.VMEM((2 * n, EXTRA), BF)],
        cost_estimate=pl.CostEstimate(flops=1 << 29, bytes_accessed=4 << 20, transcendentals=0),
        compiler_params=pltpu.CompilerParams(vmem_limit_bytes=56 << 20),
    )(tp, *mine, *came, *u, *z, *x)


def solution(mesh):
    return jax.shard_map(
        body,
        mesh=mesh,
        in_specs=(
            P("ep", None),
            P("ep", None),
            P("ep", None),
            P(),
            P(),
            P("ep", None, "tp"),
            P("ep", None, "tp"),
            P("ep", "tp", None),
        ),
        out_specs=(
            P("ep", "tp"),
            P("ep", None, "tp"),
            P("ep", None, "tp"),
            P("ep", "tp", None),
            P("ep", None),
            P("ep", None),
            P("ep", "tp"),
            P(("ep", "tp"), None),
            P(("ep", "tp"), None),
            P(("ep", "tp")),
        ),
        check_vma=False,
    )
```

profile of v0, /device:TPU:32, one launch (start us, length us, event | category | flops | bytes accessed | tf_op | source)
XLA Modules:
  0.0 158.7 jit_solution(14776293728920505200)
XLA Ops:
  0.6 8.1 %pre.1 = (bf16[1024,1152]{1,0:T(8,128)(2,1)}, f32[128,128]{1,0:T(8,128)}) custom-call(s32[1]{0:T(128)} %bitcast.tp_ref, s32[2,128]{1,0:T(2,128)} %bitcast.40, bf16[128,2048]{1,0:T(8,128)(2,1)} %tok_ref.1, bf16[128,2048]{1,0:T(8,128)(2,1)} %cot_ref.1, bf16[4,2048]{1,0:T(4,128)(2,1)} %bitcast.48, bf16[2048,128]{1,0:T(8,128)(2,1)} %rex_ref.3), custom_call_target="tpu_custom_call" | custom-call | flops 1073741824 | bytes 4194304 | tf_op jit(solution)/shard_map/pre/pallas_call | solution.py:35
  8.7 73.9 %all_to_all.10 = bf16[128,8,1152]{2,1,0:T(8,128)(2,1)S(1)} all-to-all(bf16[128,8,1152]{2,1,0:T(8,128)(2,1)} %bitcast.35), channel_id=1, replica_groups=mesh['ep'=128,'tp'=2] {'ep'}, dimensions={0} | all-to-all | bytes 4718592 | tf_op jit(solution)/shard_map/all_to_all | solution.py:269
  82.6 0.0 collective-permute-start
  82.6 1.4 copy-done.3
  84.1 6.3 %expert.2 = (bf16[256,2048]{1,0:T(8,128)(2,1)}, bf16[256,2048]{1,0:T(8,128)(2,1)}, bf16[256,128]{1,0:T(8,128)(2,1)}, bf16[256,256]{1,0:T(8,128)(2,1)}, bf16[256,...) custom-call(s32[1]{0:T(128)} %bitcast.tp_ref, ...), custom_call_target="tpu_custom_call" | custom-call | flops 3221225472 | bytes 4194304 | tf_op jit(solution)/shard_map/expert/pallas_call | solution.py:35
  90.4 0.0 collective-permute-start.2
  90.4 0.0 collective-permute-done.got_ref
  90.4 0.0 copy-start.15
  90.4 1.4 copy-done.15
  91.8 6.3 %expert.3 = (bf16[256,2048]{1,0:T(8,128)(2,1)}, bf16[256,2048]{1,0:T(8,128)(2,1)}, bf16[256,128]{1,0:T(8,128)(2,1)}, bf16[256,256]{1,0:T(8,128)(2,1)}, bf16[256,...) custom-call(s32[1]{0:T(128)} %bitcast.tp_ref, ...), custom_call_target="tpu_custom_call" | custom-call | flops 3221225472 | bytes 4194304 | tf_op jit(solution)/shard_map/expert/pallas_call | solution.py:35
  98.2 0.5 collective-permute-start.1
  98.7 0.0 copy-done.14
  98.7 0.7 copy.22.routes_ref
  99.4 3.0 %home.1 = (bf16[4,128,1024]{2,1,0:T(8,128)(2,1)}, f32[128,1024]{1,0:T(8,128)}, f32[128,1024]{1,0:T(8,128)}) custom-call(s32[1]{0:T(128)} %bitcast.tp_ref, s32[128,2]{1,0:T(8,128)} %copy.22.routes_ref, f32[128,128]{1,0:T(8,128)} %get-tuple-element.48.aux_ref, bf16[4,2048]{1,0:T(4,128)(2,1)} %bitcast.49, bf16[2048,128]{1,0:T(8,128)(2,1)} %rex_ref.3), custom_call_target="tpu_custom_call" | custom-call | flops 536870912 | bytes 4194304 | tf_op jit(solution)/shard_map/home/pallas_call | solution.py:35
  102.4 0.0 collective-permute-done.2.refs_3_
  102.4 0.0 collective-permute-done.1.refs_2_
  102.4 0.0 copy-start.7
  102.4 0.8 copy-done.6
  103.2 0.2 copy-done.7
  103.4 4.6 %pack.1 = bf16[1024,640]{1,0:T(8,128)(2,1)} custom-call(s32[1]{0:T(128)} %bitcast.tp_ref, bf16[256,1024]{1,0:T(8,128)(2,1)} %get-tuple-element.38.refs_0_, bf16[256,1024]{1,0:T(8,128)(2,1)} %get-tuple-element.39.refs_1_, bf16[256,1152]{1,0:T(8,128)(2,1)} %copy-done.7, bf16[256,1152]{1,0:T(8,128)(2,1)} %copy-done.6, f32[256,128]{1,0:T(8,128)} %get-tuple-element.42.refs_4_, ...), custom_call_target="tpu_custom_call" | custom-call | flops 536870912 | bytes 4194304 | tf_op jit(solution)/shard_map/pack/pallas_call | solution.py:327
  108.0 6.7 %all-to-all-start.1 = ((bf16[128,8,640]{2,1,0:T(8,128)(2,1)}), bf16[128,8,640]{2,1,0:T(8,128)(2,1)S(1)}, u32[]{:S(2)}, u32[]{:S(2)}) async-start(bf16[128,8,640]{2,1,0:T(8,128)(2,1)} %bitcast.32), calls=%async_computation.1 | async-start | bytes 2621440 | tf_op jit(solution)/shard_map/all_to_all | solution.py:269
  114.8 0.0 copy-start.10
  114.8 0.0 copy-done
  114.8 0.0 copy-done.11
  114.8 0.5 fusion.2
  115.3 0.0 copy-start.5
  115.3 0.0 copy-start.9
  115.3 0.4 copy-done.10
  115.7 0.5 fusion.3
  116.2 0.0 copy-start.1
  116.2 0.3 copy-done.5
  116.5 0.5 fusion.4
  117.0 0.5 copy-done.1
  117.5 0.5 multiply_reduce_fusion.2
  118.0 0.4 copy-done.12
  118.4 0.5 multiply_reduce_fusion.1
  119.0 0.1 collective-permute-start.3
  119.1 0.6 copy-done.4
  119.6 2.0 %multiply_reduce_fusion = (f32[256]{0:T(256)}, bf16[1,256,2048]{2,1,0:T(8,128)(2,1)}) fusion(f32[256,2048]{1,0:T(8,128)S(1)} %fusion.4, bf16[256,256]{1,0:T(8,128)(2,1)S(1)} %copy-done.8, bf16[256,2048]{1,0:T(8,128)(2,1)S(1)} %copy-done.4), kind=kOutput, calls=%fused_computation.3 | convolution fusion | flops 270532352 | bytes 4326400 | tf_op jit(solution)/shard_map/dot_general | solution.py:25
  121.6 1.3 copy.23
  122.9 1.3 copy.24
  124.2 0.0 collective-permute-done.3
  124.3 0.6 fusion.1
  124.9 27.0 %all-to-all-done.1 = bf16[128,8,640]{2,1,0:T(8,128)(2,1)S(1)} async-done(((bf16[128,8,640]{2,1,0:T(8,128)(2,1)}), bf16[128,8,640]{2,1,0:T(8,128)(2,1)S(1)}, u32[]{:S(2)}, u32[]{:S(2)}) %all-to-all-start.1) | async-done | bytes 1310752 | tf_op jit(solution)/shard_map/all_to_all | solution.py:269
  151.8 1.1 copy-done.2
  152.9 3.2 %final.1 = (bf16[128,1024]{1,0:T(8,128)(2,1)}, f32[8,128]{1,0:T(8,128)}, f32[8,4]{1,0:T(8,128)}, f32[8,1]{1,0:T(8,128)}) custom-call(bf16[1024,640]{1,0:T(8,128)(2,1)} %bitcast.31, bf16[4,128,1024]{2,1,0:T(8,128)(2,1)} %get-tuple-element.49.sel_ref, f32[128,128]{1,0:T(8,128)} %get-tuple-element.48.aux_ref, f32[128,1024]{1,0:T(8,128)} %get-tuple-element.50.q_ref, ...), custom_call_target="tpu_custom_call" | custom-call | flops 536870912 | bytes 4194304 | tf_op jit(solution)/shard_map/final/pallas_call | solution.py:35
  156.1 1.3 copy.25
  157.4 1.3 reduce
  (15 shorter events, 0.1 us)
Async XLA Ops:
  82.6 1.4 copy-start.3
  82.6 7.8 %collective-permute-start = (bf16[1024,1152]{1,0:T(8,128)(2,1)S(1)}, bf16[1024,1152]{1,0:T(8,128)(2,1)S(1)}, u32[]{:S(2)}, u32[]{:S(2)}) collective-permute-start(bf16[1024,1152]{1,0:T(8,128)(2,1)S(1)} %bitcast.33), channel_id=1, source_target_pairs={{0,1},{1,0},{2,3},{3,2},{4,5},{5,4},{6,7},{7,6},{8,9},{9,8},{10,11... | collective-permute-start | bytes 7077896 | tf_op jit(solution)/shard_map/ppermute | solution.py:273
  90.4 8.3 %copy-start.14 = (s32[128,2]{0,1:T(2,128)S(1)}, s32[128,2]{0,1:T(2,128)}, u32[]{:S(2)}) copy-start(s32[128,2]{0,1:T(2,128)} %param.10) | copy-start | bytes 3076
  90.4 12.0 %collective-permute-start.2 = (bf16[256,1152]{1,0:T(8,128)(2,1)}, bf16[256,1152]{1,0:T(8,128)(2,1)S(1)}, u32[]{:S(2)}, u32[]{:S(2)}) collective-permute-start(bf16[256,1152]{1,0:T(8,128)(2,1)} %get-tuple-element.41), channel_id=1, source_target_pairs={{0,1},{1,0},{2,3},{3,2},{4,5},{5,4},{6,7},{7,6},{8,9},{9,8},{10,11... | collective-permute-start | bytes 1769480 | tf_op jit(solution)/shard_map/ppermute | solution.py:273
  90.4 1.4 copy-start.15
  98.2 4.2 %collective-permute-start.1 = (bf16[256,1152]{1,0:T(8,128)(2,1)}, bf16[256,1152]{1,0:T(8,128)(2,1)S(1)}, u32[]{:S(2)}, u32[]{:S(2)}) collective-permute-start(bf16[256,1152]{1,0:T(8,128)(2,1)} %get-tuple-element.40), channel_id=1, source_target_pairs={{0,1},{1,0},{2,3},{3,2},{4,5},{5,4},{6,7},{7,6},{8,9},{9,8},{10,11... | collective-permute-start | bytes 1769480 | tf_op jit(solution)/shard_map/ppermute | solution.py:273
  102.4 0.8 copy-start.6
  102.4 1.0 copy-start.7
  108.0 6.7 %copy-start = (bf16[256,2048]{1,0:T(8,128)(2,1)S(1)}, bf16[256,2048]{1,0:T(8,128)(2,1)}, u32[]{:S(2)}) copy-start(bf16[256,2048]{1,0:T(8,128)(2,1)} %get-tuple-element.46.refs_8_) | copy-start | bytes 3145732
  108.0 6.8 %copy-start.11 = (bf16[256,256]{1,0:T(8,128)(2,1)S(1)}, bf16[256,256]{1,0:T(8,128)(2,1)}, u32[]{:S(2)}) copy-start(bf16[256,256]{1,0:T(8,128)(2,1)} %get-tuple-element.53) | copy-start | bytes 393220
  108.0 43.8 %all-to-all-start.1 = ((bf16[128,8,640]{2,1,0:T(8,128)(2,1)}), bf16[128,8,640]{2,1,0:T(8,128)(2,1)S(1)}, u32[]{:S(2)}, u32[]{:S(2)}) async-start(bf16[128,8,640]{2,1,0:T(8,128)(2,1)} %bitcast.32), calls=%async_computation.1 | async-start | bytes 2621440 | tf_op jit(solution)/shard_map/all_to_all | solution.py:269
  114.8 0.9 copy-start.10
  115.3 1.2 copy-start.5
  115.3 1.2 copy-start.9
  116.2 1.3 copy-start.1
  116.2 1.3 copy-start.13
  117.5 0.9 copy-start.12
  118.4 1.2 copy-start.4
  118.4 1.2 copy-start.8
  119.0 5.3 %collective-permute-start.3 = (f32[2,2048]{1,0:T(2,128)S(1)}, f32[2,2048]{1,0:T(2,128)S(1)}, u32[]{:S(2)}, u32[]{:S(2)}) collective-permute-start(f32[2,2048]{1,0:T(2,128)S(1)} %pad_maximum_fusion), channel_id=1, source_target_pairs={{0,1},{1,0},{2,3},{3,2},{4,5},{5,4},{6,7},{7,6},{8,9},{9,8},{10,11... | collective-permute-start | bytes 49160 | tf_op jit(solution)/shard_map/ppermute | solution.py:273
  151.8 1.1 copy-start.2
where the time goes:
time: 159 us
  blocking collectives  73.9 us (46%)
  Pallas kernels  31.5 us (20%)
  waiting for transfers between devices  27 us (17%)
  local copies, waits for them, and re-layouts  12.4 us (8%)
  starting transfers between devices  7.31 us (5%)
  matrix products  4.5 us (3%)
    all_to_all x1, blocking collectives, exchange(): lax.all_to_all(x.reshape(experts, 8, m), 'ep', split_axis=0, concat_axis=...  73.9 us
    all_to_all x1, waiting for transfers between devices, exchange(): lax.all_to_all(x.reshape(experts, 8, m), 'ep', split_axis=0, concat_axis=...  27 us
    pallas_call x5, Pallas kernels, call(): pl.pallas_call(kernel, name=name, out_shape=[jax.ShapeDtypeStruct(shape,...  26.9 us
    unnamed x36, local copies, waits for them, and re-layouts  11.8 us
    all_to_all x1, starting transfers between devices, exchange(): lax.all_to_all(x.reshape(experts, 8, m), 'ep', split_axis=0, concat_axis=...  6.72 us
    pallas_call x1, Pallas kernels, call_pack(): pl.pallas_call(pack_kernel, name='pack', out_shape=jax.ShapeDtypeStruct((...  4.64 us
    dot_general x6, matrix products, tn(): lax.dot_general(a, b, (((0,), (0,)), ((), ())), preferred_element_type=F32)  4.5 us
  transfers between devices with their start and end apart: 5, of which 1 were waited for; matrix products, arithmetic and copies ran while one was open for 5% of the time, Pallas kernels for 10%

commit v1 on v0

--- a/solution.py
+++ b/solution.py
@@ -29,17 +29,18 @@
     return lax.broadcasted_iota(jnp.int32, shape, dim)
 
 
-def call(kernel, name, flops, outs, scalars, arrays):
+def call(kernel, name, flops, limit, outs, scalars, arrays, scratch=(), spaces=None):
     smem = pl.BlockSpec(memory_space=pltpu.SMEM)
     vmem = pl.BlockSpec(memory_space=pltpu.VMEM)
     return pl.pallas_call(
         kernel,
         name=name,
         out_shape=[jax.ShapeDtypeStruct(shape, dtype) for shape, dtype in outs],
-        in_specs=[smem] * len(scalars) + [vmem] * len(arrays),
+        in_specs=[smem] * len(scalars) + (spaces or [vmem] * len(arrays)),
         out_specs=[vmem] * len(outs),
+        scratch_shapes=list(scratch),
         cost_estimate=pl.CostEstimate(flops=flops, bytes_accessed=4 << 20, transcendentals=0),
-        compiler_params=pltpu.CompilerParams(vmem_limit_bytes=56 << 20),
+        compiler_params=pltpu.CompilerParams(vmem_limit_bytes=limit << 20),
     )(*scalars, *arrays)
 
 
@@ -47,14 +48,52 @@
     return jnp.where(mask, 1.0, 0.0).astype(BF)
 
 
-def pre_kernel(tp_ref, rt_ref, tok_ref, cot_ref, rgt_ref, rex_ref, send_ref, aux_ref):
+def pre_kernel(
+    tp_ref, rt_ref, rgt_ref, tok_hbm, cot_hbm, rex_hbm,
+    send_ref, aux_ref, tok_ref, cot_ref, rex_ref, one_ref, sems,
+):
     tp = tp_ref[0]
     tok, dm = tok_ref.shape
     experts = rex_ref.shape[1]
     groups = rgt_ref.shape[0]
     gw = experts // groups
     width = dm // 4
+    loads = [
+        pltpu.make_async_copy(src, dst, sems.at[k])
+        for k, (src, dst) in enumerate(((tok_hbm, tok_ref), (rex_hbm, rex_ref), (cot_hbm, cot_ref)))
+    ]
+    for load in loads:
+        load.start()
     r0, r1 = rt_ref[0:1, :], rt_ref[1:2, :]
+    before = ones_where(iota((tok, tok), 0) < iota((tok, tok), 1))
+    blk = min(256, experts * 8)
+    blocks = experts * 8 // blk
+    row = iota((blk, tok), 0)
+    sub = row & 7
+    want = (2 * tp + (sub & 1)).astype(F32)
+    part = sub >> 1
+    for b in range(blocks):
+        rows = slice(b * blk, (b + 1) * blk)
+        expert = b * (blk // 8) + (row >> 3)
+        hit0 = r0 == expert
+        hit1 = r1 == expert
+        match = mm(ones_where(hit0 | hit1), before) == want
+        one_ref[0, rows, :] = ones_where(hit0 & match)
+        one_ref[1, rows, :] = ones_where(hit1 & match)
+
+    def spread(sel):
+        return jnp.concatenate([jnp.where(part == c, sel, 0.0).astype(BF) for c in range(4)], axis=1)
+
+    def stacked(ref):
+        return jnp.concatenate([ref[:, c * width : (c + 1) * width] for c in range(4)], axis=0)
+
+    loads[0].wait()
+    stack = stacked(tok_ref)
+    for b in range(blocks):
+        rows = slice(b * blk, (b + 1) * blk)
+        one = one_ref[0, rows, :].astype(F32) + one_ref[1, rows, :].astype(F32)
+        send_ref[rows, 0:width] = mm(spread(one), stack).astype(BF)
+    loads[1].wait()
     group_exp = jnp.exp(nt(rgt_ref[...], tok_ref[...]))
     group_prob = group_exp / jnp.sum(group_exp, axis=0, keepdims=True)
     logits = jnp.transpose(mm(tok_ref[...], rex_ref[...]))
@@ -73,44 +112,24 @@
     group_side = jnp.where(li == GROUP_LANE + chosen, 1.0, 0.0)
     for j in range(groups):
         group_side = group_side - jnp.where(li == GROUP_LANE + j, group_prob[j : j + 1, :], 0.0)
-    z0 = (p1 * diff + group_side).astype(BF)
-    z1 = (group_side - p0 * diff).astype(BF)
-    row = iota((EXTRA, tok), 0)
-    aux = jnp.where(row == 0, p0, jnp.where(row == 1, p1, 0.0))
+    side_t = jnp.concatenate([(p1 * diff + group_side).astype(BF), (group_side - p0 * diff).astype(BF)], axis=1)
+    arow = iota((EXTRA, tok), 0)
+    aux = jnp.where(arow == 0, p0, jnp.where(arow == 1, p1, 0.0))
     for j in range(groups):
-        aux = jnp.where(row == 2 + j, group_prob[j : j + 1, :], aux)
+        aux = jnp.where(arow == 2 + j, group_prob[j : j + 1, :], aux)
+    aux = jnp.where(arow == 6, r0.astype(F32), jnp.where(arow == 7, r1.astype(F32), aux))
     aux_ref[...] = jnp.transpose(aux)
-    before = ones_where(iota((tok, tok), 0) < iota((tok, tok), 1))
-    blk = 128
-
-    def step(b, carry):
-        sub = iota((blk, tok), 0) & 7
-        expert = b * 16 + (iota((blk, tok), 0) >> 3)
-        hit0 = r0 == expert
-        hit1 = r1 == expert
-        rank = mm(ones_where(hit0 | hit1), before)
-        match = rank == (2 * tp + (sub & 1)).astype(F32)
-        one0 = jnp.where(hit0 & match, 1.0, 0.0)
-        one1 = jnp.where(hit1 & match, 1.0, 0.0)
-        one = one0 + one1
-        scale = one0 * w0 + one1 * w1
-        rows = pl.ds(pl.multiple_of(b * blk, blk), blk)
-        got_tok, got_cot = None, None
-        for c in range(4):
-            here = (sub >> 1) == c
-            cols = slice(c * width, (c + 1) * width)
-            a = mm(jnp.where(here, one, 0.0).astype(BF), tok_ref[:, cols])
-            d = mm(jnp.where(here, scale, 0.0).astype(BF), cot_ref[:, cols])
-            got_tok = a if c == 0 else got_tok + a
-            got_cot = d if c == 0 else got_cot + d
-        send_ref[rows, 0:width] = got_tok.astype(BF)
-        send_ref[rows, width : 2 * width] = got_cot.astype(BF)
-        head = (sub >> 1) == 0
-        side = nt(jnp.where(head, one0, 0.0).astype(BF), z0) + nt(jnp.where(head, one1, 0.0).astype(BF), z1)
-        send_ref[rows, 2 * width :] = side.astype(BF)
-        return carry
-
-    lax.fori_loop(0, experts * 8 // blk, step, 0)
+    loads[2].wait()
+    stack = stacked(cot_ref)
+    for b in range(blocks):
+        rows = slice(b * blk, (b + 1) * blk)
+        one0, one1 = one_ref[0, rows, :].astype(F32), one_ref[1, rows, :].astype(F32)
+        send_ref[rows, width : 2 * width] = mm(spread(one0 * w0 + one1 * w1), stack).astype(BF)
+        head = part == 0
+        both = jnp.concatenate(
+            [jnp.where(head, one0, 0.0).astype(BF), jnp.where(head, one1, 0.0).astype(BF)], axis=1
+        )
+        send_ref[rows, 2 * width :] = nt(both, side_t).astype(BF)
 
 
 def expert_kernel(
@@ -120,17 +139,20 @@
     tp = tp_ref[0]
     dm = gate_ref.shape[0]
     width, half = dm // 4, dm // 2
-    o, i = iota((128, 128), 0), iota((128, 128), 1)
-    perm = ones_where(i == ((o & 31) >> 1) * 8 + (o >> 5) * 2 + (o & 1))
-    for b in range(got_ref.shape[0] // 128):
-        block = slice(b * 128, (b + 1) * 128)
-        rows = slice(b * 32, (b + 1) * 32)
+    blk = min(256, got_ref.shape[0])
+    n4 = blk // 4
+    shift = n4.bit_length() - 1
+    o, i = iota((blk, blk), 0), iota((blk, blk), 1)
+    perm = ones_where(i == ((o & (n4 - 1)) >> 1) * 8 + (o >> shift) * 2 + (o & 1))
+    for b in range(got_ref.shape[0] // blk):
+        block = slice(b * blk, (b + 1) * blk)
+        rows = slice(b * n4, (b + 1) * n4)
         y = mm(perm, got_ref[block, 0 : 2 * width]).astype(BF)
         for c in range(4):
             cols = slice(c * width, (c + 1) * width)
-            x_ref[rows, cols] = y[c * 32 : (c + 1) * 32, 0:width]
-            sc_ref[rows, cols] = y[c * 32 : (c + 1) * 32, width:]
-        z_ref[rows, :] = mm(perm[0:32], got_ref[block, 2 * width :]).astype(BF)
+            x_ref[rows, cols] = y[c * n4 : (c + 1) * n4, 0:width]
+            sc_ref[rows, cols] = y[c * n4 : (c + 1) * n4, width:]
+        z_ref[rows, :] = mm(perm[0:n4], got_ref[block, 2 * width :]).astype(BF)
     gp = mm(x_ref[...], gate_ref[...])
     upre = mm(x_ref[...], up_ref[...])
     pulled = nt(sc_ref[...], down_ref[...])
@@ -165,38 +187,69 @@
         u = us[p][...] + came[p][:, half : half + 1].astype(F32) + came[p][:, half + 1 : half + 2].astype(F32)
         y_ref[...] = (u * zs[p][...].astype(F32)).astype(BF)
         ul_ref[p * n : (p + 1) * n, :] = jnp.where(lane == U_LANE, u, 0.0).astype(BF)
-    o, i = iota((128, 128), 0), iota((128, 128), 1)
-    perm = ones_where(i == ((o >> 2) & 1) * 64 + ((o >> 1) & 1) * 32 + (o >> 3) * 2 + (o & 1))
-    wide = iota((128, EXTRA), 1) < LOW_LANE
-    for b in range(n // 32):
-        rows = slice(b * 32, (b + 1) * 32)
-        out = slice(b * 128, (b + 1) * 128)
+    blk = min(256, n * 4)
+    bs = blk // 8
+    o, i = iota((blk, blk), 0), iota((blk, blk), 1)
+    perm = ones_where(i == ((o >> 2) & 1) * (4 * bs) + ((o >> 1) & 1) * (2 * bs) + (o >> 3) * 2 + (o & 1))
+    wide = iota((blk, EXTRA), 1) < LOW_LANE
+    for b in range(n // (2 * bs)):
+        rows = slice(b * 2 * bs, (b + 1) * 2 * bs)
+        out = slice(b * blk, (b + 1) * blk)
         sums = [(mine[p][rows, :].astype(F32) + came[p][rows, 0:half].astype(F32)).astype(BF) for p in range(2)]
         stack = jnp.concatenate(
             [sums[0][:, 0:width], sums[1][:, 0:width], sums[0][:, width:], sums[1][:, width:]], axis=0
         )
         ret_ref[out, 0:width] = mm(perm, stack).astype(BF)
-        ulane = jnp.concatenate([ul_ref[rows, :], ul_ref[n + b * 32 : n + (b + 1) * 32, :]], axis=0)
-        base = mm(perm[:, 0:64], ulane)
-        pieces = []
-        for h in range(2):
-            cols = slice(b * 256 + h * 128, b * 256 + (h + 1) * 128)
-            rc = tn(xs[0][:, cols], y0_ref[...]) + tn(xs[1][:, cols], y1_ref[...])
-            rc = rc.reshape(8, 16, EXTRA)
-            pieces.append(jnp.where(tp == 0, rc[:, 0:8, :], rc[:, 8:16, :]).reshape(64, EXTRA))
-        rc = jnp.concatenate(pieces, axis=0)
+        ulane = jnp.concatenate([ul_ref[rows, :], ul_ref[n + b * 2 * bs : n + (b + 1) * 2 * bs, :]], axis=0)
+        base = mm(perm[:, 0 : 4 * bs], ulane)
+        cols = slice(b * 16 * bs, (b + 1) * 16 * bs)
+        rc = tn(xs[0][:, cols], y0_ref[...]) + tn(xs[1][:, cols], y1_ref[...])
+        rc = rc.reshape(bs, 16, EXTRA)
+        rc = jnp.where(tp == 0, rc[:, 0:8, :], rc[:, 8:16, :]).reshape(blk, EXTRA)
         high = rc.astype(BF).astype(F32)
         ret_ref[out, width:] = (base + jnp.where(wide, high, rc - high)).astype(BF)
 
 
-def home_kernel(tp_ref, routes_ref, aux_ref, rg_ref, rex_ref, sel_ref, q_ref, h_ref):
+def grads_kernel(*refs):
+    x, sc, gd, ud, hid = (refs[2 * k : 2 * k + 2] for k in range(5))
+    gate_ref, up_ref, down_ref, sq_ref, down_sq_ref, acc_ref = refs[10:]
+    dm, ff = gate_ref.shape
+    blk = 128
+    wide = 512 if dm % 512 == 0 else 128
+
+    def as_row(col):
+        return jnp.transpose(jnp.broadcast_to(col, (col.shape[0], 128)))[0:1, :]
+
+    def step(b, carry):
+        cols = pl.ds(pl.multiple_of(b * blk, blk), blk)
+        for k, (delta, out_ref) in enumerate(((gd, gate_ref), (ud, up_ref))):
+            full = tn(x[0][:, cols], delta[0][...]) + tn(x[1][:, cols], delta[1][...])
+            out_ref[cols, :] = full.astype(BF)
+            sq_ref[k : k + 1, cols] = as_row(jnp.sum(full * full, axis=1, keepdims=True))
+        return carry
+
+    lax.fori_loop(0, dm // blk, step, 0)
+    acc_ref[...] = jnp.zeros_like(acc_ref)
+
+    def down_step(b, carry):
+        cols = pl.ds(pl.multiple_of(b * wide, wide), wide)
+        full = tn(hid[0][...], sc[0][:, cols]) + tn(hid[1][...], sc[1][:, cols])
+        down_ref[:, cols] = full.astype(BF)
+        acc_ref[...] += jnp.broadcast_to(jnp.sum(full * full, axis=1, keepdims=True), acc_ref.shape)
+        return carry
+
+    lax.fori_loop(0, dm // wide, down_step, 0)
+    down_sq_ref[...] = jnp.transpose(acc_ref[...])[0:1, :]
+
+
+def home_kernel(tp_ref, aux_ref, rg_ref, rex_ref, sel_ref, q_ref, h_ref):
     tp = tp_ref[0]
-    tok = routes_ref.shape[0]
+    tok = aux_ref.shape[0]
     half = q_ref.shape[1]
     groups = rg_ref.shape[0]
     experts = rex_ref.shape[1]
     gw = experts // groups
-    r0, r1 = routes_ref[:, 0:1], routes_ref[:, 1:2]
+    r0, r1 = aux_ref[:, 6:7].astype(jnp.int32), aux_ref[:, 7:8].astype(jnp.int32)
     n = experts * 8
     col = iota((tok, n), 1)
     hit0 = r0 == (col >> 3)
@@ -223,10 +276,15 @@
     h_ref[...] = h
 
 
-def final_kernel(back_ref, sel_ref, aux_ref, q_ref, h_ref, tg_ref, rex_ref, rg_ref, rows_ref):
+def final_kernel(
+    back_ref, sel_ref, aux_ref, q_ref, h_ref, sq_ref, sqo_ref,
+    tg_ref, rex_ref, rg_ref, rows_ref, gate_sq_ref, up_sq_ref,
+):
+    gate_sq_ref[...] = sq_ref[0:1, :] + sqo_ref[0:1, :]
+    up_sq_ref[...] = sq_ref[1:2, :] + sqo_ref[1:2, :]
     width = back_ref.shape[1] - EXTRA
     experts = rex_ref.shape[1]
-    groups = rg_ref.shape[1]
+    groups = rg_ref.shape[0]
     gw = experts // groups
     extra = back_ref[:, width:]
     u0 = mm(sel_ref[0], extra)[:, U_LANE : U_LANE + 1]
@@ -240,16 +298,20 @@
     sums = jnp.sum(extra.astype(F32).reshape(groups, gw, 8, EXTRA), axis=1)
     rg = None
     square = None
+    lane = iota((8, EXTRA), 1)
     for g in range(groups):
         s = sums[g]
-        rex = s[:, 0:gw] + s[:, LOW_LANE : LOW_LANE + gw]
-        grp = s[:, GROUP_LANE : GROUP_LANE + groups] + s[:, LOW_LANE + GROUP_LANE : LOW_LANE + GROUP_LANE + groups]
+        s = s + jnp.concatenate([s[:, LOW_LANE:], s[:, 0:LOW_LANE]], axis=1)
+        rex = s[:, 0:gw]
         rex_ref[:, g * gw : (g + 1) * gw] = rex
-        rg = grp if g == 0 else rg + grp
+        rg = s if g == 0 else rg + s
         sq = jnp.sum(rex * rex, axis=1, keepdims=True)
         square = sq if g == 0 else square + sq
-    rg_ref[...] = rg
-    rows_ref[...] = square + jnp.sum(rg * rg, axis=1, keepdims=True)
+    grp = rg[:, GROUP_LANE : GROUP_LANE + groups]
+    square = square + jnp.sum(grp * grp, axis=1, keepdims=True)
+    rest = jnp.transpose(jnp.where(lane == GROUP_LANE + groups, square, rg))
+    rg_ref[...] = rest[GROUP_LANE : GROUP_LANE + groups, :]
+    rows_ref[...] = rest[GROUP_LANE + groups : GROUP_LANE + groups + 1, :]
 
 
 def body(tokens, cotangent, routes, router_group, router_expert, gate_proj, up_proj, down_proj):
@@ -273,15 +335,20 @@
         return lax.ppermute(x, "tp", swap)
 
     send, aux = call(
-        pre_kernel, "pre", 1 << 30,
+        pre_kernel, "pre", 1 << 30, 20,
         [((experts * 8, 2 * width + EXTRA), BF), ((tok, EXTRA), F32)],
-        [tp], [routes.T, tokens, cotangent, rgt, router_expert],
+        [tp], [routes.T, rgt, tokens, cotangent, router_expert],
+        scratch=[
+            pltpu.VMEM((tok, dm), BF), pltpu.VMEM((tok, dm), BF), pltpu.VMEM((dm, experts), BF),
+            pltpu.VMEM((2, experts * 8, tok), BF), pltpu.SemaphoreType.DMA((3,)),
+        ],
+        spaces=[pl.BlockSpec(memory_space=pltpu.VMEM)] * 2 + [pl.BlockSpec(memory_space=pl.ANY)] * 3,
     )
     got = exchange(send)
     other = partner(got)
     x, sc, z, gd, ud, hid, u, mine, theirs = [list(v) for v in zip(*[
         call(
-            expert_kernel, "expert", 3 << 30,
+            expert_kernel, "expert", 3 << 30, 18,
             [((n, dm), BF), ((n, dm), BF), ((n, EXTRA), BF), ((n, ff), BF), ((n, ff), BF), ((n, ff), BF),
              ((n, EXTRA), F32), ((n, half), BF), ((n, half + EXTRA), BF)],
             [tp], [g, gate, up, down],
@@ -292,32 +359,33 @@
     ret = call_pack(tp, mine, came, u, z, x, experts, width)
     back = exchange(ret)
     sel, q, h = call(
-        home_kernel, "home", 1 << 29,
+        home_kernel, "home", 1 << 29, 8,
         [((4, tok, experts * 8), BF), ((tok, half), F32), ((tok, half), F32)],
-        [tp], [routes, aux, rgt, router_expert],
-    )
-    gate_total = tn(x[0], gd[0]) + tn(x[1], gd[1])
-    up_total = tn(x[0], ud[0]) + tn(x[1], ud[1])
-    down_total = tn(hid[0], sc[0]) + tn(hid[1], sc[1])
-    sq = jnp.stack([jnp.sum(gate_total * gate_total, axis=1), jnp.sum(up_total * up_total, axis=1)])
-    sq = sq + partner(sq)
-    down_sq = jnp.sum(down_total * down_total, axis=1)
-    token_grad, rex_grad, rg_grad, rows = call(
-        final_kernel, "final", 1 << 29,
-        [((tok, half), BF), ((8, experts), F32), ((8, groups), F32), ((8, 1), F32)],
-        [], [back, sel, aux, q, h],
+        [tp], [aux, rgt, router_expert],
+    )
+    gate_grad, up_grad, down_grad, sq, down_sq = call(
+        grads_kernel, "grads", 3 << 30, 20,
+        [((dm, ff), BF), ((dm, ff), BF), ((ff, dm), BF), ((2, dm), F32), ((1, ff), F32)],
+        [], [*x, *sc, *gd, *ud, *hid], scratch=[pltpu.VMEM((ff, 128), F32)],
+    )
+    sq_other = partner(sq)
+    token_grad, rex_grad, rg_grad, rows, gate_sq, up_sq = call(
+        final_kernel, "final", 1 << 29, 10,
+        [((tok, half), BF), ((8, experts), F32), ((groups, 8), F32), ((1, 8), F32),
+         ((1, dm), F32), ((1, dm), F32)],
+        [], [back, sel, aux, q, h, sq, sq_other],
     )
     return (
         token_grad,
-        gate_total.astype(BF)[None],
-        up_total.astype(BF)[None],
-        down_total.astype(BF)[None],
-        sq[0:1],
-        sq[1:2],
-        down_sq[None],
+        gate_grad[None],
+        up_grad[None],
+        down_grad[None],
+        gate_sq,
+        up_sq,
+        down_sq,
         rex_grad,
-        rg_grad,
-        rows[:, 0],
+        rg_grad.T,
+        rows[0],
     )
 
 
@@ -332,7 +400,7 @@
         out_specs=vmem,
         scratch_shapes=[pltpu.VMEM((n, EXTRA), BF), pltpu.VMEM((n, EXTRA), BF), pltpu.VMEM((2 * n, EXTRA), BF)],
         cost_estimate=pl.CostEstimate(flops=1 << 29, bytes_accessed=4 << 20, transcendentals=0),
-        compiler_params=pltpu.CompilerParams(vmem_limit_bytes=56 << 20),
+        compiler_params=pltpu.CompilerParams(vmem_limit_bytes=16 << 20),
     )(tp, *mine, *came, *u, *z, *x)
 
 

time: 159 us -> 140 us (0.88)
  Pallas kernels: 31.5 us -> 22.1 us
  waiting for transfers between devices: 27 us -> 21.1 us
  matrix products: 4.5 us -> 0 us
  local copies, waits for them, and re-layouts: 12.4 us -> 14 us
    all_to_all x1, waiting for transfers between devices: 27 us -> 18.6 us  [exchange(): lax.all_to_all(x.reshape(experts, 8, m), 'ep', split_axis=0, concat_axis=...]
    pallas_call x5 -> x6, Pallas kernels: 26.9 us -> 19.7 us  [call(): pl.pallas_call(kernel, name=name, out_shape=[jax.ShapeDtypeStruct(shape,...]
    dot_general x6 -> x0, matrix products: 4.5 us -> none  [tn(): lax.dot_general(a, b, (((0,), (0,)), ((), ())), preferred_element_type=F32)]
    ppermute x4, waiting for transfers between devices: 0.01 us -> 2.57 us  [partner(): return lax.ppermute(x, 'tp', swap)]
    unnamed x36 -> x52, local copies, waits for them, and re-layouts: 11.8 us -> 14 us
    pallas_call x1, Pallas kernels: 4.64 us -> 2.37 us  [call_pack(): pl.pallas_call(pack_kernel, name='pack', out_shape=jax.ShapeDtypeStruct((...]
  transfers between devices with their start and end apart: 5 -> 5, of which waited for: 1 -> 4; matrix products, arithmetic and copies ran while one was open for 5% -> 0% of each run, Pallas kernels for 10% -> 11%
where the time goes in v1:
time: 140 us; the launch traced here: 139 us
  blocking collectives  74 us (53%)
  Pallas kernels  22.1 us (16%)
  waiting for transfers between devices  21.1 us (15%)
  local copies, waits for them, and re-layouts  14 us (10%)
  starting transfers between devices  7.41 us (5%)
    all_to_all x1, blocking collectives, exchange(): lax.all_to_all(x.reshape(experts, 8, m), 'ep', split_axis=0, concat_axis=...  74 us
    pallas_call x6, Pallas kernels, call(): pl.pallas_call(kernel, name=name, out_shape=[jax.ShapeDtypeStruct(shape,...  19.7 us
    all_to_all x1, waiting for transfers between devices, exchange(): lax.all_to_all(x.reshape(experts, 8, m), 'ep', split_axis=0, concat_axis=...  18.6 us
    unnamed x52, local copies, waits for them, and re-layouts  14 us
    all_to_all x1, starting transfers between devices, exchange(): lax.all_to_all(x.reshape(experts, 8, m), 'ep', split_axis=0, concat_axis=...  6.77 us
  transfers between devices with their start and end apart: 5, of which 4 were waited for; matrix products, arithmetic and copies ran while one was open for 0% of the time, Pallas kernels for 11%

profile of v1, /device:TPU:32, one launch (start us, length us, event | category | flops | bytes accessed | tf_op | source)
XLA Modules:
  0.0 139.4 jit_solution(14100239675060574766)
XLA Ops:
  0.6 0.0 copy-start.3
  0.7 1.0 copy-done.3
  1.7 1.0 copy-done.4
  2.7 1.0 copy-done.5
  3.8 0.7 copy-done.7
  4.5 0.7 copy-done.9
  5.2 2.6 %pre.1 = (bf16[1024,1152]{1,0:T(8,128)(2,1)S(1)}, f32[128,128]{1,0:T(8,128)S(1)}) custom-call(s32[1]{0:T(128)} %bitcast.tp_ref, s32[2,128]{1,0:T(2,128)S(1)} %bitcast.27, bf16[4,2048]{1,0:T(4,128)(2,1)S(1)} %bitcast.25, bf16[128,2048]{1,0:T(8,128)(2,1)S(1)} %copy-done.3, bf16[128,2048]{1,0:T(8,128)(2,1)S(1)} %copy-done.4, bf16[2048,128]{1,0:T(8,128)(2,1)S(1)} %copy-done.5), custom_call_target="tpu_custom_call" | custom-call | flops 1073741824 | bytes 4194304 | tf_op jit(solution)/shard_map/pre/pallas_call | solution.py:35
  7.8 0.0 copy-start
  7.8 0.0 copy-start.1
  7.8 0.0 copy-start.2
  7.8 74.0 %all_to_all.10 = bf16[128,8,1152]{2,1,0:T(8,128)(2,1)S(1)} all-to-all(bf16[128,8,1152]{2,1,0:T(8,128)(2,1)S(1)} %bitcast.18), channel_id=1, replica_groups=mesh['ep'=128,'tp'=2] {'ep'}, dimensions={0} | all-to-all | bytes 4718592 | tf_op jit(solution)/shard_map/all_to_all | solution.py:331
  81.8 0.0 collective-permute-start
  81.8 0.0 copy-done
  81.8 0.0 copy-done.1
  81.8 0.0 copy-done.2
  81.8 2.8 %expert.2 = (bf16[256,2048]{1,0:T(8,128)(2,1)S(1)}, bf16[256,2048]{1,0:T(8,128)(2,1)S(1)}, bf16[256,128]{1,0:T(8,128)(2,1)S(1)}, bf16[256,256]{1,0:T(8,128)(2,1)...) custom-call(s32[1]{0:T(128)} %bitcast.tp_ref, ...), custom_call_target="tpu_custom_call" | custom-call | flops 3221225472 | bytes 4194304 | tf_op jit(solution)/shard_map/expert/pallas_call | solution.py:35
  84.6 0.0 copy-start.10
  84.6 1.0 copy-done.10
  85.6 0.5 collective-permute-start.2
  86.1 0.2 collective-permute-done.got_ref
  86.3 2.8 %expert.3 = (bf16[256,2048]{1,0:T(8,128)(2,1)S(1)}, bf16[256,2048]{1,0:T(8,128)(2,1)S(1)}, bf16[256,128]{1,0:T(8,128)(2,1)S(1)}, bf16[256,256]{1,0:T(8,128)(2,1)...) custom-call(s32[1]{0:T(128)} %bitcast.tp_ref, ...), custom_call_target="tpu_custom_call" | custom-call | flops 3221225472 | bytes 4194304 | tf_op jit(solution)/shard_map/expert/pallas_call | solution.py:35
  89.1 0.0 copy-done.14
  89.1 0.0 copy-done.16
  89.2 0.0 copy-done.18
  89.2 0.0 copy-start.20
  89.2 0.6 copy-done.20
  89.8 0.1 collective-permute-start.1
  90.0 0.0 collective-permute-done.2.refs_3_
  90.0 1.9 %collective-permute-done.1.refs_2_ = bf16[256,1152]{1,0:T(8,128)(2,1)S(1)} collective-permute-done((bf16[256,1152]{1,0:T(8,128)(2,1)S(1)}, bf16[256,1152]{1,0:T(8,128)(2,1)S(1)}, u32[]{:S(2)}, u32[]{:S(2)}) %collective-permute-start.1) | collective-permute-done | bytes 589856 | tf_op jit(solution)/shard_map/ppermute | solution.py:335
  91.8 2.4 %pack.1 = bf16[1024,640]{1,0:T(8,128)(2,1)} custom-call(s32[1]{0:T(128)} %bitcast.tp_ref, bf16[256,1024]{1,0:T(8,128)(2,1)S(1)} %get-tuple-element.45.refs_0_, bf16[256,1024]{1,0:T(8,128)(2,1)S(1)} %get-tuple-element.46.refs_1_, bf16[256,1152]{1,0:T(8,128)(2,1)S(1)} %collective-permute-done.1.refs_2_, bf16[256,1152]{1,0:T(8,128)(2,1)S(1)} %collective-permute-done.2.refs_3_, ...), custom_call_target="tpu_custom_call" | custom-call | flops 536870912 | bytes 4194304 | tf_op jit(solution)/shard_map/pack/pallas_call | solution.py:395
  94.2 0.0 copy-done.12
  94.2 6.8 %all-to-all-start.1 = ((bf16[128,8,640]{2,1,0:T(8,128)(2,1)}), bf16[128,8,640]{2,1,0:T(8,128)(2,1)S(1)}, u32[]{:S(2)}, u32[]{:S(2)}) async-start(bf16[128,8,640]{2,1,0:T(8,128)(2,1)} %bitcast.8), calls=%async_computation.1 | async-start | bytes 2621440 | tf_op jit(solution)/shard_map/all_to_all | solution.py:331
  101.0 0.0 copy-start.11
  101.0 1.2 copy-done.11
  102.2 1.2 copy-done.13
  103.4 0.9 copy-done.15
  104.4 0.9 copy-done.17
  105.3 0.9 copy-done.19
  106.2 0.9 copy-done.21
  107.1 0.9 copy-done.23
  108.0 0.9 copy-done.25
  108.9 9.5 %grads.1 = (bf16[2048,256]{1,0:T(8,128)(2,1)}, bf16[2048,256]{1,0:T(8,128)(2,1)}, bf16[256,2048]{1,0:T(8,128)(2,1)}, f32[2,2048]{1,0:T(2,128)S(1)}, f32[1,256]{1,0:T(1,128)}) custom-call(bf16[256,2048]{1,0:T(8,128)(2,1)S(1)} %get-tuple-element.53.refs_8_.refs_0_, bf16[256,2048]{1,0:T(8,128)(2,1)S(1)} %get-tuple-element.54.refs_9_.refs_1_, ...), custom_call_target="tpu_custom_call" | custom-call | flops 3221225472 | bytes 4194304 | tf_op jit(solution)/shard_map/grads/pallas_call | solution.py:35
  118.4 0.0 collective-permute-start.3
  118.4 0.0 copy-done.8
  118.4 0.7 home.1
  119.1 0.5 collective-permute-done.3.sqo_ref
  119.6 18.6 %all-to-all-done.1 = bf16[128,8,640]{2,1,0:T(8,128)(2,1)S(1)} async-done(((bf16[128,8,640]{2,1,0:T(8,128)(2,1)}), bf16[128,8,640]{2,1,0:T(8,128)(2,1)S(1)}, u32[]{:S(2)}, u32[]{:S(2)}) %all-to-all-start.1) | async-done | bytes 1310752 | tf_op jit(solution)/shard_map/all_to_all | solution.py:331
  138.2 1.3 final.1
  (22 shorter events, 0.0 us)
Async XLA Ops:
  0.6 1.0 copy-start.3
  1.7 1.0 copy-start.4
  2.7 1.0 copy-start.5
  3.8 0.7 copy-start.7
  4.5 0.7 copy-start.9
  7.8 74.0 %copy-start = (bf16[1,2048,256]{2,1,0:T(8,128)(2,1)S(1)}, bf16[1,2048,256]{2,1,0:T(8,128)(2,1)}, u32[]{:S(2)}) copy-start(bf16[1,2048,256]{2,1,0:T(8,128)(2,1)} %param.13) | copy-start | bytes 3145732
  7.8 74.0 %copy-start.1 = (bf16[1,2048,256]{2,1,0:T(8,128)(2,1)S(1)}, bf16[1,2048,256]{2,1,0:T(8,128)(2,1)}, u32[]{:S(2)}) copy-start(bf16[1,2048,256]{2,1,0:T(8,128)(2,1)} %param.14) | copy-start | bytes 3145732
  7.8 74.0 %copy-start.2 = (bf16[1,256,2048]{2,1,0:T(8,128)(2,1)S(1)}, bf16[1,256,2048]{2,1,0:T(8,128)(2,1)}, u32[]{:S(2)}) copy-start(bf16[1,256,2048]{2,1,0:T(8,128)(2,1)} %param.15) | copy-start | bytes 3145732
  81.8 4.5 %collective-permute-start = (bf16[1024,1152]{1,0:T(8,128)(2,1)S(1)}, bf16[1024,1152]{1,0:T(8,128)(2,1)S(1)}, u32[]{:S(2)}, u32[]{:S(2)}) collective-permute-start(bf16[1024,1152]{1,0:T(8,128)(2,1)S(1)} %bitcast.16), channel_id=1, source_target_pairs={{0,1},{1,0},{2,3},{3,2},{4,5},{5,4},{6,7},{7,6},{8,9},{9,8},{10,11... | collective-permute-start | bytes 7077896 | tf_op jit(solution)/shard_map/ppermute | solution.py:335
  84.6 1.0 copy-start.10
  85.6 3.5 %copy-start.14 = (bf16[256,256]{1,0:T(8,128)(2,1)}, bf16[256,256]{1,0:T(8,128)(2,1)S(1)}, u32[]{:S(2)}) copy-start(bf16[256,256]{1,0:T(8,128)(2,1)S(1)} %get-tuple-element.61.refs_4_) | copy-start | bytes 393220
  85.6 3.5 %copy-start.16 = (bf16[256,256]{1,0:T(8,128)(2,1)}, bf16[256,256]{1,0:T(8,128)(2,1)S(1)}, u32[]{:S(2)}) copy-start(bf16[256,256]{1,0:T(8,128)(2,1)S(1)} %get-tuple-element.63.refs_6_) | copy-start | bytes 393220
  85.6 3.6 %copy-start.18 = (bf16[256,256]{1,0:T(8,128)(2,1)}, bf16[256,256]{1,0:T(8,128)(2,1)S(1)}, u32[]{:S(2)}) copy-start(bf16[256,256]{1,0:T(8,128)(2,1)S(1)} %get-tuple-element.65.refs_8_) | copy-start | bytes 393220
  85.6 4.4 %collective-permute-start.2 = (bf16[256,1152]{1,0:T(8,128)(2,1)S(1)}, bf16[256,1152]{1,0:T(8,128)(2,1)S(1)}, u32[]{:S(2)}, u32[]{:S(2)}) collective-permute-start(bf16[256,1152]{1,0:T(8,128)(2,1)S(1)} %get-tuple-element.48), channel_id=1, source_target_pairs={{0,1},{1,0},{2,3},{3,2},{4,5},{5,4},{6,7},{7,6},{8,9},{9,8},{10,11... | collective-permute-start | bytes 1769480 | tf_op jit(solution)/shard_map/ppermute | solution.py:335
  89.2 0.7 copy-start.20
  89.8 4.4 %copy-start.12 = (bf16[256,2048]{1,0:T(8,128)(2,1)}, bf16[256,2048]{1,0:T(8,128)(2,1)S(1)}, u32[]{:S(2)}) copy-start(bf16[256,2048]{1,0:T(8,128)(2,1)S(1)} %get-tuple-element.60.refs_3_) | copy-start | bytes 3145732
  89.8 4.4 %copy-start.22 = (bf16[256,256]{1,0:T(8,128)(2,1)}, bf16[256,256]{1,0:T(8,128)(2,1)S(1)}, u32[]{:S(2)}) copy-start(bf16[256,256]{1,0:T(8,128)(2,1)S(1)} %get-tuple-element.64.refs_7_) | copy-start | bytes 393220
  89.8 4.4 %copy-start.24 = (bf16[256,256]{1,0:T(8,128)(2,1)}, bf16[256,256]{1,0:T(8,128)(2,1)S(1)}, u32[]{:S(2)}) copy-start(bf16[256,256]{1,0:T(8,128)(2,1)S(1)} %get-tuple-element.66.refs_9_) | copy-start | bytes 393220
  89.8 2.0 %collective-permute-start.1 = (bf16[256,1152]{1,0:T(8,128)(2,1)S(1)}, bf16[256,1152]{1,0:T(8,128)(2,1)S(1)}, u32[]{:S(2)}, u32[]{:S(2)}) collective-permute-start(bf16[256,1152]{1,0:T(8,128)(2,1)S(1)} %get-tuple-element.47), channel_id=1, source_target_pairs={{0,1},{1,0},{2,3},{3,2},{4,5},{5,4},{6,7},{7,6},{8,9},{9,8},{10,11... | collective-permute-start | bytes 1769480 | tf_op jit(solution)/shard_map/ppermute | solution.py:335
  94.2 44.0 %all-to-all-start.1 = ((bf16[128,8,640]{2,1,0:T(8,128)(2,1)}), bf16[128,8,640]{2,1,0:T(8,128)(2,1)S(1)}, u32[]{:S(2)}, u32[]{:S(2)}) async-start(bf16[128,8,640]{2,1,0:T(8,128)(2,1)} %bitcast.8), calls=%async_computation.1 | async-start | bytes 2621440 | tf_op jit(solution)/shard_map/all_to_all | solution.py:331
  101.0 1.2 copy-start.11
  102.2 1.2 copy-start.13
  103.4 0.9 copy-start.15
  104.3 0.9 copy-start.17
  105.3 0.9 copy-start.19
  106.2 0.9 copy-start.21
  107.1 0.9 copy-start.23
  108.0 0.9 copy-start.25
  108.9 9.6 %copy-start.6 = (bf16[2048,128]{1,0:T(8,128)(2,1)S(1)}, bf16[2048,128]{1,0:T(8,128)(2,1)}, u32[]{:S(2)}) copy-start(bf16[2048,128]{1,0:T(8,128)(2,1)} %rex_ref.1) | copy-start | bytes 1572868
  108.9 9.6 %copy-start.8 = (bf16[2048,4]{0,1:T(4,128)(2,1)S(1)}, bf16[2048,4]{0,1:T(4,128)(2,1)}, u32[]{:S(2)}) copy-start(bf16[2048,4]{0,1:T(4,128)(2,1)} %param.11) | copy-start | bytes 49156
  118.4 1.2 collective-permute-start.3

commit v2 on v1

v2 whole, which is shorter than its diff:
```python
import functools

import jax
import jax.numpy as jnp
from jax import lax
from jax.experimental import pallas as pl
from jax.experimental.pallas import tpu as pltpu
from jax.sharding import PartitionSpec as P

BF = jnp.bfloat16
F32 = jnp.float32
GROUP_LANE = 32
EXTRA = 128


def mm(a, b):
    return lax.dot_general(a, b, (((1,), (0,)), ((), ())), preferred_element_type=F32)


def nt(a, b):
    return lax.dot_general(a, b, (((1,), (1,)), ((), ())), preferred_element_type=F32)


def tn(a, b):
    return lax.dot_general(a, b, (((0,), (0,)), ((), ())), preferred_element_type=F32)


def iota(shape, dim):
    return lax.broadcasted_iota(jnp.int32, shape, dim)


VM = pl.BlockSpec(memory_space=pltpu.VMEM)
HB = pl.BlockSpec(memory_space=pltpu.HBM)


def far(x):
    return pltpu.with_memory_space_constraint(x, pltpu.HBM)


def call(kernel, name, flops, limit, outs, scalars, arrays, scratch=(), spaces=None, out_spaces=None):
    smem = pl.BlockSpec(memory_space=pltpu.SMEM)
    vmem = pl.BlockSpec(memory_space=pltpu.VMEM)
    return pl.pallas_call(
        kernel,
        name=name,
        out_shape=[
            pltpu.HBM(shape, dtype) if out_spaces and out_spaces[k] is HB else jax.ShapeDtypeStruct(shape, dtype)
            for k, (shape, dtype) in enumerate(outs)
        ],
        in_specs=[smem] * len(scalars) + (spaces or [vmem] * len(arrays)),
        out_specs=out_spaces or [vmem] * len(outs),
        scratch_shapes=list(scratch),
        cost_estimate=pl.CostEstimate(flops=flops, bytes_accessed=4 << 20, transcendentals=0),
        compiler_params=pltpu.CompilerParams(vmem_limit_bytes=limit << 20),
    )(*scalars, *arrays)


def ones_where(mask):
    return jnp.where(mask, 1.0, 0.0).astype(BF)


def pre_kernel(
    ep_ref, tp_ref, rt_hbm, rgt_hbm, tok_hbm, cot_hbm, rex_hbm,
    send_ref, aux_ref, rt_ref, rgt_ref, tok_ref, cot_ref, rex_ref, one_ref, sems,
):
    tp = tp_ref[0]
    tok, dm = tok_ref.shape
    experts = rex_ref.shape[1]
    groups = rgt_ref.shape[0]
    gw = experts // groups
    width = dm // 4
    loads = [
        pltpu.make_async_copy(src, dst, sems.at[k])
        for k, (src, dst) in enumerate(
            ((rt_hbm, rt_ref), (tok_hbm, tok_ref), (rgt_hbm, rgt_ref), (rex_hbm, rex_ref), (cot_hbm, cot_ref))
        )
    ]
    for load in loads:
        load.start()
    loads[0].wait()
    r0, r1 = rt_ref[0:1, :], rt_ref[1:2, :]
    before = ones_where(iota((tok, tok), 0) < iota((tok, tok), 1))
    blk = min(256, experts * 8)
    blocks = experts * 8 // blk
    row = iota((blk, tok), 0)
    sub = row & 7
    want = (2 * tp + (sub & 1)).astype(F32)
    part = sub >> 1
    for b in range(blocks):
        rows = slice(b * blk, (b + 1) * blk)
        expert = b * (blk // 8) + (row >> 3)
        hit0 = r0 == expert
        hit1 = r1 == expert
        match = mm(ones_where(hit0 | hit1), before) == want
        one_ref[0, rows, :] = ones_where(hit0 & match)
        one_ref[1, rows, :] = ones_where(hit1 & match)

    def spread(sel):
        return jnp.concatenate([jnp.where(part == c, sel, 0.0).astype(BF) for c in range(4)], axis=1)

    def stacked(ref):
        return jnp.concatenate([ref[:, c * width : (c + 1) * width] for c in range(4)], axis=0)

    loads[1].wait()
    stack = stacked(tok_ref)
    for b in range(blocks):
        rows = slice(b * blk, (b + 1) * blk)
        one = one_ref[0, rows, :].astype(F32) + one_ref[1, rows, :].astype(F32)
        send_ref[rows, 0:width] = mm(spread(one), stack).astype(BF)
    loads[2].wait()
    loads[3].wait()
    group_exp = jnp.exp(nt(rgt_ref[...], tok_ref[...]))
    group_prob = group_exp / jnp.sum(group_exp, axis=0, keepdims=True)
    logits = jnp.transpose(mm(tok_ref[...], rex_ref[...]))
    ei = iota((experts, tok), 0)
    l0 = jnp.sum(jnp.where(ei == r0, logits, 0.0), axis=0, keepdims=True)
    l1 = jnp.sum(jnp.where(ei == r1, logits, 0.0), axis=0, keepdims=True)
    x0, x1 = jnp.exp(l0), jnp.exp(l1)
    p0, p1 = x0 / (x0 + x1), x1 / (x0 + x1)
    chosen = r0 // gw
    gi = iota((groups, tok), 0)
    picked = jnp.sum(jnp.where(gi == chosen, group_prob, 0.0), axis=0, keepdims=True)
    w0 = (picked * p0).astype(BF).astype(F32)
    w1 = (picked * p1).astype(BF).astype(F32)
    li = iota((EXTRA, tok), 0)
    diff = jnp.where(li == r0 - chosen * gw, 1.0, 0.0) - jnp.where(li == r1 - chosen * gw, 1.0, 0.0)
    group_side = jnp.where(li == GROUP_LANE + chosen, 1.0, 0.0)
    for j in range(groups):
        group_side = group_side - jnp.where(li == GROUP_LANE + j, group_prob[j : j + 1, :], 0.0)
    side_t = jnp.concatenate([(p1 * diff + group_side).astype(BF), (group_side - p0 * diff).astype(BF)], axis=1)
    arow = iota((EXTRA, tok), 0)
    aux = jnp.where(arow == 0, p0, jnp.where(arow == 1, p1, 0.0))
    for j in range(groups):
        aux = jnp.where(arow == 2 + j, group_prob[j : j + 1, :], aux)
    aux = jnp.where(arow == 6, r0.astype(F32), jnp.where(arow == 7, r1.astype(F32), aux))
    aux_ref[...] = jnp.transpose(aux)
    loads[4].wait()
    stack = stacked(cot_ref)
    for b in range(blocks):
        rows = slice(b * blk, (b + 1) * blk)
        one0, one1 = one_ref[0, rows, :].astype(F32), one_ref[1, rows, :].astype(F32)
        send_ref[rows, width : 2 * width] = mm(spread(one0 * w0 + one1 * w1), stack).astype(BF)
        head = part == 0
        both = jnp.concatenate(
            [jnp.where(head, one0, 0.0).astype(BF), jnp.where(head, one1, 0.0).astype(BF)], axis=1
        )
        send_ref[rows, 2 * width :] = nt(both, side_t).astype(BF)


def expert_kernel(
    tp_ref, got_ref, gate_ref, up_ref, down_ref,
    u_ref, z_ref, mine_ref, theirs_ref, x_out, sc_out, gd_out, ud_out, hid_out,
    x_ref, sc_ref, gd_ref, ud_ref, hid_ref, sems,
):
    tp = tp_ref[0]
    dm = gate_ref.shape[0]
    width, half = dm // 4, dm // 2
    blk = min(256, got_ref.shape[0])
    n4 = blk // 4
    shift = n4.bit_length() - 1
    o, i = iota((blk, blk), 0), iota((blk, blk), 1)
    perm = ones_where(i == ((o & (n4 - 1)) >> 1) * 8 + (o >> shift) * 2 + (o & 1))
    for b in range(got_ref.shape[0] // blk):
        block = slice(b * blk, (b + 1) * blk)
        rows = slice(b * n4, (b + 1) * n4)
        y = mm(perm, got_ref[block, 0 : 2 * width]).astype(BF)
        for c in range(4):
            cols = slice(c * width, (c + 1) * width)
            x_ref[rows, cols] = y[c * n4 : (c + 1) * n4, 0:width]
            sc_ref[rows, cols] = y[c * n4 : (c + 1) * n4, width:]
        z_ref[rows, :] = mm(perm[0:n4], got_ref[block, 2 * width :]).astype(BF)
    saves = [
        pltpu.make_async_copy(src, dst, sems.at[k])
        for k, (src, dst) in enumerate(
            ((x_ref, x_out), (sc_ref, sc_out), (gd_ref, gd_out), (ud_ref, ud_out), (hid_ref, hid_out))
        )
    ]
    saves[0].start()
    saves[1].start()
    gp = mm(x_ref[...], gate_ref[...])
    upre = mm(x_ref[...], up_ref[...])
    pulled = nt(sc_ref[...], down_ref[...])
    sig = 1.0 / (1.0 + jnp.exp(-gp))
    act = gp * sig
    hid = (act * upre).astype(BF)
    hid_ref[...] = hid
    u = jnp.sum(pulled * hid.astype(F32), axis=1, keepdims=True)
    gd = (pulled * (upre * sig * (1.0 + gp * (1.0 - sig)))).astype(BF)
    ud = (pulled * act).astype(BF)
    gd_ref[...] = gd
    ud_ref[...] = ud
    for save in saves[2:]:
        save.start()
    n = x_ref.shape[0]
    u_ref[...] = jnp.broadcast_to(u, (n, EXTRA))
    high = u.astype(BF).astype(F32)
    lane = iota((n, EXTRA), 1)
    theirs_ref[:, half:] = jnp.where(lane == 0, high, jnp.where(lane == 1, u - high, 0.0)).astype(BF)
    far = pl.ds(pl.multiple_of((1 - tp) * half, half), half)
    theirs_ref[:, 0:half] = (nt(gd, gate_ref[far, :]) + nt(ud, up_ref[far, :])).astype(BF)
    near = pl.ds(pl.multiple_of(tp * half, half), half)
    mine_ref[...] = (nt(gd, gate_ref[near, :]) + nt(ud, up_ref[near, :])).astype(BF)
    for save in saves:
        save.wait()


def pack_kernel(ep_ref, tp_ref, *refs):
    tp = tp_ref[0]
    mine, came, us, zs = refs[0:2], refs[2:4], refs[4:6], refs[6:8]
    rgt_hbm, rex_hbm, ret_out, y0_out, y1_out, sum_ref, ret_ref, y_ref, rgt_ref, rex_ref, sems = refs[8:19]
    n, half = mine[0].shape
    width = half // 2
    experts, groups = rex_ref.shape[1], rgt_ref.shape[0]
    gw = experts // groups
    group = ep_ref[0] // gw
    near = pl.ds(pl.multiple_of(tp * half, half), half)
    loads = [
        pltpu.make_async_copy(rex_hbm.at[near, :], rex_ref, sems.at[6]),
        pltpu.make_async_copy(rgt_hbm.at[:, near], rgt_ref, sems.at[7]),
    ]
    for load in loads:
        load.start()
    li, ei = iota((EXTRA, experts), 0), iota((EXTRA, experts), 1)
    to_expert = ones_where((ei == group * gw + li) & (li < gw))
    to_group = ones_where(iota((EXTRA, groups), 0) == GROUP_LANE + iota((EXTRA, groups), 1))
    saves = []
    for p, y_out in ((0, y0_out), (1, y1_out)):
        u = us[p][...] + came[p][:, half : half + 1].astype(F32) + came[p][:, half + 1 : half + 2].astype(F32)
        y = (u * zs[p][...].astype(F32)).astype(BF)
        y_ref[p] = y
        saves.append(pltpu.make_async_copy(y_ref.at[p], y_out, sems.at[p]))
        saves[-1].start()
    for load in loads:
        load.wait()
    for p in range(2):
        y = y_ref[p]
        route = nt(mm(y, to_expert).astype(BF), rex_ref[...])
        route = route + mm(mm(y, to_group).astype(BF), rgt_ref[...])
        sum_ref[p] = (mine[p][...].astype(F32) + came[p][:, 0:half].astype(F32) + route).astype(BF)
    blk = min(256, n * 4)
    bs = blk // 8
    o, i = iota((blk, blk), 0), iota((blk, blk), 1)
    perm = ones_where(i == ((o >> 2) & 1) * (4 * bs) + ((o >> 1) & 1) * (2 * bs) + (o >> 3) * 2 + (o & 1))
    for b in range(n // (2 * bs)):
        rows = slice(b * 2 * bs, (b + 1) * 2 * bs)
        stack = jnp.concatenate(
            [sum_ref[0, rows, 0:width], sum_ref[1, rows, 0:width], sum_ref[0, rows, width:], sum_ref[1, rows, width:]],
            axis=0,
        )
        out = pl.ds(b * blk, blk)
        ret_ref[out, :] = mm(perm, stack).astype(BF)
        saves.append(pltpu.make_async_copy(ret_ref.at[out, :], ret_out.at[out, :], sems.at[2 + b]))
        saves[-1].start()
    for save in saves:
        save.wait()


def rc_x_kernel(ep_ref, tp_ref, x0_ref, x1_ref, y0_ref, y1_ref, own_ref, s1_ref, s2_ref, s3_ref, all_ref):
    x, tp = ep_ref[0] & 3, tp_ref[0]
    planes = x0_ref.shape[1] // 256
    for b in range(planes):
        cols = slice(b * 256, (b + 1) * 256)
        rc = tn(x0_ref[:, cols], y0_ref[...]) + tn(x1_ref[:, cols], y1_ref[...])
        rc = rc.reshape(16, 16, EXTRA)
        all_ref[b * 16 : (b + 1) * 16] = jnp.where(tp == 0, rc[:, 0:8, :], rc[:, 8:16, :])
    for d, out_ref in enumerate((own_ref, s1_ref, s2_ref, s3_ref)):
        to = (x + d) & 3
        for q in range(planes * 4):
            out_ref[q * 8 : (q + 1) * 8, :] = all_ref[q * 4 + to].astype(out_ref.dtype)


def rc_y_kernel(ep_ref, tp_ref, own_ref, a_ref, b_ref, c_ref, o0_ref, o1_ref, o2_ref, o3_ref, all_ref):
    y = (ep_ref[0] >> 2) & 3
    total = own_ref[...]
    for ref in (a_ref, b_ref, c_ref):
        total = total + ref[...].astype(F32)
    all_ref[...] = total.reshape(all_ref.shape)
    for d, out_ref in enumerate((o0_ref, o1_ref, o2_ref, o3_ref)):
        to = (y + d) & 3
        for q in range(all_ref.shape[0] // 4):
            out_ref[q * 8 : (q + 1) * 8, :] = all_ref[q * 4 + to]


def rc_z_kernel(groups, gw, ep_ref, tp_ref, own_ref, a_ref, b_ref, c_ref, *refs):
    outs, all_ref = refs[:-1], refs[-1]
    planes = all_ref.shape[0]
    group, z = ep_ref[0] // gw, ep_ref[0] >> 4
    total = own_ref[...] + a_ref[...] + b_ref[...] + c_ref[...]
    rows = total.shape[0]
    near = total[:, 0:gw]
    placed = None
    for g in range(groups):
        parts = [near if h == g else jnp.zeros((rows, gw), F32) for h in range(groups)]
        spread = jnp.where(group == g, jnp.concatenate(parts, axis=1), 0.0)
        placed = spread if g == 0 else placed + spread
    all_ref[:, :, 0 : groups * gw] = placed.reshape(planes, 8, groups * gw)
    all_ref[:, :, groups * gw :] = total.reshape(planes, 8, EXTRA)
    for d, out_ref in enumerate(outs):
        out_ref[...] = all_ref[(z + d) & (planes - 1)]


def as_row(col):
    return jnp.transpose(jnp.broadcast_to(col, (col.shape[0], 128)))[0:1, :]


def in_grad_kernel(x0_ref, x1_ref, d0_ref, d1_ref, out_ref, sq_ref):
    blk = 128

    def step(b, carry):
        cols = pl.ds(pl.multiple_of(b * blk, blk), blk)
        full = tn(x0_ref[:, cols], d0_ref[...]) + tn(x1_ref[:, cols], d1_ref[...])
        out_ref[cols, :] = full.astype(BF)
        sq_ref[:, cols] = as_row(jnp.sum(full * full, axis=1, keepdims=True))
        return carry

    lax.fori_loop(0, out_ref.shape[0] // blk, step, 0)


def down_grad_kernel(h0_ref, h1_ref, s0_ref, s1_ref, out_ref, sq_ref, acc_ref):
    dm = out_ref.shape[1]
    wide = 512 if dm % 512 == 0 else 128
    acc_ref[...] = jnp.zeros_like(acc_ref)

    def step(b, carry):
        cols = pl.ds(pl.multiple_of(b * wide, wide), wide)
        full = tn(h0_ref[...], s0_ref[:, cols]) + tn(h1_ref[...], s1_ref[:, cols])
        out_ref[:, cols] = full.astype(BF)
        acc_ref[...] += jnp.broadcast_to(jnp.sum(full * full, axis=1, keepdims=True), acc_ref.shape)
        return carry

    lax.fori_loop(0, dm // wide, step, 0)
    sq_ref[...] = jnp.transpose(acc_ref[...])[0:1, :]


def home_kernel(tp_ref, aux_ref, sel_ref):
    tp = tp_ref[0]
    tok = aux_ref.shape[0]
    n = sel_ref.shape[2]
    r0, r1 = aux_ref[:, 6:7].astype(jnp.int32), aux_ref[:, 7:8].astype(jnp.int32)
    col = iota((tok, n), 1)
    hit = jnp.where(r0 == (col >> 3), 1.0, 0.0) + jnp.where(r1 == (col >> 3), 1.0, 0.0)
    earlier = ones_where(iota((tok, tok), 1) < iota((tok, tok), 0))
    rank = mm(earlier, hit.astype(BF))
    one = jnp.where(rank == ((2 * tp + (col & 3)) & 3).astype(F32), hit, 0.0)
    lower = (col & 4) == 0
    sel_ref[0] = jnp.where(lower, one, 0.0).astype(BF)
    sel_ref[1] = jnp.where(lower, 0.0, one).astype(BF)


def final_kernel(blocks, *refs):
    back_ref, sel_ref, g0_ref, g1_ref, u0_ref, u1_ref = refs[0:6]
    rcs = refs[6 : 6 + blocks]
    tg_ref, rex_ref, rg_ref, rows_ref, gate_sq_ref, up_sq_ref = refs[6 + blocks :]
    width = back_ref.shape[1]
    experts, groups = rex_ref.shape[1], rg_ref.shape[0]
    gate_sq_ref[...] = g0_ref[...] + g1_ref[...]
    up_sq_ref[...] = u0_ref[...] + u1_ref[...]
    for c in range(2):
        tg_ref[:, c * width : (c + 1) * width] = mm(sel_ref[c], back_ref[...]).astype(BF)
    total = rcs[0][...]
    for ref in rcs[1:]:
        total = total + ref[...]
    rex = total[:, 0:experts]
    rg = total[:, experts:]
    lane = iota(rg.shape, 1)
    rex_ref[...] = rex
    grp = jnp.where((lane >= GROUP_LANE) & (lane < GROUP_LANE + groups), rg, 0.0)
    square = jnp.sum(rex * rex, axis=1, keepdims=True) + jnp.sum(grp * grp, axis=1, keepdims=True)
    rest = jnp.transpose(jnp.where(lane == GROUP_LANE + groups, square, grp))
    rg_ref[...] = rest[GROUP_LANE : GROUP_LANE + groups, :]
    rows_ref[...] = rest[GROUP_LANE + groups : GROUP_LANE + groups + 1, :]


def body(tokens, cotangent, routes, router_group, router_expert, gate_proj, up_proj, down_proj):
    tok, dm = tokens.shape
    experts = router_expert.shape[1]
    groups = router_group.shape[1]
    width, half = dm // 4, dm // 2
    ff = gate_proj.shape[2]
    n = experts * 2
    tp = lax.axis_index("tp").reshape(1)
    swap = [(0, 1), (1, 0)]
    rgt = router_group.T
    ep = lax.axis_index("ep")
    planes = experts // 16
    idx = [ep.reshape(1), tp]
    gate, up, down = gate_proj[0], up_proj[0], down_proj[0]

    def exchange(x):
        m = x.shape[1]
        y = lax.all_to_all(x.reshape(experts, 8, m), "ep", split_axis=0, concat_axis=0, tiled=True)
        return y.reshape(experts * 8, m)

    def partner(x):
        return lax.ppermute(x, "tp", swap)

    def shift(v, stride, d):
        size = planes if stride == 16 else 4
        pairs = []
        for e in range(experts):
            at = e // stride % size
            pairs.append((e, e + ((at + d) % size - at) * stride))
        return lax.ppermute(v, "ep", pairs)

    send, aux = call(
        pre_kernel, "pre", 1 << 30, 20,
        [((experts * 8, 2 * width + EXTRA), BF), ((tok, EXTRA), F32)],
        idx, [far(routes.T), far(rgt), far(tokens), far(cotangent), far(router_expert)],
        scratch=[
            pltpu.VMEM((2, tok), jnp.int32), pltpu.VMEM((groups, dm), BF),
            pltpu.VMEM((tok, dm), BF), pltpu.VMEM((tok, dm), BF), pltpu.VMEM((dm, experts), BF),
            pltpu.VMEM((2, experts * 8, tok), BF), pltpu.SemaphoreType.DMA((5,)),
        ],
        spaces=[HB] * 5,
    )
    got = exchange(send)
    other = partner(got)
    u, z, mine, theirs, x, sc, gd, ud, hid = [list(v) for v in zip(*[
        call(
            expert_kernel, "expert", 3 << 30, 18,
            [((n, EXTRA), F32), ((n, EXTRA), BF), ((n, half), BF), ((n, half + EXTRA), BF),
             ((n, dm), BF), ((n, dm), BF), ((n, ff), BF), ((n, ff), BF), ((n, ff), BF)],
            [tp], [g, gate, up, down],
            scratch=[pltpu.VMEM((n, w), BF) for w in (dm, dm, ff, ff, ff)] + [pltpu.SemaphoreType.DMA((5,))],
            out_spaces=[VM] * 4 + [HB] * 5,
        )
        for g in (got, other)
    ])]
    came = [partner(theirs[1]), partner(theirs[0])]
    ret, y0, y1 = call(
        pack_kernel, "pack", 1 << 29, 16,
        [((experts * 8, width), BF), ((n, EXTRA), BF), ((n, EXTRA), BF)],
        idx, [*mine, *came, *u, *z, far(rgt), far(router_expert)],
        spaces=[VM] * 8 + [HB] * 2,
        scratch=[pltpu.VMEM((2, n, half), BF), pltpu.VMEM((experts * 8, width), BF), pltpu.VMEM((2, n, EXTRA), BF),
                 pltpu.VMEM((groups, half), BF), pltpu.VMEM((half, experts), BF), pltpu.SemaphoreType.DMA((8,))],
        out_spaces=[HB] * 3,
    )
    back = exchange(ret)
    r = planes * 32
    own, *sends = call(
        rc_x_kernel, "rc_x", 1 << 29, 12,
        [((r, EXTRA), F32)] + [((r, EXTRA), BF)] * 3,
        idx, [*x, y0, y1], scratch=[pltpu.VMEM((experts, 8, EXTRA), F32)],
    )
    came_x = [shift(v, 1, d + 1) for d, v in enumerate(sends)]
    own, *sends = call(
        rc_y_kernel, "rc_y", 1 << 20, 8, [((r // 4, EXTRA), F32)] * 4,
        idx, [own, *came_x], scratch=[pltpu.VMEM((planes * 4, 8, EXTRA), F32)],
    )
    came_y = [shift(v, 4, d + 1) for d, v in enumerate(sends)]
    wide = experts + EXTRA
    own, *sends = call(
        functools.partial(rc_z_kernel, groups, experts // groups), "rc_z", 1 << 20, 8, [((8, wide), F32)] * planes,
        idx, [own, *came_y], scratch=[pltpu.VMEM((planes, 8, wide), F32)],
    )
    rcs = [own] + [shift(v, 16, d + 1) for d, v in enumerate(sends)]
    in_grads = [
        call(
            in_grad_kernel, name, 1 << 30, 12, [((dm, ff), BF), ((1, dm), F32)], [], [*x, *delta],
        )
        for name, delta in (("gate_grad", gd), ("up_grad", ud))
    ]
    (gate_grad, gate_sq), (up_grad, up_sq) = in_grads
    down_grad, down_sq = call(
        down_grad_kernel, "down_grad", 1 << 30, 12, [((ff, dm), BF), ((1, ff), F32)],
        [], [*hid, *sc], scratch=[pltpu.VMEM((ff, 128), F32)],
    )
    (sel,) = call(home_kernel, "home", 1 << 26, 8, [((2, tok, experts * 8), BF)], [tp], [aux])
    token_grad, rex_grad, rg_grad, rows, gate_sq, up_sq = call(
        functools.partial(final_kernel, len(rcs)), "final", 1 << 29, 10,
        [((tok, half), BF), ((8, experts), F32), ((groups, 8), F32), ((1, 8), F32),
         ((1, dm), F32), ((1, dm), F32)],
        [], [back, sel, gate_sq, partner(gate_sq), up_sq, partner(up_sq), *rcs],
    )
    return (
        token_grad,
        gate_grad[None],
        up_grad[None],
        down_grad[None],
        gate_sq,
        up_sq,
        down_sq,
        rex_grad,
        rg_grad.T,
        rows[0],
    )


def solution(mesh):
    return jax.shard_map(
        body,
        mesh=mesh,
        in_specs=(
            P("ep", None),
            P("ep", None),
            P("ep", None),
            P(),
            P(),
            P("ep", None, "tp"),
            P("ep", None, "tp"),
            P("ep", "tp", None),
        ),
        out_specs=(
            P("ep", "tp"),
            P("ep", None, "tp"),
            P("ep", None, "tp"),
            P("ep", "tp", None),
            P("ep", None),
            P("ep", None),
            P("ep", "tp"),
            P(("ep", "tp"), None),
            P(("ep", "tp"), None),
            P(("ep", "tp")),
        ),
        check_vma=False,
    )
```

time: 140 us -> 147 us (1.050); the launches traced: 139 us -> 145 us
  starting transfers between devices: 7.41 us -> 34.8 us
  waiting for transfers between devices: 21.1 us -> 2.98 us
  local copies, waits for them, and re-layouts: 14 us -> 1.73 us
  Pallas kernels: 22.1 us -> 30.6 us
    ppermute x0 -> x13, starting transfers between devices: none -> 27.1 us  [shift(): return lax.ppermute(v, 'ep', pairs)]
    all_to_all x1, waiting for transfers between devices: 18.6 us -> 0.01 us  [exchange(): lax.all_to_all(x.reshape(experts, 8, m), 'ep', split_axis=0, concat_axis=...]
    unnamed x52 -> x30, local copies, waits for them, and re-layouts: 14 us -> 1.73 us
    pallas_call x7 -> x12, Pallas kernels: 22.1 us -> 30.6 us  [call(): pl.pallas_call(kernel, name=name, out_shape=[pltpu.HBM(shape, dtype) if o...]
    ppermute x4 -> x5, waiting for transfers between devices: 2.57 us -> 2.95 us  [partner(): return lax.ppermute(x, 'tp', swap)]
  transfers between devices with their start and end apart: 5 -> 19, of which waited for: 4 -> 2; matrix products, arithmetic and copies ran while one was open for 0% -> 0% of each run, Pallas kernels for 11% -> 16%
where the time goes in v2:
time: 147 us; the launch traced here: 145 us
  blocking collectives  74 us (50%)
  starting transfers between devices  34.8 us (24%)
  Pallas kernels  30.6 us (21%)
  waiting for transfers between devices  2.98 us (2%)
  local copies, waits for them, and re-layouts  1.73 us (1%)
    all_to_all x1, blocking collectives, exchange(): lax.all_to_all(x.reshape(experts, 8, m), 'ep', split_axis=0, concat_axis=...  74 us
    pallas_call x12, Pallas kernels, call(): pl.pallas_call(kernel, name=name, out_shape=[pltpu.HBM(shape, dtype) if o...  30.6 us
    ppermute x13, starting transfers between devices, shift(): return lax.ppermute(v, 'ep', pairs)  27.1 us
    all_to_all x1, starting transfers between devices, exchange(): lax.all_to_all(x.reshape(experts, 8, m), 'ep', split_axis=0, concat_axis=...  6.91 us
    ppermute x5, waiting for transfers between devices, partner(): return lax.ppermute(x, 'tp', swap)  2.95 us
  transfers between devices with their start and end apart: 19, of which 2 were waited for; matrix products, arithmetic and copies ran while one was open for 0% of the time, Pallas kernels for 16%

profile of v2, /device:TPU:32, one launch (start us, length us, event | category | flops | bytes accessed | tf_op | source)
XLA Modules:
  0.0 144.9 jit_solution(9913171512761249155)
XLA Ops:
  0.6 3.3 %pre.1 = (bf16[1024,1152]{1,0:T(8,128)(2,1)S(1)}, f32[128,128]{1,0:T(8,128)S(1)}) custom-call(s32[1]{0:T(128)} %bitcast.ep_ref, s32[1]{0:T(128)} %bitcast.1.tp_ref, s32[2,128]{1,0:T(2,128)} %bitcast.29, bf16[4,2048]{1,0:T(4,128)(2,1)} %bitcast.27, bf16[128,2048]{1,0:T(8,128)(2,1)} %tok_hbm.1, bf16[128,2048]{1,0:T(8,128)(2,1)} %cot_hbm.1, ...), custom_call_target="tpu_custom_call" | custom-call | flops 1073741824 | bytes 4194304 | tf_op jit(solution)/shard_map/pre/pallas_call | solution.py:43
  3.9 0.0 copy-start.4
  4.0 0.0 copy-start.5
  4.0 0.0 copy-start.6
  4.0 74.0 %all_to_all.10 = bf16[128,8,1152]{2,1,0:T(8,128)(2,1)S(1)} all-to-all(bf16[128,8,1152]{2,1,0:T(8,128)(2,1)S(1)} %bitcast.18), channel_id=1, replica_groups=mesh['ep'=128,'tp'=2] {'ep'}, dimensions={0} | all-to-all | bytes 4718592 | tf_op jit(solution)/shard_map/all_to_all | solution.py:391
  77.9 0.0 collective-permute-start
  78.0 2.9 %expert.2 = (f32[256,128]{1,0:T(8,128)S(1)}, bf16[256,128]{1,0:T(8,128)(2,1)S(1)}, bf16[256,1024]{1,0:T(8,128)(2,1)S(1)}, bf16[256,1152]{1,0:T(8,128)(2,1)S(1)},...) custom-call(s32[1]{0:T(128)} %bitcast.1.tp_ref, ...), custom_call_target="tpu_custom_call" | custom-call | flops 3221225472 | bytes 4194304 | tf_op jit(solution)/shard_map/expert/pallas_call | solution.py:43
  80.8 0.6 collective-permute-start.2
  81.4 1.1 collective-permute-done.got_ref
  82.5 2.8 %expert.3 = (f32[256,128]{1,0:T(8,128)S(1)}, bf16[256,128]{1,0:T(8,128)(2,1)S(1)}, bf16[256,1024]{1,0:T(8,128)(2,1)S(1)}, bf16[256,1152]{1,0:T(8,128)(2,1)S(1)},...) custom-call(s32[1]{0:T(128)} %bitcast.1.tp_ref, ...), custom_call_target="tpu_custom_call" | custom-call | flops 3221225472 | bytes 4194304 | tf_op jit(solution)/shard_map/expert/pallas_call | solution.py:43
  85.3 0.2 collective-permute-start.1
  85.6 1.9 %collective-permute-done.1.refs_2_ = bf16[256,1152]{1,0:T(8,128)(2,1)S(1)} collective-permute-done((bf16[256,1152]{1,0:T(8,128)(2,1)S(1)}, bf16[256,1152]{1,0:T(8,128)(2,1)S(1)}, u32[]{:S(2)}, u32[]{:S(2)}) %collective-permute-start.1) | collective-permute-done | bytes 589856 | tf_op jit(solution)/shard_map/ppermute | solution.py:395
  87.4 3.4 %pack.1 = (bf16[1024,512]{1,0:T(8,128)(2,1)}, bf16[256,128]{1,0:T(8,128)(2,1)}, bf16[256,128]{1,0:T(8,128)(2,1)}) custom-call(s32[1]{0:T(128)} %bitcast.ep_ref, s32[1]{0:T(128)} %bitcast.1.tp_ref, bf16[256,1024]{1,0:T(8,128)(2,1)S(1)} %get-tuple-element.62.refs_0_, bf16[256,1024]{1,0:T(8,128)(2,1)S(1)} %get-tuple-element.63.refs_1_, ...), custom_call_target="tpu_custom_call" | custom-call | flops 536870912 | bytes 4194304 | tf_op jit(solution)/shard_map/pack/pallas_call | solution.py:43
  90.8 0.0 copy-start.13
  90.8 6.9 %all-to-all-start.1 = ((bf16[128,8,512]{2,1,0:T(8,128)(2,1)}), bf16[128,8,512]{2,1,0:T(8,128)(2,1)S(1)}, u32[]{:S(2)}, u32[]{:S(2)}) async-start(bf16[128,8,512]{2,1,0:T(8,128)(2,1)} %bitcast.26), calls=%async_computation.1 | async-start | bytes 2097152 | tf_op jit(solution)/shard_map/all_to_all | solution.py:391
  97.8 0.8 copy-done.2
  98.6 0.8 copy-done.3
  99.4 0.8 rc_x.1
  100.3 0.0 copy-start.11
  100.3 1.6 %collective-permute-start.5 = (bf16[256,128]{1,0:T(8,128)(2,1)S(1)}, bf16[256,128]{1,0:T(8,128)(2,1)S(1)}, u32[]{:S(2)}, u32[]{:S(2)}) collective-permute-start(bf16[256,128]{1,0:T(8,128)(2,1)S(1)} %get-tuple-element.83), channel_id=1, source_target_pairs={{0,2},{2,4},{4,6},{6,0},{8,10},{10,12},{12,14},{14,8},{16,18},{18,... | collective-permute-start | bytes 196616 | tf_op jit(solution)/shard_map/ppermute | solution.py:403
  101.9 2.7 %collective-permute-start.6 = (bf16[256,128]{1,0:T(8,128)(2,1)S(1)}, bf16[256,128]{1,0:T(8,128)(2,1)S(1)}, u32[]{:S(2)}, u32[]{:S(2)}) collective-permute-start(bf16[256,128]{1,0:T(8,128)(2,1)S(1)} %get-tuple-element.84), channel_id=1, source_target_pairs={{0,4},{2,6},{4,0},{6,2},{8,12},{10,14},{12,8},{14,10},{16,20},{18,... | collective-permute-start | bytes 196616 | tf_op jit(solution)/shard_map/ppermute | solution.py:403
  104.6 1.4 collective-permute-start.7
  106.0 6.6 %up_grad.1 = (bf16[2048,256]{1,0:T(8,128)(2,1)}, f32[1,2048]{1,0:T(1,128)S(1)}) custom-call(bf16[256,2048]{1,0:T(8,128)(2,1)S(1)} %copy-done, bf16[256,2048]{1,0:T(8,128)(2,1)S(1)} %copy-done.1, bf16[256,256]{1,0:T(8,128)(2,1)S(1)} %copy-done.13, bf16[256,256]{1,0:T(8,128)(2,1)S(1)} %copy-done.14), custom_call_target="tpu_custom_call" | custom-call | flops 1073741824 | bytes 4194304 | tf_op jit(solution)/shard_map/up_grad/pallas_call | solution.py:43
  112.6 0.0 collective-permute-start.4
  112.6 0.0 collective-permute-done.5.a_ref
  112.6 0.0 collective-permute-done.6.b_ref
  112.6 0.1 rc_y.1
  112.7 2.8 %collective-permute-start.10 = (f32[64,128]{1,0:T(8,128)S(1)}, f32[64,128]{1,0:T(8,128)S(1)}, u32[]{:S(2)}, u32[]{:S(2)}) collective-permute-start(f32[64,128]{1,0:T(8,128)S(1)} %get-tuple-element.89), channel_id=1, source_target_pairs={{0,24},{2,26},{4,28},{6,30},{8,0},{10,2},{12,4},{14,6},{16,8},{18,... | collective-permute-start | bytes 98312 | tf_op jit(solution)/shard_map/ppermute | solution.py:403
  115.5 2.3 %collective-permute-start.9 = (f32[64,128]{1,0:T(8,128)S(1)}, f32[64,128]{1,0:T(8,128)S(1)}, u32[]{:S(2)}, u32[]{:S(2)}) collective-permute-start(f32[64,128]{1,0:T(8,128)S(1)} %get-tuple-element.88), channel_id=1, source_target_pairs={{0,16},{2,18},{4,20},{6,22},{8,24},{10,26},{12,28},{14,30},{16,0},... | collective-permute-start | bytes 98312 | tf_op jit(solution)/shard_map/ppermute | solution.py:403
  117.8 6.6 %gate_grad.1 = (bf16[2048,256]{1,0:T(8,128)(2,1)}, f32[1,2048]{1,0:T(1,128)S(1)}) custom-call(bf16[256,2048]{1,0:T(8,128)(2,1)S(1)} %copy-done, bf16[256,2048]{1,0:T(8,128)(2,1)S(1)} %copy-done.1, bf16[256,256]{1,0:T(8,128)(2,1)S(1)} %copy-done.11, bf16[256,256]{1,0:T(8,128)(2,1)S(1)} %copy-done.12), custom_call_target="tpu_custom_call" | custom-call | flops 1073741824 | bytes 4194304 | tf_op jit(solution)/shard_map/gate_grad/pallas_call | solution.py:43
  124.4 0.0 collective-permute-start.3
  124.4 0.0 collective-permute-done.10.c_ref
  124.4 0.0 collective-permute-done.9.b_ref
  124.4 0.1 rc_z.1
  124.5 1.6 %collective-permute-start.11 = (f32[8,256]{1,0:T(8,128)S(1)}, f32[8,256]{1,0:T(8,128)S(1)}, u32[]{:S(2)}, u32[]{:S(2)}) collective-permute-start(f32[8,256]{1,0:T(8,128)S(1)} %get-tuple-element.91), channel_id=1, source_target_pairs={{0,32},{2,34},{4,36},{6,38},{8,40},{10,42},{12,44},{14,46},{16,48}... | collective-permute-start | bytes 24584 | tf_op jit(solution)/shard_map/ppermute | solution.py:403
  126.2 3.8 %collective-permute-start.12 = (f32[8,256]{1,0:T(8,128)S(1)}, f32[8,256]{1,0:T(8,128)S(1)}, u32[]{:S(2)}, u32[]{:S(2)}) collective-permute-start(f32[8,256]{1,0:T(8,128)S(1)} %get-tuple-element.92), channel_id=1, source_target_pairs={{0,64},{2,66},{4,68},{6,70},{8,72},{10,74},{12,76},{14,78},{16,80}... | collective-permute-start | bytes 24584 | tf_op jit(solution)/shard_map/ppermute | solution.py:403
  130.0 0.4 home.1.refs_1_
  130.3 1.0 collective-permute-start.13
  131.3 2.8 %collective-permute-start.14 = (f32[8,256]{1,0:T(8,128)S(1)}, f32[8,256]{1,0:T(8,128)S(1)}, u32[]{:S(2)}, u32[]{:S(2)}) collective-permute-start(f32[8,256]{1,0:T(8,128)S(1)} %get-tuple-element.94), channel_id=1, source_target_pairs={{0,128},{2,130},{4,132},{6,134},{8,136},{10,138},{12,140},{14,142}... | collective-permute-start | bytes 24584 | tf_op jit(solution)/shard_map/ppermute | solution.py:403
  134.1 0.0 collective-permute-done.3.refs_3_
  134.1 1.7 %collective-permute-start.15 = (f32[8,256]{1,0:T(8,128)S(1)}, f32[8,256]{1,0:T(8,128)S(1)}, u32[]{:S(2)}, u32[]{:S(2)}) collective-permute-start(f32[8,256]{1,0:T(8,128)S(1)} %get-tuple-element.95), channel_id=1, source_target_pairs={{0,160},{2,162},{4,164},{6,166},{8,168},{10,170},{12,172},{14,174}... | collective-permute-start | bytes 24584 | tf_op jit(solution)/shard_map/ppermute | solution.py:403
  135.9 0.0 collective-permute-done.11.refs_7_
  135.9 2.7 %collective-permute-start.16 = (f32[8,256]{1,0:T(8,128)S(1)}, f32[8,256]{1,0:T(8,128)S(1)}, u32[]{:S(2)}, u32[]{:S(2)}) collective-permute-start(f32[8,256]{1,0:T(8,128)S(1)} %get-tuple-element.96), channel_id=1, source_target_pairs={{0,192},{2,194},{4,196},{6,198},{8,200},{10,202},{12,204},{14,206}... | collective-permute-start | bytes 24584 | tf_op jit(solution)/shard_map/ppermute | solution.py:403
  138.6 0.0 collective-permute-done.12.refs_8_
  138.6 2.6 %collective-permute-start.17 = (f32[8,256]{1,0:T(8,128)S(1)}, f32[8,256]{1,0:T(8,128)S(1)}, u32[]{:S(2)}, u32[]{:S(2)}) collective-permute-start(f32[8,256]{1,0:T(8,128)S(1)} %get-tuple-element.97), channel_id=1, source_target_pairs={{0,224},{2,226},{4,228},{6,230},{8,232},{10,234},{12,236},{14,238}... | collective-permute-start | bytes 24584 | tf_op jit(solution)/shard_map/ppermute | solution.py:403
  141.2 2.5 %down_grad.1 = (bf16[256,2048]{1,0:T(8,128)(2,1)}, f32[1,256]{1,0:T(1,128)}) custom-call(bf16[256,256]{1,0:T(8,128)(2,1)S(1)} %copy-done.9, bf16[256,256]{1,0:T(8,128)(2,1)S(1)} %copy-done.10, bf16[256,2048]{1,0:T(8,128)(2,1)S(1)} %copy-done.7, bf16[256,2048]{1,0:T(8,128)(2,1)S(1)} %copy-done.8), custom_call_target="tpu_custom_call" | custom-call | flops 1073741824 | bytes 4194304 | tf_op jit(solution)/shard_map/down_grad/pallas_call | solution.py:43
  143.7 0.0 collective-permute-done.13.refs_9_
  143.8 1.2 final.1
  (33 shorter events, 0.1 us)
Async XLA Ops:
  3.9 74.0 %copy-start.4 = (bf16[1,2048,256]{2,1,0:T(8,128)(2,1)S(1)}, bf16[1,2048,256]{2,1,0:T(8,128)(2,1)}, u32[]{:S(2)}) copy-start(bf16[1,2048,256]{2,1,0:T(8,128)(2,1)} %param.13) | copy-start | bytes 3145732
  4.0 74.0 %copy-start.5 = (bf16[1,2048,256]{2,1,0:T(8,128)(2,1)S(1)}, bf16[1,2048,256]{2,1,0:T(8,128)(2,1)}, u32[]{:S(2)}) copy-start(bf16[1,2048,256]{2,1,0:T(8,128)(2,1)} %param.14) | copy-start | bytes 3145732
  4.0 74.0 %copy-start.6 = (bf16[1,256,2048]{2,1,0:T(8,128)(2,1)S(1)}, bf16[1,256,2048]{2,1,0:T(8,128)(2,1)}, u32[]{:S(2)}) copy-start(bf16[1,256,2048]{2,1,0:T(8,128)(2,1)} %param.15) | copy-start | bytes 3145732
  77.9 4.5 %collective-permute-start = (bf16[1024,1152]{1,0:T(8,128)(2,1)S(1)}, bf16[1024,1152]{1,0:T(8,128)(2,1)S(1)}, u32[]{:S(2)}, u32[]{:S(2)}) collective-permute-start(bf16[1024,1152]{1,0:T(8,128)(2,1)S(1)} %bitcast.16), channel_id=1, source_target_pairs={{0,1},{1,0},{2,3},{3,2},{4,5},{5,4},{6,7},{7,6},{8,9},{9,8},{10,11... | collective-permute-start | bytes 7077896 | tf_op jit(solution)/shard_map/ppermute | solution.py:395
  80.8 4.7 %collective-permute-start.2 = (bf16[256,1152]{1,0:T(8,128)(2,1)S(1)}, bf16[256,1152]{1,0:T(8,128)(2,1)S(1)}, u32[]{:S(2)}, u32[]{:S(2)}) collective-permute-start(bf16[256,1152]{1,0:T(8,128)(2,1)S(1)} %get-tuple-element.65), channel_id=1, source_target_pairs={{0,1},{1,0},{2,3},{3,2},{4,5},{5,4},{6,7},{7,6},{8,9},{9,8},{10,11... | collective-permute-start | bytes 1769480 | tf_op jit(solution)/shard_map/ppermute | solution.py:395
  85.3 2.1 %collective-permute-start.1 = (bf16[256,1152]{1,0:T(8,128)(2,1)S(1)}, bf16[256,1152]{1,0:T(8,128)(2,1)S(1)}, u32[]{:S(2)}, u32[]{:S(2)}) collective-permute-start(bf16[256,1152]{1,0:T(8,128)(2,1)S(1)} %get-tuple-element.64), channel_id=1, source_target_pairs={{0,1},{1,0},{2,3},{3,2},{4,5},{5,4},{6,7},{7,6},{8,9},{9,8},{10,11... | collective-permute-start | bytes 1769480 | tf_op jit(solution)/shard_map/ppermute | solution.py:395
  87.4 10.3 %copy-start = (bf16[256,2048]{1,0:T(8,128)(2,1)S(1)}, bf16[256,2048]{1,0:T(8,128)(2,1)}, u32[]{:S(2)}) copy-start(bf16[256,2048]{1,0:T(8,128)(2,1)} %get-tuple-element.72.x0_ref) | copy-start | bytes 3145732
  87.4 10.3 %copy-start.1 = (bf16[256,2048]{1,0:T(8,128)(2,1)S(1)}, bf16[256,2048]{1,0:T(8,128)(2,1)}, u32[]{:S(2)}) copy-start(bf16[256,2048]{1,0:T(8,128)(2,1)} %get-tuple-element.73.x1_ref) | copy-start | bytes 3145732
  90.8 15.2 %copy-start.13 = (bf16[256,256]{1,0:T(8,128)(2,1)S(1)}, bf16[256,256]{1,0:T(8,128)(2,1)}, u32[]{:S(2)}) copy-start(bf16[256,256]{1,0:T(8,128)(2,1)} %get-tuple-element.77.d0_ref) | copy-start | bytes 393220
  90.8 15.2 %copy-start.14 = (bf16[256,256]{1,0:T(8,128)(2,1)S(1)}, bf16[256,256]{1,0:T(8,128)(2,1)}, u32[]{:S(2)}) copy-start(bf16[256,256]{1,0:T(8,128)(2,1)} %get-tuple-element.78.d1_ref) | copy-start | bytes 393220
  90.8 52.9 %all-to-all-start.1 = ((bf16[128,8,512]{2,1,0:T(8,128)(2,1)}), bf16[128,8,512]{2,1,0:T(8,128)(2,1)S(1)}, u32[]{:S(2)}, u32[]{:S(2)}) async-start(bf16[128,8,512]{2,1,0:T(8,128)(2,1)} %bitcast.26), calls=%async_computation.1 | async-start | bytes 2097152 | tf_op jit(solution)/shard_map/all_to_all | solution.py:391
  97.8 0.8 copy-start.2
  98.6 0.8 copy-start.3
  100.3 17.5 %copy-start.11 = (bf16[256,256]{1,0:T(8,128)(2,1)S(1)}, bf16[256,256]{1,0:T(8,128)(2,1)}, u32[]{:S(2)}) copy-start(bf16[256,256]{1,0:T(8,128)(2,1)} %get-tuple-element.74.d0_ref) | copy-start | bytes 393220
  100.3 17.5 %copy-start.12 = (bf16[256,256]{1,0:T(8,128)(2,1)S(1)}, bf16[256,256]{1,0:T(8,128)(2,1)}, u32[]{:S(2)}) copy-start(bf16[256,256]{1,0:T(8,128)(2,1)} %get-tuple-element.75.d1_ref) | copy-start | bytes 393220
  100.3 12.3 %collective-permute-start.5 = (bf16[256,128]{1,0:T(8,128)(2,1)S(1)}, bf16[256,128]{1,0:T(8,128)(2,1)S(1)}, u32[]{:S(2)}, u32[]{:S(2)}) collective-permute-start(bf16[256,128]{1,0:T(8,128)(2,1)S(1)} %get-tuple-element.83), channel_id=1, source_target_pairs={{0,2},{2,4},{4,6},{6,0},{8,10},{10,12},{12,14},{14,8},{16,18},{18,... | collective-permute-start | bytes 196616 | tf_op jit(solution)/shard_map/ppermute | solution.py:403
  101.9 10.7 %collective-permute-start.6 = (bf16[256,128]{1,0:T(8,128)(2,1)S(1)}, bf16[256,128]{1,0:T(8,128)(2,1)S(1)}, u32[]{:S(2)}, u32[]{:S(2)}) collective-permute-start(bf16[256,128]{1,0:T(8,128)(2,1)S(1)} %get-tuple-element.84), channel_id=1, source_target_pairs={{0,4},{2,6},{4,0},{6,2},{8,12},{10,14},{12,8},{14,10},{16,20},{18,... | collective-permute-start | bytes 196616 | tf_op jit(solution)/shard_map/ppermute | solution.py:403
  104.6 8.0 %collective-permute-start.7 = (bf16[256,128]{1,0:T(8,128)(2,1)S(1)}, bf16[256,128]{1,0:T(8,128)(2,1)S(1)}, u32[]{:S(2)}, u32[]{:S(2)}) collective-permute-start(bf16[256,128]{1,0:T(8,128)(2,1)S(1)} %get-tuple-element.85), channel_id=1, source_target_pairs={{0,6},{2,0},{4,2},{6,4},{8,14},{10,8},{12,10},{14,12},{16,22},{18,... | collective-permute-start | bytes 196616 | tf_op jit(solution)/shard_map/ppermute | solution.py:403
  112.6 18.7 %collective-permute-start.4 = (f32[1,2048]{1,0:T(1,128)S(1)}, f32[1,2048]{1,0:T(1,128)S(1)}, u32[]{:S(2)}, u32[]{:S(2)}) collective-permute-start(f32[1,2048]{1,0:T(1,128)S(1)} %get-tuple-element.79.refs_4_), channel_id=1, source_target_pairs={{0,1},{1,0},{2,3},{3,2},{4,5},{5,4},{6,7},{7,6},{8,9},{9,8},{10,11... | collective-permute-start | bytes 24584 | tf_op jit(solution)/shard_map/ppermute | solution.py:395
  112.7 11.7 %collective-permute-start.10 = (f32[64,128]{1,0:T(8,128)S(1)}, f32[64,128]{1,0:T(8,128)S(1)}, u32[]{:S(2)}, u32[]{:S(2)}) collective-permute-start(f32[64,128]{1,0:T(8,128)S(1)} %get-tuple-element.89), channel_id=1, source_target_pairs={{0,24},{2,26},{4,28},{6,30},{8,0},{10,2},{12,4},{14,6},{16,8},{18,... | collective-permute-start | bytes 98312 | tf_op jit(solution)/shard_map/ppermute | solution.py:403
  115.5 8.9 %collective-permute-start.8 = (f32[64,128]{1,0:T(8,128)S(1)}, f32[64,128]{1,0:T(8,128)S(1)}, u32[]{:S(2)}, u32[]{:S(2)}) collective-permute-start(f32[64,128]{1,0:T(8,128)S(1)} %get-tuple-element.87), channel_id=1, source_target_pairs={{0,8},{2,10},{4,12},{6,14},{8,16},{10,18},{12,20},{14,22},{16,24},... | collective-permute-start | bytes 98312 | tf_op jit(solution)/shard_map/ppermute | solution.py:403
  115.5 8.9 %collective-permute-start.9 = (f32[64,128]{1,0:T(8,128)S(1)}, f32[64,128]{1,0:T(8,128)S(1)}, u32[]{:S(2)}, u32[]{:S(2)}) collective-permute-start(f32[64,128]{1,0:T(8,128)S(1)} %get-tuple-element.88), channel_id=1, source_target_pairs={{0,16},{2,18},{4,20},{6,22},{8,24},{10,26},{12,28},{14,30},{16,0},... | collective-permute-start | bytes 98312 | tf_op jit(solution)/shard_map/ppermute | solution.py:403
  117.8 23.4 %copy-start.7 = (bf16[256,2048]{1,0:T(8,128)(2,1)S(1)}, bf16[256,2048]{1,0:T(8,128)(2,1)}, u32[]{:S(2)}) copy-start(bf16[256,2048]{1,0:T(8,128)(2,1)} %get-tuple-element.103.s0_ref) | copy-start | bytes 3145732
  117.8 23.4 %copy-start.8 = (bf16[256,2048]{1,0:T(8,128)(2,1)S(1)}, bf16[256,2048]{1,0:T(8,128)(2,1)}, u32[]{:S(2)}) copy-start(bf16[256,2048]{1,0:T(8,128)(2,1)} %get-tuple-element.104.s1_ref) | copy-start | bytes 3145732
  117.8 23.4 %copy-start.9 = (bf16[256,256]{1,0:T(8,128)(2,1)S(1)}, bf16[256,256]{1,0:T(8,128)(2,1)}, u32[]{:S(2)}) copy-start(bf16[256,256]{1,0:T(8,128)(2,1)} %get-tuple-element.101.h0_ref) | copy-start | bytes 393220
  117.8 23.4 %copy-start.10 = (bf16[256,256]{1,0:T(8,128)(2,1)S(1)}, bf16[256,256]{1,0:T(8,128)(2,1)}, u32[]{:S(2)}) copy-start(bf16[256,256]{1,0:T(8,128)(2,1)} %get-tuple-element.102.h1_ref) | copy-start | bytes 393220
  124.4 9.7 %collective-permute-start.3 = (f32[1,2048]{1,0:T(1,128)S(1)}, f32[1,2048]{1,0:T(1,128)S(1)}, u32[]{:S(2)}, u32[]{:S(2)}) collective-permute-start(f32[1,2048]{1,0:T(1,128)S(1)} %get-tuple-element.76.refs_2_), channel_id=1, source_target_pairs={{0,1},{1,0},{2,3},{3,2},{4,5},{5,4},{6,7},{7,6},{8,9},{9,8},{10,11... | collective-permute-start | bytes 24584 | tf_op jit(solution)/shard_map/ppermute | solution.py:395
  124.5 11.3 %collective-permute-start.11 = (f32[8,256]{1,0:T(8,128)S(1)}, f32[8,256]{1,0:T(8,128)S(1)}, u32[]{:S(2)}, u32[]{:S(2)}) collective-permute-start(f32[8,256]{1,0:T(8,128)S(1)} %get-tuple-element.91), channel_id=1, source_target_pairs={{0,32},{2,34},{4,36},{6,38},{8,40},{10,42},{12,44},{14,46},{16,48}... | collective-permute-start | bytes 24584 | tf_op jit(solution)/shard_map/ppermute | solution.py:403
  126.2 12.4 %collective-permute-start.12 = (f32[8,256]{1,0:T(8,128)S(1)}, f32[8,256]{1,0:T(8,128)S(1)}, u32[]{:S(2)}, u32[]{:S(2)}) collective-permute-start(f32[8,256]{1,0:T(8,128)S(1)} %get-tuple-element.92), channel_id=1, source_target_pairs={{0,64},{2,66},{4,68},{6,70},{8,72},{10,74},{12,76},{14,78},{16,80}... | collective-permute-start | bytes 24584 | tf_op jit(solution)/shard_map/ppermute | solution.py:403
  130.3 13.4 %collective-permute-start.13 = (f32[8,256]{1,0:T(8,128)S(1)}, f32[8,256]{1,0:T(8,128)S(1)}, u32[]{:S(2)}, u32[]{:S(2)}) collective-permute-start(f32[8,256]{1,0:T(8,128)S(1)} %get-tuple-element.93), channel_id=1, source_target_pairs={{0,96},{2,98},{4,100},{6,102},{8,104},{10,106},{12,108},{14,110},{... | collective-permute-start | bytes 24584 | tf_op jit(solution)/shard_map/ppermute | solution.py:403
  131.3 12.4 %collective-permute-start.14 = (f32[8,256]{1,0:T(8,128)S(1)}, f32[8,256]{1,0:T(8,128)S(1)}, u32[]{:S(2)}, u32[]{:S(2)}) collective-permute-start(f32[8,256]{1,0:T(8,128)S(1)} %get-tuple-element.94), channel_id=1, source_target_pairs={{0,128},{2,130},{4,132},{6,134},{8,136},{10,138},{12,140},{14,142}... | collective-permute-start | bytes 24584 | tf_op jit(solution)/shard_map/ppermute | solution.py:403
  134.1 9.6 %collective-permute-start.15 = (f32[8,256]{1,0:T(8,128)S(1)}, f32[8,256]{1,0:T(8,128)S(1)}, u32[]{:S(2)}, u32[]{:S(2)}) collective-permute-start(f32[8,256]{1,0:T(8,128)S(1)} %get-tuple-element.95), channel_id=1, source_target_pairs={{0,160},{2,162},{4,164},{6,166},{8,168},{10,170},{12,172},{14,174}... | collective-permute-start | bytes 24584 | tf_op jit(solution)/shard_map/ppermute | solution.py:403
  135.9 7.9 %collective-permute-start.16 = (f32[8,256]{1,0:T(8,128)S(1)}, f32[8,256]{1,0:T(8,128)S(1)}, u32[]{:S(2)}, u32[]{:S(2)}) collective-permute-start(f32[8,256]{1,0:T(8,128)S(1)} %get-tuple-element.96), channel_id=1, source_target_pairs={{0,192},{2,194},{4,196},{6,198},{8,200},{10,202},{12,204},{14,206}... | collective-permute-start | bytes 24584 | tf_op jit(solution)/shard_map/ppermute | solution.py:403
  138.6 5.1 %collective-permute-start.17 = (f32[8,256]{1,0:T(8,128)S(1)}, f32[8,256]{1,0:T(8,128)S(1)}, u32[]{:S(2)}, u32[]{:S(2)}) collective-permute-start(f32[8,256]{1,0:T(8,128)S(1)} %get-tuple-element.97), channel_id=1, source_target_pairs={{0,224},{2,226},{4,228},{6,230},{8,232},{10,234},{12,236},{14,238}... | collective-permute-start | bytes 24584 | tf_op jit(solution)/shard_map/ppermute | solution.py:403

commit v3 on v1

--- a/solution.py
+++ b/solution.py
@@ -1,3 +1,5 @@
+import functools
+
 import jax
 import jax.numpy as jnp
 from jax import lax
@@ -5,6 +7,7 @@
 from jax.experimental.pallas import tpu as pltpu
 from jax.sharding import PartitionSpec as P
 
+
 BF = jnp.bfloat16
 F32 = jnp.float32
 GROUP_LANE = 32
@@ -29,15 +32,25 @@
     return lax.broadcasted_iota(jnp.int32, shape, dim)
 
 
-def call(kernel, name, flops, limit, outs, scalars, arrays, scratch=(), spaces=None):
+VM = pl.BlockSpec(memory_space=pltpu.VMEM)
+HB = pl.BlockSpec(memory_space=pltpu.HBM)
+
+
+def far(x):
+    return pltpu.with_memory_space_constraint(x, pltpu.HBM)
+
+
+def call(kernel, flops, limit, outs, scalars, arrays, scratch=(), spaces=None, out_spaces=None):
     smem = pl.BlockSpec(memory_space=pltpu.SMEM)
     vmem = pl.BlockSpec(memory_space=pltpu.VMEM)
     return pl.pallas_call(
         kernel,
-        name=name,
-        out_shape=[jax.ShapeDtypeStruct(shape, dtype) for shape, dtype in outs],
+        out_shape=[
+            pltpu.HBM(shape, dtype) if out_spaces and out_spaces[k] is HB else jax.ShapeDtypeStruct(shape, dtype)
+            for k, (shape, dtype) in enumerate(outs)
+        ],
         in_specs=[smem] * len(scalars) + (spaces or [vmem] * len(arrays)),
-        out_specs=[vmem] * len(outs),
+        out_specs=out_spaces or [vmem] * len(outs),
         scratch_shapes=list(scratch),
         cost_estimate=pl.CostEstimate(flops=flops, bytes_accessed=4 << 20, transcendentals=0),
         compiler_params=pltpu.CompilerParams(vmem_limit_bytes=limit << 20),
@@ -49,8 +62,8 @@
 
 
 def pre_kernel(
-    tp_ref, rt_ref, rgt_ref, tok_hbm, cot_hbm, rex_hbm,
-    send_ref, aux_ref, tok_ref, cot_ref, rex_ref, one_ref, sems,
+    ep_ref, tp_ref, rt_hbm, rgt_hbm, tok_hbm, cot_hbm, rex_hbm,
+    send_out, aux_ref, send_ref, rt_ref, rgt_ref, tok_ref, cot_ref, rex_ref, one_ref, sems,
 ):
     tp = tp_ref[0]
     tok, dm = tok_ref.shape
@@ -60,10 +73,13 @@
     width = dm // 4
     loads = [
         pltpu.make_async_copy(src, dst, sems.at[k])
-        for k, (src, dst) in enumerate(((tok_hbm, tok_ref), (rex_hbm, rex_ref), (cot_hbm, cot_ref)))
+        for k, (src, dst) in enumerate(
+            ((rt_hbm, rt_ref), (tok_hbm, tok_ref), (rgt_hbm, rgt_ref), (rex_hbm, rex_ref), (cot_hbm, cot_ref))
+        )
     ]
     for load in loads:
         load.start()
+    loads[0].wait()
     r0, r1 = rt_ref[0:1, :], rt_ref[1:2, :]
     before = ones_where(iota((tok, tok), 0) < iota((tok, tok), 1))
     blk = min(256, experts * 8)
@@ -87,13 +103,21 @@
     def stacked(ref):
         return jnp.concatenate([ref[:, c * width : (c + 1) * width] for c in range(4)], axis=0)
 
-    loads[0].wait()
+    saves = []
+
+    def save(k, rows, cols):
+        saves.append(pltpu.make_async_copy(send_ref.at[rows, cols], send_out.at[rows, cols], sems.at[5 + k]))
+        saves[-1].start()
+
+    loads[1].wait()
     stack = stacked(tok_ref)
     for b in range(blocks):
         rows = slice(b * blk, (b + 1) * blk)
         one = one_ref[0, rows, :].astype(F32) + one_ref[1, rows, :].astype(F32)
         send_ref[rows, 0:width] = mm(spread(one), stack).astype(BF)
-    loads[1].wait()
+        save(2 * b, rows, slice(0, width))
+    loads[2].wait()
+    loads[3].wait()
     group_exp = jnp.exp(nt(rgt_ref[...], tok_ref[...]))
     group_prob = group_exp / jnp.sum(group_exp, axis=0, keepdims=True)
     logits = jnp.transpose(mm(tok_ref[...], rex_ref[...]))
@@ -107,36 +131,114 @@
     picked = jnp.sum(jnp.where(gi == chosen, group_prob, 0.0), axis=0, keepdims=True)
     w0 = (picked * p0).astype(BF).astype(F32)
     w1 = (picked * p1).astype(BF).astype(F32)
-    li = iota((EXTRA, tok), 0) & (LOW_LANE - 1)
-    diff = jnp.where(li == r0 - chosen * gw, 1.0, 0.0) - jnp.where(li == r1 - chosen * gw, 1.0, 0.0)
-    group_side = jnp.where(li == GROUP_LANE + chosen, 1.0, 0.0)
-    for j in range(groups):
-        group_side = group_side - jnp.where(li == GROUP_LANE + j, group_prob[j : j + 1, :], 0.0)
-    side_t = jnp.concatenate([(p1 * diff + group_side).astype(BF), (group_side - p0 * diff).astype(BF)], axis=1)
     arow = iota((EXTRA, tok), 0)
     aux = jnp.where(arow == 0, p0, jnp.where(arow == 1, p1, 0.0))
     for j in range(groups):
         aux = jnp.where(arow == 2 + j, group_prob[j : j + 1, :], aux)
     aux = jnp.where(arow == 6, r0.astype(F32), jnp.where(arow == 7, r1.astype(F32), aux))
-    aux_ref[...] = jnp.transpose(aux)
-    loads[2].wait()
+    aux_ref[...] = aux
+    loads[4].wait()
     stack = stacked(cot_ref)
     for b in range(blocks):
         rows = slice(b * blk, (b + 1) * blk)
         one0, one1 = one_ref[0, rows, :].astype(F32), one_ref[1, rows, :].astype(F32)
         send_ref[rows, width : 2 * width] = mm(spread(one0 * w0 + one1 * w1), stack).astype(BF)
-        head = part == 0
-        both = jnp.concatenate(
-            [jnp.where(head, one0, 0.0).astype(BF), jnp.where(head, one1, 0.0).astype(BF)], axis=1
+        save(2 * b + 1, rows, slice(width, 2 * width))
+    for copy in saves:
+        copy.wait()
+
+
+def pick_rows(outs, rows_in, stride, at):
+    n = rows_in.shape[0] // stride
+    for d, out_ref in enumerate(outs):
+        want = iota((n, n * stride), 0) * stride + ((at + d) & (stride - 1))
+        out_ref[...] = mm(ones_where(iota((n, n * stride), 1) == want), rows_in).astype(BF)
+
+
+def side_x_kernel(groups, ep_ref, aux_ref, *outs):
+    tok = aux_ref.shape[1]
+    experts = outs[0].shape[0] * 4
+    gw = experts // groups
+    r0, r1 = aux_ref[6:7, :].astype(jnp.int32), aux_ref[7:8, :].astype(jnp.int32)
+    ei = iota((experts, tok), 0)
+    one0 = jnp.where(ei == r0, 1.0, 0.0)
+    one1 = jnp.where(ei == r1, 1.0, 0.0)
+    before = ones_where(iota((tok, tok), 0) < iota((tok, tok), 1))
+    rank = mm((one0 + one1).astype(BF), before)
+    li = iota((EXTRA, tok), 0)
+    base = (r0 // gw) * gw
+    shared = jnp.zeros((EXTRA, tok), F32)
+    for j in range(groups):
+        shared = jnp.where((li & 7) == 2 + j, aux_ref[2 + j : 3 + j, :], shared)
+    kinds = []
+    for other, prob in ((r1, aux_ref[1:2, :]), (r0, aux_ref[0:1, :])):
+        kinds.append(
+            jnp.where((li & 7) == 0, (other - base).astype(F32), jnp.where((li & 7) == 1, prob, shared))
         )
-        send_ref[rows, 2 * width :] = nt(both, side_t).astype(BF)
-
-
-def expert_kernel(
-    tp_ref, got_ref, gate_ref, up_ref, down_ref,
-    x_ref, sc_ref, z_ref, gd_ref, ud_ref, hid_ref, u_ref, mine_ref, theirs_ref,
-):
+    total = None
+    for r in range(4):
+        for one, kind in ((one0, kinds[0]), (one1, kinds[1])):
+            left = jnp.where(rank == float(r), one, 0.0).astype(BF)
+            right = jnp.where((li >> 3) == r, kind, 0.0).astype(BF)
+            term = nt(left, right)
+            total = term if total is None else total + term
+    pick_rows(outs, total.astype(BF), 4, ep_ref[0] & 3)
+
+
+def side_y_kernel(ep_ref, a_ref, b_ref, c_ref, d_ref, *outs):
+    rows = jnp.concatenate([a_ref[...], b_ref[...], c_ref[...], d_ref[...]], axis=0)
+    pick_rows(outs, rows, 4, (ep_ref[0] >> 2) & 3)
+
+
+def side_z_kernel(ep_ref, a_ref, b_ref, c_ref, d_ref, *outs):
+    rows = jnp.concatenate([a_ref[...], b_ref[...], c_ref[...], d_ref[...]], axis=0)
+    pick_rows(outs, rows, len(outs), ep_ref[0] >> 4)
+
+
+def side_end_kernel(groups, ep_ref, tp_ref, *refs):
+    ins, outs = refs[:-2], refs[-2:]
+    rows = jnp.concatenate([ref[...] for ref in ins], axis=0)
+    experts = rows.shape[0]
+    planes = len(ins)
+    gw = experts // groups
+    e, tp = ep_ref[0], tp_ref[0]
+    n = experts * 2
+    src = iota((n, experts), 0) >> 1
+    dz = ((e >> 4) - (src >> 4)) & (planes - 1)
+    dy = ((e >> 2) - (src >> 2)) & 3
+    dx = (e - src) & 3
+    spread = mm(ones_where(iota((n, experts), 1) == dz * 16 + dy * 4 + dx), rows)
+    lane = iota((n, EXTRA), 1)
+    li = lane & (LOW_LANE - 1)
+    chosen = e // gw
+    own = jnp.where(li == e - chosen * gw, 1.0, 0.0)
+    mark = jnp.where(li == GROUP_LANE + chosen, 1.0, 0.0)
+    for p, out_ref in enumerate(outs):
+        slot = 2 * ((tp + p) & 1) + (iota((n, EXTRA), 0) & 1)
+
+        def value(v):
+            return jnp.sum(jnp.where(lane == slot * 8 + v, spread, 0.0), axis=1, keepdims=True)
+
+        z = value(1) * (own - jnp.where(li.astype(F32) == value(0), 1.0, 0.0)) + mark
+        for j in range(groups):
+            z = z - jnp.where(li == GROUP_LANE + j, value(2 + j), 0.0)
+        out_ref[...] = z.astype(BF)
+
+
+def expert_kernel(load, tp_ref, got_ref, *refs):
     tp = tp_ref[0]
+    weights, refs = refs[:3], refs[3:]
+    u_ref, mine_ref, theirs_ref, x_ref, x_out, sc_out, gd_out, ud_out, hid_out = refs[:9]
+    sc_ref, gd_ref, ud_ref, hid_ref, sems = refs[-5:]
+    gate_ref, up_ref, down_ref = refs[9:12] if load else weights
+    loads = []
+    if load:
+        loads = [
+            pltpu.make_async_copy(src, dst, sems.at[5 + k])
+            for k, (src, dst) in enumerate(zip(weights, (gate_ref, up_ref, down_ref)))
+        ]
+        for copy in loads:
+            copy.start()
     dm = gate_ref.shape[0]
     width, half = dm // 4, dm // 2
     blk = min(256, got_ref.shape[0])
@@ -152,9 +254,22 @@
             cols = slice(c * width, (c + 1) * width)
             x_ref[rows, cols] = y[c * n4 : (c + 1) * n4, 0:width]
             sc_ref[rows, cols] = y[c * n4 : (c + 1) * n4, width:]
-        z_ref[rows, :] = mm(perm[0:n4], got_ref[block, 2 * width :]).astype(BF)
+    saves = [
+        pltpu.make_async_copy(src, dst, sems.at[k])
+        for k, (src, dst) in enumerate(
+            ((x_ref, x_out), (sc_ref, sc_out), (gd_ref, gd_out), (ud_ref, ud_out), (hid_ref, hid_out))
+        )
+    ]
+    saves[0].start()
+    saves[1].start()
+    if load:
+        loads[0].wait()
     gp = mm(x_ref[...], gate_ref[...])
+    if load:
+        loads[1].wait()
     upre = mm(x_ref[...], up_ref[...])
+    if load:
+        loads[2].wait()
     pulled = nt(sc_ref[...], down_ref[...])
     sig = 1.0 / (1.0 + jnp.exp(-gp))
     act = gp * sig
@@ -165,6 +280,8 @@
     ud = (pulled * act).astype(BF)
     gd_ref[...] = gd
     ud_ref[...] = ud
+    for save in saves[2:]:
+        save.start()
     n = x_ref.shape[0]
     u_ref[...] = jnp.broadcast_to(u, (n, EXTRA))
     high = u.astype(BF).astype(F32)
@@ -174,12 +291,15 @@
     theirs_ref[:, 0:half] = (nt(gd, gate_ref[far, :]) + nt(ud, up_ref[far, :])).astype(BF)
     near = pl.ds(pl.multiple_of(tp * half, half), half)
     mine_ref[...] = (nt(gd, gate_ref[near, :]) + nt(ud, up_ref[near, :])).astype(BF)
+    for save in saves:
+        save.wait()
 
 
 def pack_kernel(tp_ref, *refs):
     tp = tp_ref[0]
     mine, came, us, zs, xs = refs[0:2], refs[2:4], refs[4:6], refs[6:8], refs[8:10]
-    ret_ref, y0_ref, y1_ref, ul_ref = refs[10:14]
+    ret_out, ret_ref, y0_ref, y1_ref, ul_ref, sems = refs[10:16]
+    saves = []
     n, half = mine[0].shape
     width = half // 2
     lane = iota((n, EXTRA), 1)
@@ -208,12 +328,16 @@
         rc = jnp.where(tp == 0, rc[:, 0:8, :], rc[:, 8:16, :]).reshape(blk, EXTRA)
         high = rc.astype(BF).astype(F32)
         ret_ref[out, width:] = (base + jnp.where(wide, high, rc - high)).astype(BF)
+        saves.append(pltpu.make_async_copy(ret_ref.at[out, :], ret_out.at[out, :], sems.at[b]))
+        saves[-1].start()
+    for save in saves:
+        save.wait()
 
 
 def grads_kernel(*refs):
     x, sc, gd, ud, hid = (refs[2 * k : 2 * k + 2] for k in range(5))
     gate_ref, up_ref, down_ref, sq_ref, down_sq_ref, acc_ref = refs[10:]
-    dm, ff = gate_ref.shape
+    dm, _ = gate_ref.shape
     blk = 128
     wide = 512 if dm % 512 == 0 else 128
 
@@ -242,8 +366,9 @@
     down_sq_ref[...] = jnp.transpose(acc_ref[...])[0:1, :]
 
 
-def home_kernel(tp_ref, aux_ref, rg_ref, rex_ref, sel_ref, q_ref, h_ref):
+def home_kernel(tp_ref, raux_ref, rg_ref, rex_ref, sel_ref, q_ref, h_ref, aux_ref):
     tp = tp_ref[0]
+    aux_ref[...] = jnp.transpose(raux_ref[...])
     tok = aux_ref.shape[0]
     half = q_ref.shape[1]
     groups = rg_ref.shape[0]
@@ -324,6 +449,9 @@
     tp = lax.axis_index("tp").reshape(1)
     swap = [(0, 1), (1, 0)]
     rgt = router_group.T
+    ep = lax.axis_index("ep")
+    planes = experts // 16
+    idx = [ep.reshape(1), tp]
     gate, up, down = gate_proj[0], up_proj[0], down_proj[0]
 
     def exchange(x):
@@ -334,46 +462,81 @@
     def partner(x):
         return lax.ppermute(x, "tp", swap)
 
+    def shift(v, stride, d):
+        size = planes if stride == 16 else 4
+        pairs = []
+        for e in range(experts):
+            at = e // stride % size
+            pairs.append((e, e + ((at + d) % size - at) * stride))
+        return lax.ppermute(v, "ep", pairs)
+
     send, aux = call(
-        pre_kernel, "pre", 1 << 30, 20,
-        [((experts * 8, 2 * width + EXTRA), BF), ((tok, EXTRA), F32)],
-        [tp], [routes.T, rgt, tokens, cotangent, router_expert],
+        pre_kernel, 1 << 30, 20,
+        [((experts * 8, 2 * width), BF), ((EXTRA, tok), F32)],
+        idx, [far(routes.T), far(rgt), far(tokens), far(cotangent), far(router_expert)],
         scratch=[
+            pltpu.VMEM((experts * 8, 2 * width), BF), pltpu.VMEM((2, tok), jnp.int32), pltpu.VMEM((groups, dm), BF),
             pltpu.VMEM((tok, dm), BF), pltpu.VMEM((tok, dm), BF), pltpu.VMEM((dm, experts), BF),
-            pltpu.VMEM((2, experts * 8, tok), BF), pltpu.SemaphoreType.DMA((3,)),
+            pltpu.VMEM((2, experts * 8, tok), BF), pltpu.SemaphoreType.DMA((13,)),
         ],
-        spaces=[pl.BlockSpec(memory_space=pltpu.VMEM)] * 2 + [pl.BlockSpec(memory_space=pl.ANY)] * 3,
+        spaces=[HB] * 5,
+        out_spaces=[HB, VM],
     )
     got = exchange(send)
+    sides = call(
+        functools.partial(side_x_kernel, groups), 1 << 28, 6,
+        [((experts // 4, EXTRA), BF)] * 4, idx[:1], [aux],
+    )
+    sides = [shift(v, 1, d) if d else v for d, v in enumerate(sides)]
+    sides = call(side_y_kernel, 1 << 24, 6, [((experts // 4, EXTRA), BF)] * 4, idx[:1], sides)
+    sides = [shift(v, 4, d) if d else v for d, v in enumerate(sides)]
+    sides = call(side_z_kernel, 1 << 24, 6, [((16, EXTRA), BF)] * planes, idx[:1], sides)
+    sides = [shift(v, 16, d) if d else v for d, v in enumerate(sides)]
+    z = call(functools.partial(side_end_kernel, groups), 1 << 24, 6, [((n, EXTRA), BF)] * 2, idx, sides)
     other = partner(got)
-    x, sc, z, gd, ud, hid, u, mine, theirs = [list(v) for v in zip(*[
-        call(
-            expert_kernel, "expert", 3 << 30, 18,
-            [((n, dm), BF), ((n, dm), BF), ((n, EXTRA), BF), ((n, ff), BF), ((n, ff), BF), ((n, ff), BF),
-             ((n, EXTRA), F32), ((n, half), BF), ((n, half + EXTRA), BF)],
-            [tp], [g, gate, up, down],
+
+    def expert(g, weights, load):
+        held = [((dm, ff), BF), ((dm, ff), BF), ((ff, dm), BF)] if load else []
+        return call(
+            functools.partial(expert_kernel, load), 3 << 30, 18,
+            [((n, EXTRA), F32), ((n, half), BF), ((n, half + EXTRA), BF), ((n, dm), BF),
+             ((n, dm), BF), ((n, dm), BF), ((n, ff), BF), ((n, ff), BF), ((n, ff), BF)] + held,
+            [tp], [g, *weights],
+            scratch=[pltpu.VMEM((n, w), BF) for w in (dm, ff, ff, ff)] + [pltpu.SemaphoreType.DMA((8,))],
+            spaces=[VM] + [HB if load else VM] * 3,
+            out_spaces=[VM] * 4 + [HB] * 5 + [VM] * len(held),
         )
-        for g in (got, other)
-    ])]
+
+    first = expert(got, [far(gate), far(up), far(down)], True)
+    second = expert(other, first[9:], False)
+    u, mine, theirs, xv, x, sc, gd, ud, hid = [list(v) for v in zip(first[:9], second)]
     came = [partner(theirs[1]), partner(theirs[0])]
-    ret = call_pack(tp, mine, came, u, z, x, experts, width)
+    (ret,) = call(
+        pack_kernel, 1 << 29, 16, [((experts * 8, width + EXTRA), BF)],
+        [tp], [*mine, *came, *u, *z, *xv],
+        scratch=[
+            pltpu.VMEM((experts * 8, width + EXTRA), BF), pltpu.VMEM((n, EXTRA), BF), pltpu.VMEM((n, EXTRA), BF),
+            pltpu.VMEM((2 * n, EXTRA), BF), pltpu.SemaphoreType.DMA((4,)),
+        ],
+        out_spaces=[HB],
+    )
     back = exchange(ret)
-    sel, q, h = call(
-        home_kernel, "home", 1 << 29, 8,
-        [((4, tok, experts * 8), BF), ((tok, half), F32), ((tok, half), F32)],
-        [tp], [aux, rgt, router_expert],
-    )
     gate_grad, up_grad, down_grad, sq, down_sq = call(
-        grads_kernel, "grads", 3 << 30, 20,
+        grads_kernel, 3 << 30, 20,
         [((dm, ff), BF), ((dm, ff), BF), ((ff, dm), BF), ((2, dm), F32), ((1, ff), F32)],
         [], [*x, *sc, *gd, *ud, *hid], scratch=[pltpu.VMEM((ff, 128), F32)],
     )
     sq_other = partner(sq)
+    sel, q, h, aux_cols = call(
+        home_kernel, 1 << 29, 8,
+        [((4, tok, experts * 8), BF), ((tok, half), F32), ((tok, half), F32), ((tok, EXTRA), F32)],
+        [tp], [aux, rgt, router_expert],
+    )
     token_grad, rex_grad, rg_grad, rows, gate_sq, up_sq = call(
-        final_kernel, "final", 1 << 29, 10,
+        final_kernel, 1 << 29, 10,
         [((tok, half), BF), ((8, experts), F32), ((groups, 8), F32), ((1, 8), F32),
          ((1, dm), F32), ((1, dm), F32)],
-        [], [back, sel, aux, q, h, sq, sq_other],
+        [], [back, sel, aux_cols, q, h, sq, sq_other],
     )
     return (
         token_grad,
@@ -387,21 +550,6 @@
         rg_grad.T,
         rows[0],
     )
-
-
-def call_pack(tp, mine, came, u, z, x, experts, width):
-    n = mine[0].shape[0]
-    vmem = pl.BlockSpec(memory_space=pltpu.VMEM)
-    return pl.pallas_call(
-        pack_kernel,
-        name="pack",
-        out_shape=jax.ShapeDtypeStruct((experts * 8, width + EXTRA), BF),
-        in_specs=[pl.BlockSpec(memory_space=pltpu.SMEM)] + [vmem] * 10,
-        out_specs=vmem,
-        scratch_shapes=[pltpu.VMEM((n, EXTRA), BF), pltpu.VMEM((n, EXTRA), BF), pltpu.VMEM((2 * n, EXTRA), BF)],
-        cost_estimate=pl.CostEstimate(flops=1 << 29, bytes_accessed=4 << 20, transcendentals=0),
-        compiler_params=pltpu.CompilerParams(vmem_limit_bytes=16 << 20),
-    )(tp, *mine, *came, *u, *z, *x)
 
 
 def solution(mesh):

time: 140 us -> 160 us (1.14)
  starting transfers between devices: 7.41 us -> 32.2 us
  local copies, waits for them, and re-layouts: 14 us -> 7.89 us
  Pallas kernels: 22.1 us -> 27.8 us
  blocking collectives: 74 us -> 68.4 us
    ppermute x0 -> x13, starting transfers between devices: none -> 19.1 us  [shift(): return lax.ppermute(v, 'ep', pairs)]
    ppermute x0 -> x13, waiting for transfers between devices: none -> 9.6 us  [shift(): return lax.ppermute(v, 'ep', pairs)]
    all_to_all x1, waiting for transfers between devices: 18.6 us -> 12.4 us  [exchange(): lax.all_to_all(x.reshape(experts, 8, m), 'ep', split_axis=0, concat_axis=...]
    unnamed x52 -> x28, local copies, waits for them, and re-layouts: 14 us -> 7.89 us
    pallas_call x7 -> x11, Pallas kernels: 22.1 us -> 27.8 us  [call(): pl.pallas_call(kernel, out_shape=[pltpu.HBM(shape, dtype) if out_spaces a...]
    all_to_all x1, blocking collectives: 74 us -> 68.4 us  [exchange(): lax.all_to_all(x.reshape(experts, 8, m), 'ep', split_axis=0, concat_axis=...]
    all_to_all x1, starting transfers between devices: 6.77 us -> 12.3 us  [exchange(): lax.all_to_all(x.reshape(experts, 8, m), 'ep', split_axis=0, concat_axis=...]
    ppermute x4, waiting for transfers between devices: 2.57 us -> 0.45 us  [partner(): return lax.ppermute(x, 'tp', swap)]
  transfers between devices with their start and end apart: 5 -> 18, of which waited for: 4 -> 11; matrix products, arithmetic and copies ran while one was open for 0% -> 0% of each run, Pallas kernels for 11% -> 13%
where the time goes in v3:
time: 160 us; the launch traced here: 159 us
  blocking collectives  68.4 us (43%)
  starting transfers between devices  32.2 us (20%)
  Pallas kernels  27.8 us (17%)
  waiting for transfers between devices  22.5 us (14%)
  local copies, waits for them, and re-layouts  7.89 us (5%)
    all_to_all x1, blocking collectives, exchange(): lax.all_to_all(x.reshape(experts, 8, m), 'ep', split_axis=0, concat_axis=...  68.4 us
    pallas_call x11, Pallas kernels, call(): pl.pallas_call(kernel, out_shape=[pltpu.HBM(shape, dtype) if out_spaces a...  27.8 us
    ppermute x13, starting transfers between devices, shift(): return lax.ppermute(v, 'ep', pairs)  19.1 us
    all_to_all x1, waiting for transfers between devices, exchange(): lax.all_to_all(x.reshape(experts, 8, m), 'ep', split_axis=0, concat_axis=...  12.4 us
    all_to_all x1, starting transfers between devices, exchange(): lax.all_to_all(x.reshape(experts, 8, m), 'ep', split_axis=0, concat_axis=...  12.3 us
    ppermute x13, waiting for transfers between devices, shift(): return lax.ppermute(v, 'ep', pairs)  9.6 us
    unnamed x28, local copies, waits for them, and re-layouts  7.89 us
  transfers between devices with their start and end apart: 18, of which 11 were waited for; matrix products, arithmetic and copies ran while one was open for 0% of the time, Pallas kernels for 13%

profile of v3, /device:TPU:32, one launch (start us, length us, event | category | flops | bytes accessed | tf_op | source)
XLA Modules:
  0.0 159.4 jit_solution(14681293508851380450)
XLA Ops:
  0.6 3.9 %shard_map.159 = (bf16[1024,1024]{1,0:T(8,128)(2,1)}, f32[128,128]{1,0:T(8,128)S(1)}) custom-call(s32[1]{0:T(128)} %bitcast.1.ep_ref, s32[1]{0:T(128)} %bitcast.tp_ref, s32[2,128]{1,0:T(2,128)} %bitcast.27, bf16[4,2048]{1,0:T(4,128)(2,1)} %bitcast.19, bf16[128,2048]{1,0:T(8,128)(2,1)} %tok_hbm.1, bf16[128,2048]{1,0:T(8,128)(2,1)} %cot_hbm.1, ...), custom_call_target="tpu_custom_call" | custom-call | flops 1073741824 | bytes 4194304 | tf_op jit(solution)/shard_map/pallas_call | solution.py:46
  4.5 68.4 %all_to_all.10 = bf16[128,8,1024]{2,1,0:T(8,128)(2,1)S(1)} all-to-all(bf16[128,8,1024]{2,1,0:T(8,128)(2,1)} %bitcast.22), channel_id=1, replica_groups=mesh['ep'=128,'tp'=2] {'ep'}, dimensions={0} | all-to-all | bytes 4194304 | tf_op jit(solution)/shard_map/all_to_all | solution.py:459
  72.9 5.3 %shard_map.160 = (f32[256,128]{1,0:T(8,128)S(1)}, bf16[256,1024]{1,0:T(8,128)(2,1)S(1)}, bf16[256,1152]{1,0:T(8,128)(2,1)S(1)}, bf16[256,2048]{1,0:T(8,128)(2,1)...) custom-call(s32[1]{0:T(128)} %bitcast.tp_ref, ...), custom_call_target="tpu_custom_call" | custom-call | flops 3221225472 | bytes 4194304 | tf_op jit(solution)/shard_map/pallas_call | solution.py:46
  78.1 0.6 collective-permute-start.2
  78.7 3.4 %shard_map.161 = (f32[256,128]{1,0:T(8,128)S(1)}, bf16[256,1024]{1,0:T(8,128)(2,1)S(1)}, bf16[256,1152]{1,0:T(8,128)(2,1)S(1)}, bf16[256,2048]{1,0:T(8,128)(2,1)...) custom-call(s32[1]{0:T(128)} %bitcast.tp_ref, ...), custom_call_target="tpu_custom_call" | custom-call | flops 3221225472 | bytes 4194304 | tf_op jit(solution)/shard_map/pallas_call | solution.py:46
  82.2 0.1 collective-permute-start.1
  82.3 0.6 shard_map.162
  82.9 0.8 collective-permute-start.3
  83.7 0.9 collective-permute-start.4
  84.5 1.9 %collective-permute-start.5 = (bf16[32,128]{1,0:T(8,128)(2,1)S(1)}, bf16[32,128]{1,0:T(8,128)(2,1)S(1)}, u32[]{:S(2)}, u32[]{:S(2)}) collective-permute-start(bf16[32,128]{1,0:T(8,128)(2,1)S(1)} %get-tuple-element.80), channel_id=1, source_target_pairs={{0,6},{2,0},{4,2},{6,4},{8,14},{10,8},{12,10},{14,12},{16,22},{18,... | collective-permute-start | bytes 24584 | tf_op jit(solution)/shard_map/ppermute | solution.py:471
  86.4 1.4 collective-permute-done.3.b_ref
  87.8 1.0 collective-permute-done.4.c_ref
  88.8 0.1 shard_map.163
  89.0 2.0 %collective-permute-start.7 = (bf16[32,128]{1,0:T(8,128)(2,1)S(1)}, bf16[32,128]{1,0:T(8,128)(2,1)S(1)}, u32[]{:S(2)}, u32[]{:S(2)}) collective-permute-start(bf16[32,128]{1,0:T(8,128)(2,1)S(1)} %get-tuple-element.83), channel_id=1, source_target_pairs={{0,16},{2,18},{4,20},{6,22},{8,24},{10,26},{12,28},{14,30},{16,0},... | collective-permute-start | bytes 24584 | tf_op jit(solution)/shard_map/ppermute | solution.py:471
  91.0 1.2 collective-permute-start.8
  92.2 1.6 %collective-permute-done.6.b_ref = bf16[32,128]{1,0:T(8,128)(2,1)S(1)} collective-permute-done((bf16[32,128]{1,0:T(8,128)(2,1)S(1)}, bf16[32,128]{1,0:T(8,128)(2,1)S(1)}, u32[]{:S(2)}, u32[]{:S(2)}) %collective-permute-start.6) | collective-permute-done | bytes 8224 | tf_op jit(solution)/shard_map/ppermute | solution.py:471
  93.8 0.4 collective-permute-done.7.c_ref
  94.2 0.6 collective-permute-done.8.d_ref
  94.8 0.2 shard_map.164
  95.0 1.3 collective-permute-start.10
  96.2 3.3 %collective-permute-start.11 = (bf16[16,128]{1,0:T(8,128)(2,1)S(1)}, bf16[16,128]{1,0:T(8,128)(2,1)S(1)}, u32[]{:S(2)}, u32[]{:S(2)}) collective-permute-start(bf16[16,128]{1,0:T(8,128)(2,1)S(1)} %get-tuple-element.88), channel_id=1, source_target_pairs={{0,96},{2,98},{4,100},{6,102},{8,104},{10,106},{12,108},{14,110},{... | collective-permute-start | bytes 12296 | tf_op jit(solution)/shard_map/ppermute | solution.py:471
  99.5 2.2 %collective-permute-start.12 = (bf16[16,128]{1,0:T(8,128)(2,1)S(1)}, bf16[16,128]{1,0:T(8,128)(2,1)S(1)}, u32[]{:S(2)}, u32[]{:S(2)}) collective-permute-start(bf16[16,128]{1,0:T(8,128)(2,1)S(1)} %get-tuple-element.89), channel_id=1, source_target_pairs={{0,128},{2,130},{4,132},{6,134},{8,136},{10,138},{12,140},{14,142}... | collective-permute-start | bytes 12296 | tf_op jit(solution)/shard_map/ppermute | solution.py:471
  101.7 3.1 %collective-permute-start.13 = (bf16[16,128]{1,0:T(8,128)(2,1)S(1)}, bf16[16,128]{1,0:T(8,128)(2,1)S(1)}, u32[]{:S(2)}, u32[]{:S(2)}) collective-permute-start(bf16[16,128]{1,0:T(8,128)(2,1)S(1)} %get-tuple-element.90), channel_id=1, source_target_pairs={{0,160},{2,162},{4,164},{6,166},{8,168},{10,170},{12,172},{14,174}... | collective-permute-start | bytes 12296 | tf_op jit(solution)/shard_map/ppermute | solution.py:471
  104.9 1.0 collective-permute-start.14
  105.9 1.2 collective-permute-done.12.refs_4_
  107.0 0.4 collective-permute-start.15
  107.5 0.9 collective-permute-done.13.refs_5_
  108.3 1.0 collective-permute-start.9
  109.3 0.0 collective-permute-done.14.refs_6_
  109.4 1.3 collective-permute-done.15.refs_7_
  110.6 1.3 collective-permute-done.9.refs_1_
  112.0 0.6 shard_map.165
  112.6 2.2 %shard_map.166 = bf16[1024,640]{1,0:T(8,128)(2,1)} custom-call(s32[1]{0:T(128)} %bitcast.tp_ref, bf16[256,1024]{1,0:T(8,128)(2,1)S(1)} %get-tuple-element.67.refs_0_, bf16[256,1024]{1,0:T(8,128)(2,1)S(1)} %get-tuple-element.71.refs_1_, bf16[256,1152]{1,0:T(8,128)(2,1)S(1)} %collective-permute-done.1.refs_2_, ...), custom_call_target="tpu_custom_call" | custom-call | flops 536870912 | bytes 4194304 | tf_op jit(solution)/shard_map/pallas_call | solution.py:46
  114.8 0.0 copy-start.4
  114.8 12.3 %all-to-all-start.1 = ((bf16[128,8,640]{2,1,0:T(8,128)(2,1)}), bf16[128,8,640]{2,1,0:T(8,128)(2,1)S(1)}, u32[]{:S(2)}, u32[]{:S(2)}) async-start(bf16[128,8,640]{2,1,0:T(8,128)(2,1)} %bitcast.21), calls=%async_computation.1 | async-start | bytes 2621440 | tf_op jit(solution)/shard_map/all_to_all | solution.py:459
  127.2 1.2 copy-done.6
  128.4 1.2 copy-done.7
  129.6 0.9 copy-done.8
  130.5 0.9 copy-done.9
  131.4 0.9 copy-done.10
  132.3 0.9 copy-done.11
  133.2 0.9 copy-done.12
  134.1 0.9 copy-done.13
  135.1 9.5 %shard_map.168 = (bf16[2048,256]{1,0:T(8,128)(2,1)}, bf16[2048,256]{1,0:T(8,128)(2,1)}, bf16[256,2048]{1,0:T(8,128)(2,1)}, f32[2,2048]{1,0:T(2,128)S(1)}, f32[1,256]{1,0:T(1,128)}) custom-call(bf16[256,2048]{1,0:T(8,128)(2,1)S(1)} %copy-done.4, bf16[256,2048]{1,0:T(8,128)(2,1)S(1)} %copy-done.6, bf16[256,2048]{1,0:T(8,128)(2,1)S(1)} %copy-done.5, ...), custom_call_target="tpu_custom_call" | custom-call | flops 3221225472 | bytes 4194304 | tf_op jit(solution)/shard_map/pallas_call | solution.py:46
  144.6 0.7 shard_map.167
  145.3 0.4 collective-permute-done.16.sqo_ref
  145.8 12.4 %all-to-all-done.1 = bf16[128,8,640]{2,1,0:T(8,128)(2,1)S(1)} async-done(((bf16[128,8,640]{2,1,0:T(8,128)(2,1)}), bf16[128,8,640]{2,1,0:T(8,128)(2,1)S(1)}, u32[]{:S(2)}, u32[]{:S(2)}) %all-to-all-start.1) | async-done | bytes 1310752 | tf_op jit(solution)/shard_map/all_to_all | solution.py:459
  158.2 1.3 shard_map.169
  (28 shorter events, 0.1 us)
Async XLA Ops:
  4.5 77.8 %copy-start.2 = (f32[128,128]{1,0:T(8,128)}, f32[128,128]{1,0:T(8,128)S(1)}, u32[]{:S(2)}) copy-start(f32[128,128]{1,0:T(8,128)S(1)} %get-tuple-element.76.aux_ref.raux_ref) | copy-start | bytes 196612
  72.9 5.9 %collective-permute-start = (bf16[1024,1024]{1,0:T(8,128)(2,1)S(1)}, bf16[1024,1024]{1,0:T(8,128)(2,1)S(1)}, u32[]{:S(2)}, u32[]{:S(2)}) collective-permute-start(bf16[1024,1024]{1,0:T(8,128)(2,1)S(1)} %bitcast.17), channel_id=1, source_target_pairs={{0,1},{1,0},{2,3},{3,2},{4,5},{5,4},{6,7},{7,6},{8,9},{9,8},{10,11... | collective-permute-start | bytes 6291464 | tf_op jit(solution)/shard_map/ppermute | solution.py:463
  78.1 34.5 %collective-permute-start.2 = (bf16[256,1152]{1,0:T(8,128)(2,1)S(1)}, bf16[256,1152]{1,0:T(8,128)(2,1)S(1)}, u32[]{:S(2)}, u32[]{:S(2)}) collective-permute-start(bf16[256,1152]{1,0:T(8,128)(2,1)S(1)} %get-tuple-element.73), channel_id=1, source_target_pairs={{0,1},{1,0},{2,3},{3,2},{4,5},{5,4},{6,7},{7,6},{8,9},{9,8},{10,11... | collective-permute-start | bytes 1769480 | tf_op jit(solution)/shard_map/ppermute | solution.py:463
  82.2 30.4 %collective-permute-start.1 = (bf16[256,1152]{1,0:T(8,128)(2,1)S(1)}, bf16[256,1152]{1,0:T(8,128)(2,1)S(1)}, u32[]{:S(2)}, u32[]{:S(2)}) collective-permute-start(bf16[256,1152]{1,0:T(8,128)(2,1)S(1)} %get-tuple-element.72), channel_id=1, source_target_pairs={{0,1},{1,0},{2,3},{3,2},{4,5},{5,4},{6,7},{7,6},{8,9},{9,8},{10,11... | collective-permute-start | bytes 1769480 | tf_op jit(solution)/shard_map/ppermute | solution.py:463
  82.9 4.9 %collective-permute-start.3 = (bf16[32,128]{1,0:T(8,128)(2,1)S(1)}, bf16[32,128]{1,0:T(8,128)(2,1)S(1)}, u32[]{:S(2)}, u32[]{:S(2)}) collective-permute-start(bf16[32,128]{1,0:T(8,128)(2,1)S(1)} %get-tuple-element.78), channel_id=1, source_target_pairs={{0,2},{2,4},{4,6},{6,0},{8,10},{10,12},{12,14},{14,8},{16,18},{18,... | collective-permute-start | bytes 24584 | tf_op jit(solution)/shard_map/ppermute | solution.py:471
  83.7 5.2 %collective-permute-start.4 = (bf16[32,128]{1,0:T(8,128)(2,1)S(1)}, bf16[32,128]{1,0:T(8,128)(2,1)S(1)}, u32[]{:S(2)}, u32[]{:S(2)}) collective-permute-start(bf16[32,128]{1,0:T(8,128)(2,1)S(1)} %get-tuple-element.79), channel_id=1, source_target_pairs={{0,4},{2,6},{4,0},{6,2},{8,12},{10,14},{12,8},{14,10},{16,20},{18,... | collective-permute-start | bytes 24584 | tf_op jit(solution)/shard_map/ppermute | solution.py:471
  84.5 4.3 %collective-permute-start.5 = (bf16[32,128]{1,0:T(8,128)(2,1)S(1)}, bf16[32,128]{1,0:T(8,128)(2,1)S(1)}, u32[]{:S(2)}, u32[]{:S(2)}) collective-permute-start(bf16[32,128]{1,0:T(8,128)(2,1)S(1)} %get-tuple-element.80), channel_id=1, source_target_pairs={{0,6},{2,0},{4,2},{6,4},{8,14},{10,8},{12,10},{14,12},{16,22},{18,... | collective-permute-start | bytes 24584 | tf_op jit(solution)/shard_map/ppermute | solution.py:471
  89.0 4.9 %collective-permute-start.6 = (bf16[32,128]{1,0:T(8,128)(2,1)S(1)}, bf16[32,128]{1,0:T(8,128)(2,1)S(1)}, u32[]{:S(2)}, u32[]{:S(2)}) collective-permute-start(bf16[32,128]{1,0:T(8,128)(2,1)S(1)} %get-tuple-element.82), channel_id=1, source_target_pairs={{0,8},{2,10},{4,12},{6,14},{8,16},{10,18},{12,20},{14,22},{16,24},... | collective-permute-start | bytes 24584 | tf_op jit(solution)/shard_map/ppermute | solution.py:471
  89.0 5.2 %collective-permute-start.7 = (bf16[32,128]{1,0:T(8,128)(2,1)S(1)}, bf16[32,128]{1,0:T(8,128)(2,1)S(1)}, u32[]{:S(2)}, u32[]{:S(2)}) collective-permute-start(bf16[32,128]{1,0:T(8,128)(2,1)S(1)} %get-tuple-element.83), channel_id=1, source_target_pairs={{0,16},{2,18},{4,20},{6,22},{8,24},{10,26},{12,28},{14,30},{16,0},... | collective-permute-start | bytes 24584 | tf_op jit(solution)/shard_map/ppermute | solution.py:471
  91.0 3.8 %collective-permute-start.8 = (bf16[32,128]{1,0:T(8,128)(2,1)S(1)}, bf16[32,128]{1,0:T(8,128)(2,1)S(1)}, u32[]{:S(2)}, u32[]{:S(2)}) collective-permute-start(bf16[32,128]{1,0:T(8,128)(2,1)S(1)} %get-tuple-element.84), channel_id=1, source_target_pairs={{0,24},{2,26},{4,28},{6,30},{8,0},{10,2},{12,4},{14,6},{16,8},{18,... | collective-permute-start | bytes 24584 | tf_op jit(solution)/shard_map/ppermute | solution.py:471
  95.0 6.8 %collective-permute-start.10 = (bf16[16,128]{1,0:T(8,128)(2,1)S(1)}, bf16[16,128]{1,0:T(8,128)(2,1)S(1)}, u32[]{:S(2)}, u32[]{:S(2)}) collective-permute-start(bf16[16,128]{1,0:T(8,128)(2,1)S(1)} %get-tuple-element.87), channel_id=1, source_target_pairs={{0,64},{2,66},{4,68},{6,70},{8,72},{10,74},{12,76},{14,78},{16,80}... | collective-permute-start | bytes 12296 | tf_op jit(solution)/shard_map/ppermute | solution.py:471
  96.2 8.6 %collective-permute-start.11 = (bf16[16,128]{1,0:T(8,128)(2,1)S(1)}, bf16[16,128]{1,0:T(8,128)(2,1)S(1)}, u32[]{:S(2)}, u32[]{:S(2)}) collective-permute-start(bf16[16,128]{1,0:T(8,128)(2,1)S(1)} %get-tuple-element.88), channel_id=1, source_target_pairs={{0,96},{2,98},{4,100},{6,102},{8,104},{10,106},{12,108},{14,110},{... | collective-permute-start | bytes 12296 | tf_op jit(solution)/shard_map/ppermute | solution.py:471
  99.5 7.5 %collective-permute-start.12 = (bf16[16,128]{1,0:T(8,128)(2,1)S(1)}, bf16[16,128]{1,0:T(8,128)(2,1)S(1)}, u32[]{:S(2)}, u32[]{:S(2)}) collective-permute-start(bf16[16,128]{1,0:T(8,128)(2,1)S(1)} %get-tuple-element.89), channel_id=1, source_target_pairs={{0,128},{2,130},{4,132},{6,134},{8,136},{10,138},{12,140},{14,142}... | collective-permute-start | bytes 12296 | tf_op jit(solution)/shard_map/ppermute | solution.py:471
  101.7 6.6 %collective-permute-start.13 = (bf16[16,128]{1,0:T(8,128)(2,1)S(1)}, bf16[16,128]{1,0:T(8,128)(2,1)S(1)}, u32[]{:S(2)}, u32[]{:S(2)}) collective-permute-start(bf16[16,128]{1,0:T(8,128)(2,1)S(1)} %get-tuple-element.90), channel_id=1, source_target_pairs={{0,160},{2,162},{4,164},{6,166},{8,168},{10,170},{12,172},{14,174}... | collective-permute-start | bytes 12296 | tf_op jit(solution)/shard_map/ppermute | solution.py:471
  104.9 4.5 %collective-permute-start.14 = (bf16[16,128]{1,0:T(8,128)(2,1)S(1)}, bf16[16,128]{1,0:T(8,128)(2,1)S(1)}, u32[]{:S(2)}, u32[]{:S(2)}) collective-permute-start(bf16[16,128]{1,0:T(8,128)(2,1)S(1)} %get-tuple-element.91), channel_id=1, source_target_pairs={{0,192},{2,194},{4,196},{6,198},{8,200},{10,202},{12,204},{14,206}... | collective-permute-start | bytes 12296 | tf_op jit(solution)/shard_map/ppermute | solution.py:471
  107.0 3.6 %collective-permute-start.15 = (bf16[16,128]{1,0:T(8,128)(2,1)S(1)}, bf16[16,128]{1,0:T(8,128)(2,1)S(1)}, u32[]{:S(2)}, u32[]{:S(2)}) collective-permute-start(bf16[16,128]{1,0:T(8,128)(2,1)S(1)} %get-tuple-element.92), channel_id=1, source_target_pairs={{0,224},{2,226},{4,228},{6,230},{8,232},{10,234},{12,236},{14,238}... | collective-permute-start | bytes 12296 | tf_op jit(solution)/shard_map/ppermute | solution.py:471
  108.3 3.6 %collective-permute-start.9 = (bf16[16,128]{1,0:T(8,128)(2,1)S(1)}, bf16[16,128]{1,0:T(8,128)(2,1)S(1)}, u32[]{:S(2)}, u32[]{:S(2)}) collective-permute-start(bf16[16,128]{1,0:T(8,128)(2,1)S(1)} %get-tuple-element.86), channel_id=1, source_target_pairs={{0,32},{2,34},{4,36},{6,38},{8,40},{10,42},{12,44},{14,46},{16,48}... | collective-permute-start | bytes 12296 | tf_op jit(solution)/shard_map/ppermute | solution.py:471
  114.8 12.3 %copy-start.4 = (bf16[256,2048]{1,0:T(8,128)(2,1)S(1)}, bf16[256,2048]{1,0:T(8,128)(2,1)}, u32[]{:S(2)}) copy-start(bf16[256,2048]{1,0:T(8,128)(2,1)} %get-tuple-element.101.refs_0_) | copy-start | bytes 3145732
  114.8 12.3 %copy-start.5 = (bf16[256,2048]{1,0:T(8,128)(2,1)S(1)}, bf16[256,2048]{1,0:T(8,128)(2,1)}, u32[]{:S(2)}) copy-start(bf16[256,2048]{1,0:T(8,128)(2,1)} %get-tuple-element.103.refs_2_) | copy-start | bytes 3145732
  114.8 43.3 %all-to-all-start.1 = ((bf16[128,8,640]{2,1,0:T(8,128)(2,1)}), bf16[128,8,640]{2,1,0:T(8,128)(2,1)S(1)}, u32[]{:S(2)}, u32[]{:S(2)}) async-start(bf16[128,8,640]{2,1,0:T(8,128)(2,1)} %bitcast.21), calls=%async_computation.1 | async-start | bytes 2621440 | tf_op jit(solution)/shard_map/all_to_all | solution.py:459
  127.2 1.2 copy-start.6
  128.4 1.2 copy-start.7
  129.6 0.9 copy-start.8
  130.5 0.9 copy-start.9
  131.4 0.9 copy-start.10
  132.3 0.9 copy-start.11
  133.2 0.9 copy-start.12
  134.1 0.9 copy-start.13
  135.0 9.6 %copy-start = (bf16[2048,128]{1,0:T(8,128)(2,1)S(1)}, bf16[2048,128]{1,0:T(8,128)(2,1)}, u32[]{:S(2)}) copy-start(bf16[2048,128]{1,0:T(8,128)(2,1)} %rex_ref.1) | copy-start | bytes 1572868
  135.0 9.6 %copy-start.1 = (bf16[2048,4]{0,1:T(4,128)(2,1)S(1)}, bf16[2048,4]{0,1:T(4,128)(2,1)}, u32[]{:S(2)}) copy-start(bf16[2048,4]{0,1:T(4,128)(2,1)} %param.11) | copy-start | bytes 49156
  135.1 9.6 %copy-start.3 = (f32[128,128]{1,0:T(8,128)S(1)}, f32[128,128]{1,0:T(8,128)}, u32[]{:S(2)}) copy-start(f32[128,128]{1,0:T(8,128)} %copy-done.2) | copy-start | bytes 196612
  144.6 1.2 collective-permute-start.16

commit v4 on v3

--- a/solution.py
+++ b/solution.py
@@ -155,6 +155,10 @@
         out_ref[...] = mm(ones_where(iota((n, n * stride), 1) == want), rows_in).astype(BF)
 
 
+def mark_kernel(aux_ref, out_ref):
+    out_ref[...] = jnp.transpose(aux_ref[...])
+
+
 def side_x_kernel(groups, ep_ref, aux_ref, *outs):
     tok = aux_ref.shape[1]
     experts = outs[0].shape[0] * 4
@@ -230,12 +234,13 @@
     weights, refs = refs[:3], refs[3:]
     u_ref, mine_ref, theirs_ref, x_ref, x_out, sc_out, gd_out, ud_out, hid_out = refs[:9]
     sc_ref, gd_ref, ud_ref, hid_ref, sems = refs[-5:]
-    gate_ref, up_ref, down_ref = refs[9:12] if load else weights
+    gate_ref = weights[0]
+    up_ref, down_ref = refs[9:11] if load else weights[1:]
     loads = []
     if load:
         loads = [
             pltpu.make_async_copy(src, dst, sems.at[5 + k])
-            for k, (src, dst) in enumerate(zip(weights, (gate_ref, up_ref, down_ref)))
+            for k, (src, dst) in enumerate(zip(weights[1:], (up_ref, down_ref)))
         ]
         for copy in loads:
             copy.start()
@@ -260,16 +265,12 @@
             ((x_ref, x_out), (sc_ref, sc_out), (gd_ref, gd_out), (ud_ref, ud_out), (hid_ref, hid_out))
         )
     ]
+    gp = mm(x_ref[...], gate_ref[...])
+    for copy in loads:
+        copy.wait()
     saves[0].start()
     saves[1].start()
-    if load:
-        loads[0].wait()
-    gp = mm(x_ref[...], gate_ref[...])
-    if load:
-        loads[1].wait()
     upre = mm(x_ref[...], up_ref[...])
-    if load:
-        loads[2].wait()
     pulled = nt(sc_ref[...], down_ref[...])
     sig = 1.0 / (1.0 + jnp.exp(-gp))
     act = gp * sig
@@ -366,9 +367,8 @@
     down_sq_ref[...] = jnp.transpose(acc_ref[...])[0:1, :]
 
 
-def home_kernel(tp_ref, raux_ref, rg_ref, rex_ref, sel_ref, q_ref, h_ref, aux_ref):
+def home_kernel(tp_ref, aux_ref, rg_ref, rex_ref, sel_ref, q_ref, h_ref):
     tp = tp_ref[0]
-    aux_ref[...] = jnp.transpose(raux_ref[...])
     tok = aux_ref.shape[0]
     half = q_ref.shape[1]
     groups = rg_ref.shape[0]
@@ -492,23 +492,24 @@
     sides = [shift(v, 4, d) if d else v for d, v in enumerate(sides)]
     sides = call(side_z_kernel, 1 << 24, 6, [((16, EXTRA), BF)] * planes, idx[:1], sides)
     sides = [shift(v, 16, d) if d else v for d, v in enumerate(sides)]
+    (aux_cols,) = call(mark_kernel, 1 << 20, 4, [((tok, EXTRA), F32)], [], [aux])
     z = call(functools.partial(side_end_kernel, groups), 1 << 24, 6, [((n, EXTRA), BF)] * 2, idx, sides)
     other = partner(got)
 
     def expert(g, weights, load):
-        held = [((dm, ff), BF), ((dm, ff), BF), ((ff, dm), BF)] if load else []
+        held = [((dm, ff), BF), ((ff, dm), BF)] if load else []
         return call(
             functools.partial(expert_kernel, load), 3 << 30, 18,
             [((n, EXTRA), F32), ((n, half), BF), ((n, half + EXTRA), BF), ((n, dm), BF),
              ((n, dm), BF), ((n, dm), BF), ((n, ff), BF), ((n, ff), BF), ((n, ff), BF)] + held,
             [tp], [g, *weights],
             scratch=[pltpu.VMEM((n, w), BF) for w in (dm, ff, ff, ff)] + [pltpu.SemaphoreType.DMA((8,))],
-            spaces=[VM] + [HB if load else VM] * 3,
+            spaces=[VM] * 2 + [HB if load else VM] * 2,
             out_spaces=[VM] * 4 + [HB] * 5 + [VM] * len(held),
         )
 
-    first = expert(got, [far(gate), far(up), far(down)], True)
-    second = expert(other, first[9:], False)
+    first = expert(got, [gate, far(up), far(down)], True)
+    second = expert(other, [gate, *first[9:]], False)
     u, mine, theirs, xv, x, sc, gd, ud, hid = [list(v) for v in zip(first[:9], second)]
     came = [partner(theirs[1]), partner(theirs[0])]
     (ret,) = call(
@@ -527,10 +528,10 @@
         [], [*x, *sc, *gd, *ud, *hid], scratch=[pltpu.VMEM((ff, 128), F32)],
     )
     sq_other = partner(sq)
-    sel, q, h, aux_cols = call(
+    sel, q, h = call(
         home_kernel, 1 << 29, 8,
-        [((4, tok, experts * 8), BF), ((tok, half), F32), ((tok, half), F32), ((tok, EXTRA), F32)],
-        [tp], [aux, rgt, router_expert],
+        [((4, tok, experts * 8), BF), ((tok, half), F32), ((tok, half), F32)],
+        [tp], [aux_cols, rgt, router_expert],
     )
     token_grad, rex_grad, rg_grad, rows, gate_sq, up_sq = call(
         final_kernel, 1 << 29, 10,

time: 160 us -> 159 us (level)
  local copies, waits for them, and re-layouts: 7.89 us -> 3.72 us
  waiting for transfers between devices: 22.5 us -> 26.6 us
    unnamed x28 -> x26, local copies, waits for them, and re-layouts: 7.89 us -> 3.72 us
    all_to_all x1, waiting for transfers between devices: 12.4 us -> 16.5 us  [exchange(): lax.all_to_all(x.reshape(experts, 8, m), 'ep', split_axis=0, concat_axis=...]
    pallas_call x11 -> x12, Pallas kernels: 27.8 us -> 26.4 us  [call(): pl.pallas_call(kernel, out_shape=[pltpu.HBM(shape, dtype) if out_spaces a...]
  transfers between devices with their start and end apart: 18 -> 18, of which waited for: 11 -> 11; matrix products, arithmetic and copies ran while one was open for 0% -> 0% of each run, Pallas kernels for 13% -> 12%
where the time goes in v4:
time: 159 us; the launch traced here: 158 us
  blocking collectives  68.5 us (43%)
  starting transfers between devices  32.1 us (20%)
  waiting for transfers between devices  26.6 us (17%)
  Pallas kernels  26.4 us (17%)
  local copies, waits for them, and re-layouts  3.72 us (2%)
    all_to_all x1, blocking collectives, exchange(): lax.all_to_all(x.reshape(experts, 8, m), 'ep', split_axis=0, concat_axis=...  68.5 us
    pallas_call x12, Pallas kernels, call(): pl.pallas_call(kernel, out_shape=[pltpu.HBM(shape, dtype) if out_spaces a...  26.4 us
    ppermute x13, starting transfers between devices, shift(): return lax.ppermute(v, 'ep', pairs)  19.1 us
    all_to_all x1, waiting for transfers between devices, exchange(): lax.all_to_all(x.reshape(experts, 8, m), 'ep', split_axis=0, concat_axis=...  16.5 us
    all_to_all x1, starting transfers between devices, exchange(): lax.all_to_all(x.reshape(experts, 8, m), 'ep', split_axis=0, concat_axis=...  12.3 us
    ppermute x13, waiting for transfers between devices, shift(): return lax.ppermute(v, 'ep', pairs)  9.61 us
    unnamed x26, local copies, waits for them, and re-layouts  3.72 us
  transfers between devices with their start and end apart: 18, of which 11 were waited for; matrix products, arithmetic and copies ran while one was open for 0% of the time, Pallas kernels for 12%

profile of v4, /device:TPU:32, one launch (start us, length us, event | category | flops | bytes accessed | tf_op | source)
XLA Modules:
  0.0 158.2 jit_solution(13537290187694434462)
XLA Ops:
  0.6 3.8 %shard_map.159 = (bf16[1024,1024]{1,0:T(8,128)(2,1)}, f32[128,128]{1,0:T(8,128)S(1)}) custom-call(s32[1]{0:T(128)} %bitcast.1.ep_ref, s32[1]{0:T(128)} %bitcast.tp_ref, s32[2,128]{1,0:T(2,128)} %bitcast.28, bf16[4,2048]{1,0:T(4,128)(2,1)} %bitcast.21, bf16[128,2048]{1,0:T(8,128)(2,1)} %tok_hbm.1, bf16[128,2048]{1,0:T(8,128)(2,1)} %cot_hbm.1, ...), custom_call_target="tpu_custom_call" | custom-call | flops 1073741824 | bytes 4194304 | tf_op jit(solution)/shard_map/pallas_call | solution.py:46
  4.5 0.0 copy-start
  4.5 68.5 %all_to_all.10 = bf16[128,8,1024]{2,1,0:T(8,128)(2,1)S(1)} all-to-all(bf16[128,8,1024]{2,1,0:T(8,128)(2,1)} %bitcast.24), channel_id=1, replica_groups=mesh['ep'=128,'tp'=2] {'ep'}, dimensions={0} | all-to-all | bytes 4194304 | tf_op jit(solution)/shard_map/all_to_all | solution.py:459
  73.0 3.9 %shard_map.160 = (f32[256,128]{1,0:T(8,128)S(1)}, bf16[256,1024]{1,0:T(8,128)(2,1)S(1)}, bf16[256,1152]{1,0:T(8,128)(2,1)S(1)}, bf16[256,2048]{1,0:T(8,128)(2,1)...) custom-call(s32[1]{0:T(128)} %bitcast.tp_ref, ...), custom_call_target="tpu_custom_call" | custom-call | flops 3221225472 | bytes 4194304 | tf_op jit(solution)/shard_map/pallas_call | solution.py:46
  76.9 0.6 collective-permute-start.2
  77.5 0.0 collective-permute-done.got_ref
  77.5 3.4 %shard_map.161 = (f32[256,128]{1,0:T(8,128)S(1)}, bf16[256,1024]{1,0:T(8,128)(2,1)S(1)}, bf16[256,1152]{1,0:T(8,128)(2,1)S(1)}, bf16[256,2048]{1,0:T(8,128)(2,1)...) custom-call(s32[1]{0:T(128)} %bitcast.tp_ref, ...), custom_call_target="tpu_custom_call" | custom-call | flops 3221225472 | bytes 4194304 | tf_op jit(solution)/shard_map/pallas_call | solution.py:46
  80.9 0.1 collective-permute-start.1
  81.0 0.6 shard_map.162
  81.6 0.8 collective-permute-start.3
  82.4 0.8 collective-permute-start.4
  83.3 1.9 %collective-permute-start.5 = (bf16[32,128]{1,0:T(8,128)(2,1)S(1)}, bf16[32,128]{1,0:T(8,128)(2,1)S(1)}, u32[]{:S(2)}, u32[]{:S(2)}) collective-permute-start(bf16[32,128]{1,0:T(8,128)(2,1)S(1)} %get-tuple-element.77), channel_id=1, source_target_pairs={{0,6},{2,0},{4,2},{6,4},{8,14},{10,8},{12,10},{14,12},{16,22},{18,... | collective-permute-start | bytes 24584 | tf_op jit(solution)/shard_map/ppermute | solution.py:471
  85.2 1.4 collective-permute-done.3.b_ref
  86.6 1.0 collective-permute-done.4.c_ref
  87.6 0.1 shard_map.163
  87.7 2.0 %collective-permute-start.7 = (bf16[32,128]{1,0:T(8,128)(2,1)S(1)}, bf16[32,128]{1,0:T(8,128)(2,1)S(1)}, u32[]{:S(2)}, u32[]{:S(2)}) collective-permute-start(bf16[32,128]{1,0:T(8,128)(2,1)S(1)} %get-tuple-element.80), channel_id=1, source_target_pairs={{0,16},{2,18},{4,20},{6,22},{8,24},{10,26},{12,28},{14,30},{16,0},... | collective-permute-start | bytes 24584 | tf_op jit(solution)/shard_map/ppermute | solution.py:471
  89.7 1.2 collective-permute-start.8
  91.0 1.6 %collective-permute-done.6.b_ref = bf16[32,128]{1,0:T(8,128)(2,1)S(1)} collective-permute-done((bf16[32,128]{1,0:T(8,128)(2,1)S(1)}, bf16[32,128]{1,0:T(8,128)(2,1)S(1)}, u32[]{:S(2)}, u32[]{:S(2)}) %collective-permute-start.6) | collective-permute-done | bytes 8224 | tf_op jit(solution)/shard_map/ppermute | solution.py:471
  92.6 0.4 collective-permute-done.7.c_ref
  93.0 0.6 collective-permute-done.8.d_ref
  93.5 0.2 shard_map.164
  93.7 1.3 collective-permute-start.10
  95.0 3.3 %collective-permute-start.11 = (bf16[16,128]{1,0:T(8,128)(2,1)S(1)}, bf16[16,128]{1,0:T(8,128)(2,1)S(1)}, u32[]{:S(2)}, u32[]{:S(2)}) collective-permute-start(bf16[16,128]{1,0:T(8,128)(2,1)S(1)} %get-tuple-element.85), channel_id=1, source_target_pairs={{0,96},{2,98},{4,100},{6,102},{8,104},{10,106},{12,108},{14,110},{... | collective-permute-start | bytes 12296 | tf_op jit(solution)/shard_map/ppermute | solution.py:471
  98.2 2.2 %collective-permute-start.12 = (bf16[16,128]{1,0:T(8,128)(2,1)S(1)}, bf16[16,128]{1,0:T(8,128)(2,1)S(1)}, u32[]{:S(2)}, u32[]{:S(2)}) collective-permute-start(bf16[16,128]{1,0:T(8,128)(2,1)S(1)} %get-tuple-element.86), channel_id=1, source_target_pairs={{0,128},{2,130},{4,132},{6,134},{8,136},{10,138},{12,140},{14,142}... | collective-permute-start | bytes 12296 | tf_op jit(solution)/shard_map/ppermute | solution.py:471
  100.5 3.1 %collective-permute-start.13 = (bf16[16,128]{1,0:T(8,128)(2,1)S(1)}, bf16[16,128]{1,0:T(8,128)(2,1)S(1)}, u32[]{:S(2)}, u32[]{:S(2)}) collective-permute-start(bf16[16,128]{1,0:T(8,128)(2,1)S(1)} %get-tuple-element.87), channel_id=1, source_target_pairs={{0,160},{2,162},{4,164},{6,166},{8,168},{10,170},{12,172},{14,174}... | collective-permute-start | bytes 12296 | tf_op jit(solution)/shard_map/ppermute | solution.py:471
  103.6 1.0 collective-permute-start.14
  104.6 1.2 collective-permute-done.12.refs_4_
  105.8 0.4 collective-permute-start.15
  106.2 0.9 collective-permute-done.13.refs_5_
  107.1 1.0 collective-permute-start.9
  108.1 0.0 collective-permute-done.14.refs_6_
  108.1 1.3 collective-permute-done.15.refs_7_
  109.4 1.3 collective-permute-done.9.refs_1_
  110.7 0.6 shard_map.165
  111.4 2.1 %shard_map.166 = bf16[1024,640]{1,0:T(8,128)(2,1)} custom-call(s32[1]{0:T(128)} %bitcast.tp_ref, bf16[256,1024]{1,0:T(8,128)(2,1)S(1)} %get-tuple-element.65.refs_0_, bf16[256,1024]{1,0:T(8,128)(2,1)S(1)} %get-tuple-element.68.refs_1_, bf16[256,1152]{1,0:T(8,128)(2,1)S(1)} %collective-permute-done.1.refs_2_, ...), custom_call_target="tpu_custom_call" | custom-call | flops 536870912 | bytes 4194304 | tf_op jit(solution)/shard_map/pallas_call | solution.py:46
  113.5 0.0 copy-start.3
  113.5 0.0 copy-start.7
  113.6 12.3 %all-to-all-start.1 = ((bf16[128,8,640]{2,1,0:T(8,128)(2,1)}), bf16[128,8,640]{2,1,0:T(8,128)(2,1)S(1)}, u32[]{:S(2)}, u32[]{:S(2)}) async-start(bf16[128,8,640]{2,1,0:T(8,128)(2,1)} %bitcast.23), calls=%async_computation.1 | async-start | bytes 2621440 | tf_op jit(solution)/shard_map/all_to_all | solution.py:459
  125.9 0.1 shard_map.167.aux_ref
  126.0 0.0 copy-start.4
  126.1 1.2 copy-done.4
  127.3 1.2 copy-done.5
  128.5 1.2 copy-done.6
  129.7 9.5 %shard_map.169 = (bf16[2048,256]{1,0:T(8,128)(2,1)}, bf16[2048,256]{1,0:T(8,128)(2,1)}, bf16[256,2048]{1,0:T(8,128)(2,1)}, f32[2,2048]{1,0:T(2,128)S(1)}, f32[1,256]{1,0:T(1,128)}) custom-call(bf16[256,2048]{1,0:T(8,128)(2,1)S(1)} %copy-done.3, bf16[256,2048]{1,0:T(8,128)(2,1)S(1)} %copy-done.5, bf16[256,2048]{1,0:T(8,128)(2,1)S(1)} %copy-done.4, ...), custom_call_target="tpu_custom_call" | custom-call | flops 3221225472 | bytes 4194304 | tf_op jit(solution)/shard_map/pallas_call | solution.py:46
  139.3 0.7 shard_map.168
  140.0 0.5 collective-permute-done.16.sqo_ref
  140.5 16.5 %all-to-all-done.1 = bf16[128,8,640]{2,1,0:T(8,128)(2,1)S(1)} async-done(((bf16[128,8,640]{2,1,0:T(8,128)(2,1)}), bf16[128,8,640]{2,1,0:T(8,128)(2,1)S(1)}, u32[]{:S(2)}, u32[]{:S(2)}) %all-to-all-start.1) | async-done | bytes 1310752 | tf_op jit(solution)/shard_map/all_to_all | solution.py:459
  156.9 1.3 shard_map.170
  (27 shorter events, 0.1 us)
Async XLA Ops:
  4.5 68.5 %copy-start = (bf16[1,2048,256]{2,1,0:T(8,128)(2,1)S(1)}, bf16[1,2048,256]{2,1,0:T(8,128)(2,1)}, u32[]{:S(2)}) copy-start(bf16[1,2048,256]{2,1,0:T(8,128)(2,1)} %param.13) | copy-start | bytes 3145732
  73.0 4.5 %collective-permute-start = (bf16[1024,1024]{1,0:T(8,128)(2,1)S(1)}, bf16[1024,1024]{1,0:T(8,128)(2,1)S(1)}, u32[]{:S(2)}, u32[]{:S(2)}) collective-permute-start(bf16[1024,1024]{1,0:T(8,128)(2,1)S(1)} %bitcast.17), channel_id=1, source_target_pairs={{0,1},{1,0},{2,3},{3,2},{4,5},{5,4},{6,7},{7,6},{8,9},{9,8},{10,11... | collective-permute-start | bytes 6291464 | tf_op jit(solution)/shard_map/ppermute | solution.py:463
  76.9 34.4 %collective-permute-start.2 = (bf16[256,1152]{1,0:T(8,128)(2,1)S(1)}, bf16[256,1152]{1,0:T(8,128)(2,1)S(1)}, u32[]{:S(2)}, u32[]{:S(2)}) collective-permute-start(bf16[256,1152]{1,0:T(8,128)(2,1)S(1)} %get-tuple-element.70), channel_id=1, source_target_pairs={{0,1},{1,0},{2,3},{3,2},{4,5},{5,4},{6,7},{7,6},{8,9},{9,8},{10,11... | collective-permute-start | bytes 1769480 | tf_op jit(solution)/shard_map/ppermute | solution.py:463
  80.9 30.4 %collective-permute-start.1 = (bf16[256,1152]{1,0:T(8,128)(2,1)S(1)}, bf16[256,1152]{1,0:T(8,128)(2,1)S(1)}, u32[]{:S(2)}, u32[]{:S(2)}) collective-permute-start(bf16[256,1152]{1,0:T(8,128)(2,1)S(1)} %get-tuple-element.69), channel_id=1, source_target_pairs={{0,1},{1,0},{2,3},{3,2},{4,5},{5,4},{6,7},{7,6},{8,9},{9,8},{10,11... | collective-permute-start | bytes 1769480 | tf_op jit(solution)/shard_map/ppermute | solution.py:463
  81.6 4.9 %collective-permute-start.3 = (bf16[32,128]{1,0:T(8,128)(2,1)S(1)}, bf16[32,128]{1,0:T(8,128)(2,1)S(1)}, u32[]{:S(2)}, u32[]{:S(2)}) collective-permute-start(bf16[32,128]{1,0:T(8,128)(2,1)S(1)} %get-tuple-element.75), channel_id=1, source_target_pairs={{0,2},{2,4},{4,6},{6,0},{8,10},{10,12},{12,14},{14,8},{16,18},{18,... | collective-permute-start | bytes 24584 | tf_op jit(solution)/shard_map/ppermute | solution.py:471
  82.4 5.2 %collective-permute-start.4 = (bf16[32,128]{1,0:T(8,128)(2,1)S(1)}, bf16[32,128]{1,0:T(8,128)(2,1)S(1)}, u32[]{:S(2)}, u32[]{:S(2)}) collective-permute-start(bf16[32,128]{1,0:T(8,128)(2,1)S(1)} %get-tuple-element.76), channel_id=1, source_target_pairs={{0,4},{2,6},{4,0},{6,2},{8,12},{10,14},{12,8},{14,10},{16,20},{18,... | collective-permute-start | bytes 24584 | tf_op jit(solution)/shard_map/ppermute | solution.py:471
  83.3 4.3 %collective-permute-start.5 = (bf16[32,128]{1,0:T(8,128)(2,1)S(1)}, bf16[32,128]{1,0:T(8,128)(2,1)S(1)}, u32[]{:S(2)}, u32[]{:S(2)}) collective-permute-start(bf16[32,128]{1,0:T(8,128)(2,1)S(1)} %get-tuple-element.77), channel_id=1, source_target_pairs={{0,6},{2,0},{4,2},{6,4},{8,14},{10,8},{12,10},{14,12},{16,22},{18,... | collective-permute-start | bytes 24584 | tf_op jit(solution)/shard_map/ppermute | solution.py:471
  87.7 4.9 %collective-permute-start.6 = (bf16[32,128]{1,0:T(8,128)(2,1)S(1)}, bf16[32,128]{1,0:T(8,128)(2,1)S(1)}, u32[]{:S(2)}, u32[]{:S(2)}) collective-permute-start(bf16[32,128]{1,0:T(8,128)(2,1)S(1)} %get-tuple-element.79), channel_id=1, source_target_pairs={{0,8},{2,10},{4,12},{6,14},{8,16},{10,18},{12,20},{14,22},{16,24},... | collective-permute-start | bytes 24584 | tf_op jit(solution)/shard_map/ppermute | solution.py:471
  87.7 5.2 %collective-permute-start.7 = (bf16[32,128]{1,0:T(8,128)(2,1)S(1)}, bf16[32,128]{1,0:T(8,128)(2,1)S(1)}, u32[]{:S(2)}, u32[]{:S(2)}) collective-permute-start(bf16[32,128]{1,0:T(8,128)(2,1)S(1)} %get-tuple-element.80), channel_id=1, source_target_pairs={{0,16},{2,18},{4,20},{6,22},{8,24},{10,26},{12,28},{14,30},{16,0},... | collective-permute-start | bytes 24584 | tf_op jit(solution)/shard_map/ppermute | solution.py:471
  89.7 3.8 %collective-permute-start.8 = (bf16[32,128]{1,0:T(8,128)(2,1)S(1)}, bf16[32,128]{1,0:T(8,128)(2,1)S(1)}, u32[]{:S(2)}, u32[]{:S(2)}) collective-permute-start(bf16[32,128]{1,0:T(8,128)(2,1)S(1)} %get-tuple-element.81), channel_id=1, source_target_pairs={{0,24},{2,26},{4,28},{6,30},{8,0},{10,2},{12,4},{14,6},{16,8},{18,... | collective-permute-start | bytes 24584 | tf_op jit(solution)/shard_map/ppermute | solution.py:471
  93.7 6.8 %collective-permute-start.10 = (bf16[16,128]{1,0:T(8,128)(2,1)S(1)}, bf16[16,128]{1,0:T(8,128)(2,1)S(1)}, u32[]{:S(2)}, u32[]{:S(2)}) collective-permute-start(bf16[16,128]{1,0:T(8,128)(2,1)S(1)} %get-tuple-element.84), channel_id=1, source_target_pairs={{0,64},{2,66},{4,68},{6,70},{8,72},{10,74},{12,76},{14,78},{16,80}... | collective-permute-start | bytes 12296 | tf_op jit(solution)/shard_map/ppermute | solution.py:471
  95.0 8.6 %collective-permute-start.11 = (bf16[16,128]{1,0:T(8,128)(2,1)S(1)}, bf16[16,128]{1,0:T(8,128)(2,1)S(1)}, u32[]{:S(2)}, u32[]{:S(2)}) collective-permute-start(bf16[16,128]{1,0:T(8,128)(2,1)S(1)} %get-tuple-element.85), channel_id=1, source_target_pairs={{0,96},{2,98},{4,100},{6,102},{8,104},{10,106},{12,108},{14,110},{... | collective-permute-start | bytes 12296 | tf_op jit(solution)/shard_map/ppermute | solution.py:471
  98.2 7.5 %collective-permute-start.12 = (bf16[16,128]{1,0:T(8,128)(2,1)S(1)}, bf16[16,128]{1,0:T(8,128)(2,1)S(1)}, u32[]{:S(2)}, u32[]{:S(2)}) collective-permute-start(bf16[16,128]{1,0:T(8,128)(2,1)S(1)} %get-tuple-element.86), channel_id=1, source_target_pairs={{0,128},{2,130},{4,132},{6,134},{8,136},{10,138},{12,140},{14,142}... | collective-permute-start | bytes 12296 | tf_op jit(solution)/shard_map/ppermute | solution.py:471
  100.5 6.6 %collective-permute-start.13 = (bf16[16,128]{1,0:T(8,128)(2,1)S(1)}, bf16[16,128]{1,0:T(8,128)(2,1)S(1)}, u32[]{:S(2)}, u32[]{:S(2)}) collective-permute-start(bf16[16,128]{1,0:T(8,128)(2,1)S(1)} %get-tuple-element.87), channel_id=1, source_target_pairs={{0,160},{2,162},{4,164},{6,166},{8,168},{10,170},{12,172},{14,174}... | collective-permute-start | bytes 12296 | tf_op jit(solution)/shard_map/ppermute | solution.py:471
  103.6 4.5 %collective-permute-start.14 = (bf16[16,128]{1,0:T(8,128)(2,1)S(1)}, bf16[16,128]{1,0:T(8,128)(2,1)S(1)}, u32[]{:S(2)}, u32[]{:S(2)}) collective-permute-start(bf16[16,128]{1,0:T(8,128)(2,1)S(1)} %get-tuple-element.88), channel_id=1, source_target_pairs={{0,192},{2,194},{4,196},{6,198},{8,200},{10,202},{12,204},{14,206}... | collective-permute-start | bytes 12296 | tf_op jit(solution)/shard_map/ppermute | solution.py:471
  105.8 3.6 %collective-permute-start.15 = (bf16[16,128]{1,0:T(8,128)(2,1)S(1)}, bf16[16,128]{1,0:T(8,128)(2,1)S(1)}, u32[]{:S(2)}, u32[]{:S(2)}) collective-permute-start(bf16[16,128]{1,0:T(8,128)(2,1)S(1)} %get-tuple-element.89), channel_id=1, source_target_pairs={{0,224},{2,226},{4,228},{6,230},{8,232},{10,234},{12,236},{14,238}... | collective-permute-start | bytes 12296 | tf_op jit(solution)/shard_map/ppermute | solution.py:471
  107.1 3.6 %collective-permute-start.9 = (bf16[16,128]{1,0:T(8,128)(2,1)S(1)}, bf16[16,128]{1,0:T(8,128)(2,1)S(1)}, u32[]{:S(2)}, u32[]{:S(2)}) collective-permute-start(bf16[16,128]{1,0:T(8,128)(2,1)S(1)} %get-tuple-element.83), channel_id=1, source_target_pairs={{0,32},{2,34},{4,36},{6,38},{8,40},{10,42},{12,44},{14,46},{16,48}... | collective-permute-start | bytes 12296 | tf_op jit(solution)/shard_map/ppermute | solution.py:471
  113.5 12.5 %copy-start.3 = (bf16[256,2048]{1,0:T(8,128)(2,1)S(1)}, bf16[256,2048]{1,0:T(8,128)(2,1)}, u32[]{:S(2)}) copy-start(bf16[256,2048]{1,0:T(8,128)(2,1)} %get-tuple-element.97.refs_0_) | copy-start | bytes 3145732
  113.5 12.5 %copy-start.7 = (bf16[256,256]{1,0:T(8,128)(2,1)S(1)}, bf16[256,256]{1,0:T(8,128)(2,1)}, u32[]{:S(2)}) copy-start(bf16[256,256]{1,0:T(8,128)(2,1)} %get-tuple-element.101.refs_4_) | copy-start | bytes 393220
  113.5 12.5 %copy-start.8 = (bf16[256,256]{1,0:T(8,128)(2,1)S(1)}, bf16[256,256]{1,0:T(8,128)(2,1)}, u32[]{:S(2)}) copy-start(bf16[256,256]{1,0:T(8,128)(2,1)} %get-tuple-element.103.refs_6_) | copy-start | bytes 393220
  113.5 12.5 %copy-start.9 = (bf16[256,256]{1,0:T(8,128)(2,1)S(1)}, bf16[256,256]{1,0:T(8,128)(2,1)}, u32[]{:S(2)}) copy-start(bf16[256,256]{1,0:T(8,128)(2,1)} %get-tuple-element.105.refs_8_) | copy-start | bytes 393220
  113.5 12.5 %copy-start.10 = (bf16[256,256]{1,0:T(8,128)(2,1)S(1)}, bf16[256,256]{1,0:T(8,128)(2,1)}, u32[]{:S(2)}) copy-start(bf16[256,256]{1,0:T(8,128)(2,1)} %get-tuple-element.102.refs_5_) | copy-start | bytes 393220
  113.6 12.5 %copy-start.11 = (bf16[256,256]{1,0:T(8,128)(2,1)S(1)}, bf16[256,256]{1,0:T(8,128)(2,1)}, u32[]{:S(2)}) copy-start(bf16[256,256]{1,0:T(8,128)(2,1)} %get-tuple-element.104.refs_7_) | copy-start | bytes 393220
  113.6 12.5 %copy-start.12 = (bf16[256,256]{1,0:T(8,128)(2,1)S(1)}, bf16[256,256]{1,0:T(8,128)(2,1)}, u32[]{:S(2)}) copy-start(bf16[256,256]{1,0:T(8,128)(2,1)} %get-tuple-element.106.refs_9_) | copy-start | bytes 393220
  113.6 43.3 %all-to-all-start.1 = ((bf16[128,8,640]{2,1,0:T(8,128)(2,1)}), bf16[128,8,640]{2,1,0:T(8,128)(2,1)S(1)}, u32[]{:S(2)}, u32[]{:S(2)}) async-start(bf16[128,8,640]{2,1,0:T(8,128)(2,1)} %bitcast.23), calls=%async_computation.1 | async-start | bytes 2621440 | tf_op jit(solution)/shard_map/all_to_all | solution.py:459
  126.0 1.2 copy-start.4
  127.3 1.2 copy-start.5
  128.5 1.2 copy-start.6
  129.7 9.5 %copy-start.1 = (bf16[2048,128]{1,0:T(8,128)(2,1)S(1)}, bf16[2048,128]{1,0:T(8,128)(2,1)}, u32[]{:S(2)}) copy-start(bf16[2048,128]{1,0:T(8,128)(2,1)} %rex_ref.1) | copy-start | bytes 1572868
  129.7 9.5 %copy-start.2 = (bf16[2048,4]{0,1:T(4,128)(2,1)S(1)}, bf16[2048,4]{0,1:T(4,128)(2,1)}, u32[]{:S(2)}) copy-start(bf16[2048,4]{0,1:T(4,128)(2,1)} %param.11) | copy-start | bytes 49156
  139.3 1.2 collective-permute-start.16

commit v5 on v4

--- a/solution.py
+++ b/solution.py
@@ -63,7 +63,7 @@
 
 def pre_kernel(
     ep_ref, tp_ref, rt_hbm, rgt_hbm, tok_hbm, cot_hbm, rex_hbm,
-    send_out, aux_ref, send_ref, rt_ref, rgt_ref, tok_ref, cot_ref, rex_ref, one_ref, sems,
+    send_out, aux_ref, send_ref, sel_ref, rt_ref, rgt_ref, tok_ref, cot_ref, rex_ref, one_ref, sems,
 ):
     tp = tp_ref[0]
     tok, dm = tok_ref.shape
@@ -114,7 +114,8 @@
     for b in range(blocks):
         rows = slice(b * blk, (b + 1) * blk)
         one = one_ref[0, rows, :].astype(F32) + one_ref[1, rows, :].astype(F32)
-        send_ref[rows, 0:width] = mm(spread(one), stack).astype(BF)
+        sel_ref[rows, :] = spread(one)
+        send_ref[rows, 0:width] = mm(sel_ref[rows, :], stack).astype(BF)
         save(2 * b, rows, slice(0, width))
     loads[2].wait()
     loads[3].wait()
@@ -142,7 +143,8 @@
     for b in range(blocks):
         rows = slice(b * blk, (b + 1) * blk)
         one0, one1 = one_ref[0, rows, :].astype(F32), one_ref[1, rows, :].astype(F32)
-        send_ref[rows, width : 2 * width] = mm(spread(one0 * w0 + one1 * w1), stack).astype(BF)
+        scale = jnp.sum(one0 * w0 + one1 * w1, axis=1, keepdims=True)
+        send_ref[rows, width : 2 * width] = (mm(sel_ref[rows, :], stack) * scale).astype(BF)
         save(2 * b + 1, rows, slice(width, 2 * width))
     for copy in saves:
         copy.wait()
@@ -265,12 +267,17 @@
             ((x_ref, x_out), (sc_ref, sc_out), (gd_ref, gd_out), (ud_ref, ud_out), (hid_ref, hid_out))
         )
     ]
+    if not load:
+        saves[0].start()
+        saves[1].start()
     gp = mm(x_ref[...], gate_ref[...])
-    for copy in loads:
-        copy.wait()
-    saves[0].start()
-    saves[1].start()
+    if load:
+        loads[0].wait()
     upre = mm(x_ref[...], up_ref[...])
+    if load:
+        loads[1].wait()
+        saves[0].start()
+        saves[1].start()
     pulled = nt(sc_ref[...], down_ref[...])
     sig = 1.0 / (1.0 + jnp.exp(-gp))
     act = gp * sig
@@ -296,18 +303,38 @@
         save.wait()
 
 
+def summed(u_ref, came_ref):
+    half = came_ref.shape[1] - EXTRA
+    return u_ref[...] + came_ref[:, half : half + 1].astype(F32) + came_ref[:, half + 1 : half + 2].astype(F32)
+
+
+def router_terms(tp, x_ref, y_ref, b, bs):
+    cols = slice(b * 16 * bs, (b + 1) * 16 * bs)
+    rc = tn(x_ref[:, cols], y_ref[...]).reshape(bs, 16, EXTRA)
+    return jnp.where(tp == 0, rc[:, 0:8, :], rc[:, 8:16, :]).reshape(bs * 8, EXTRA)
+
+
+def early_kernel(tp_ref, came_ref, u_ref, z_ref, x_ref, rc_ref, ul_ref, y_ref):
+    tp = tp_ref[0]
+    n = u_ref.shape[0]
+    u = summed(u_ref, came_ref)
+    y_ref[...] = (u * z_ref[...].astype(F32)).astype(BF)
+    ul_ref[...] = jnp.where(iota((n, EXTRA), 1) == U_LANE, u, 0.0).astype(BF)
+    bs = min(32, n // 2)
+    for b in range(n // (2 * bs)):
+        rc_ref[b * bs * 8 : (b + 1) * bs * 8, :] = router_terms(tp, x_ref, y_ref, b, bs)
+
+
 def pack_kernel(tp_ref, *refs):
     tp = tp_ref[0]
-    mine, came, us, zs, xs = refs[0:2], refs[2:4], refs[4:6], refs[6:8], refs[8:10]
-    ret_out, ret_ref, y0_ref, y1_ref, ul_ref, sems = refs[10:16]
+    mine, came = refs[0:2], refs[2:4]
+    u_ref, z_ref, x_ref, rc1_ref, ul1_ref, ret_out, ret_ref, y_ref, ul_ref, sems = refs[4:14]
     saves = []
     n, half = mine[0].shape
     width = half // 2
-    lane = iota((n, EXTRA), 1)
-    for p, y_ref in ((0, y0_ref), (1, y1_ref)):
-        u = us[p][...] + came[p][:, half : half + 1].astype(F32) + came[p][:, half + 1 : half + 2].astype(F32)
-        y_ref[...] = (u * zs[p][...].astype(F32)).astype(BF)
-        ul_ref[p * n : (p + 1) * n, :] = jnp.where(lane == U_LANE, u, 0.0).astype(BF)
+    u = summed(u_ref, came[0])
+    y_ref[...] = (u * z_ref[...].astype(F32)).astype(BF)
+    ul_ref[...] = jnp.where(iota((n, EXTRA), 1) == U_LANE, u, 0.0).astype(BF)
     blk = min(256, n * 4)
     bs = blk // 8
     o, i = iota((blk, blk), 0), iota((blk, blk), 1)
@@ -321,12 +348,9 @@
             [sums[0][:, 0:width], sums[1][:, 0:width], sums[0][:, width:], sums[1][:, width:]], axis=0
         )
         ret_ref[out, 0:width] = mm(perm, stack).astype(BF)
-        ulane = jnp.concatenate([ul_ref[rows, :], ul_ref[n + b * 2 * bs : n + (b + 1) * 2 * bs, :]], axis=0)
+        ulane = jnp.concatenate([ul_ref[rows, :], ul1_ref[rows, :]], axis=0)
         base = mm(perm[:, 0 : 4 * bs], ulane)
-        cols = slice(b * 16 * bs, (b + 1) * 16 * bs)
-        rc = tn(xs[0][:, cols], y0_ref[...]) + tn(xs[1][:, cols], y1_ref[...])
-        rc = rc.reshape(bs, 16, EXTRA)
-        rc = jnp.where(tp == 0, rc[:, 0:8, :], rc[:, 8:16, :]).reshape(blk, EXTRA)
+        rc = router_terms(tp, x_ref, y_ref, b, bs) + rc1_ref[out, :]
         high = rc.astype(BF).astype(F32)
         ret_ref[out, width:] = (base + jnp.where(wide, high, rc - high)).astype(BF)
         saves.append(pltpu.make_async_copy(ret_ref.at[out, :], ret_out.at[out, :], sems.at[b]))
@@ -475,7 +499,8 @@
         [((experts * 8, 2 * width), BF), ((EXTRA, tok), F32)],
         idx, [far(routes.T), far(rgt), far(tokens), far(cotangent), far(router_expert)],
         scratch=[
-            pltpu.VMEM((experts * 8, 2 * width), BF), pltpu.VMEM((2, tok), jnp.int32), pltpu.VMEM((groups, dm), BF),
+            pltpu.VMEM((experts * 8, 2 * width), BF), pltpu.VMEM((experts * 8, 4 * tok), BF),
+            pltpu.VMEM((2, tok), jnp.int32), pltpu.VMEM((groups, dm), BF),
             pltpu.VMEM((tok, dm), BF), pltpu.VMEM((tok, dm), BF), pltpu.VMEM((dm, experts), BF),
             pltpu.VMEM((2, experts * 8, tok), BF), pltpu.SemaphoreType.DMA((13,)),
         ],
@@ -512,12 +537,16 @@
     second = expert(other, [gate, *first[9:]], False)
     u, mine, theirs, xv, x, sc, gd, ud, hid = [list(v) for v in zip(first[:9], second)]
     came = [partner(theirs[1]), partner(theirs[0])]
+    rc1, ul1 = call(
+        early_kernel, 1 << 28, 8, [((experts * 8, EXTRA), F32), ((n, EXTRA), BF)],
+        [tp], [came[1], u[1], z[1], xv[1]], scratch=[pltpu.VMEM((n, EXTRA), BF)],
+    )
     (ret,) = call(
         pack_kernel, 1 << 29, 16, [((experts * 8, width + EXTRA), BF)],
-        [tp], [*mine, *came, *u, *z, *xv],
+        [tp], [*mine, *came, u[0], z[0], xv[0], rc1, ul1],
         scratch=[
             pltpu.VMEM((experts * 8, width + EXTRA), BF), pltpu.VMEM((n, EXTRA), BF), pltpu.VMEM((n, EXTRA), BF),
-            pltpu.VMEM((2 * n, EXTRA), BF), pltpu.SemaphoreType.DMA((4,)),
+            pltpu.SemaphoreType.DMA((4,)),
         ],
         out_spaces=[HB],
     )

time: 159 us -> 159 us (level)
    pallas_call x12 -> x13, Pallas kernels: 26.4 us -> 27 us  [call(): pl.pallas_call(kernel, out_shape=[pltpu.HBM(shape, dtype) if out_spaces a...]
  transfers between devices with their start and end apart: 18 -> 18, of which waited for: 11 -> 11; matrix products, arithmetic and copies ran while one was open for 0% -> 0% of each run, Pallas kernels for 12% -> 13%
where the time goes in v5:
time: 159 us
  blocking collectives  68.5 us (43%)
  starting transfers between devices  32.2 us (20%)
  Pallas kernels  27 us (17%)
  waiting for transfers between devices  26.5 us (17%)
  local copies, waits for them, and re-layouts  3.72 us (2%)
    all_to_all x1, blocking collectives, exchange(): lax.all_to_all(x.reshape(experts, 8, m), 'ep', split_axis=0, concat_axis=...  68.5 us
    pallas_call x13, Pallas kernels, call(): pl.pallas_call(kernel, out_shape=[pltpu.HBM(shape, dtype) if out_spaces a...  27 us
    ppermute x13, starting transfers between devices, shift(): return lax.ppermute(v, 'ep', pairs)  19.2 us
    all_to_all x1, waiting for transfers between devices, exchange(): lax.all_to_all(x.reshape(experts, 8, m), 'ep', split_axis=0, concat_axis=...  16.5 us
    all_to_all x1, starting transfers between devices, exchange(): lax.all_to_all(x.reshape(experts, 8, m), 'ep', split_axis=0, concat_axis=...  12.3 us
    ppermute x13, waiting for transfers between devices, shift(): return lax.ppermute(v, 'ep', pairs)  9.58 us
    unnamed x26, local copies, waits for them, and re-layouts  3.72 us
  transfers between devices with their start and end apart: 18, of which 11 were waited for; matrix products, arithmetic and copies ran while one was open for 0% of the time, Pallas kernels for 13%

profile of v5, /device:TPU:32, one launch (start us, length us, event | category | flops | bytes accessed | tf_op | source)
XLA Modules:
  0.0 158.8 jit_solution(16950374801420548669)
XLA Ops:
  0.6 3.9 %shard_map.159 = (bf16[1024,1024]{1,0:T(8,128)(2,1)}, f32[128,128]{1,0:T(8,128)S(1)}) custom-call(s32[1]{0:T(128)} %bitcast.1.ep_ref, s32[1]{0:T(128)} %bitcast.tp_ref, s32[2,128]{1,0:T(2,128)} %bitcast.28, bf16[4,2048]{1,0:T(4,128)(2,1)} %bitcast.21, bf16[128,2048]{1,0:T(8,128)(2,1)} %tok_hbm.1, bf16[128,2048]{1,0:T(8,128)(2,1)} %cot_hbm.1, ...), custom_call_target="tpu_custom_call" | custom-call | flops 1073741824 | bytes 4194304 | tf_op jit(solution)/shard_map/pallas_call | solution.py:46
  4.5 0.0 copy-start
  4.5 68.5 %all_to_all.10 = bf16[128,8,1024]{2,1,0:T(8,128)(2,1)S(1)} all-to-all(bf16[128,8,1024]{2,1,0:T(8,128)(2,1)} %bitcast.24), channel_id=1, replica_groups=mesh['ep'=128,'tp'=2] {'ep'}, dimensions={0} | all-to-all | bytes 4194304 | tf_op jit(solution)/shard_map/all_to_all | solution.py:483
  73.0 4.3 %shard_map.160 = (f32[256,128]{1,0:T(8,128)S(1)}, bf16[256,1024]{1,0:T(8,128)(2,1)S(1)}, bf16[256,1152]{1,0:T(8,128)(2,1)S(1)}, bf16[256,2048]{1,0:T(8,128)(2,1)...) custom-call(s32[1]{0:T(128)} %bitcast.tp_ref, ...), custom_call_target="tpu_custom_call" | custom-call | flops 3221225472 | bytes 4194304 | tf_op jit(solution)/shard_map/pallas_call | solution.py:46
  77.4 0.6 collective-permute-start.2
  77.9 3.4 %shard_map.161 = (f32[256,128]{1,0:T(8,128)S(1)}, bf16[256,1024]{1,0:T(8,128)(2,1)S(1)}, bf16[256,1152]{1,0:T(8,128)(2,1)S(1)}, bf16[256,2048]{1,0:T(8,128)(2,1)...) custom-call(s32[1]{0:T(128)} %bitcast.tp_ref, ...), custom_call_target="tpu_custom_call" | custom-call | flops 3221225472 | bytes 4194304 | tf_op jit(solution)/shard_map/pallas_call | solution.py:46
  81.4 0.1 collective-permute-start.1
  81.5 0.6 shard_map.162
  82.1 0.8 collective-permute-start.3
  82.9 0.9 collective-permute-start.4
  83.7 1.9 %collective-permute-start.5 = (bf16[32,128]{1,0:T(8,128)(2,1)S(1)}, bf16[32,128]{1,0:T(8,128)(2,1)S(1)}, u32[]{:S(2)}, u32[]{:S(2)}) collective-permute-start(bf16[32,128]{1,0:T(8,128)(2,1)S(1)} %get-tuple-element.78), channel_id=1, source_target_pairs={{0,6},{2,0},{4,2},{6,4},{8,14},{10,8},{12,10},{14,12},{16,22},{18,... | collective-permute-start | bytes 24584 | tf_op jit(solution)/shard_map/ppermute | solution.py:495
  85.6 1.4 collective-permute-done.3.b_ref
  87.0 1.0 collective-permute-done.4.c_ref
  88.0 0.1 shard_map.163
  88.2 2.0 %collective-permute-start.7 = (bf16[32,128]{1,0:T(8,128)(2,1)S(1)}, bf16[32,128]{1,0:T(8,128)(2,1)S(1)}, u32[]{:S(2)}, u32[]{:S(2)}) collective-permute-start(bf16[32,128]{1,0:T(8,128)(2,1)S(1)} %get-tuple-element.81), channel_id=1, source_target_pairs={{0,16},{2,18},{4,20},{6,22},{8,24},{10,26},{12,28},{14,30},{16,0},... | collective-permute-start | bytes 24584 | tf_op jit(solution)/shard_map/ppermute | solution.py:495
  90.2 1.2 collective-permute-start.8
  91.4 1.6 %collective-permute-done.6.b_ref = bf16[32,128]{1,0:T(8,128)(2,1)S(1)} collective-permute-done((bf16[32,128]{1,0:T(8,128)(2,1)S(1)}, bf16[32,128]{1,0:T(8,128)(2,1)S(1)}, u32[]{:S(2)}, u32[]{:S(2)}) %collective-permute-start.6) | collective-permute-done | bytes 8224 | tf_op jit(solution)/shard_map/ppermute | solution.py:495
  93.0 0.4 collective-permute-done.7.c_ref
  93.4 0.6 collective-permute-done.8.d_ref
  94.0 0.2 shard_map.164
  94.1 1.3 collective-permute-start.10
  95.4 3.3 %collective-permute-start.11 = (bf16[16,128]{1,0:T(8,128)(2,1)S(1)}, bf16[16,128]{1,0:T(8,128)(2,1)S(1)}, u32[]{:S(2)}, u32[]{:S(2)}) collective-permute-start(bf16[16,128]{1,0:T(8,128)(2,1)S(1)} %get-tuple-element.86), channel_id=1, source_target_pairs={{0,96},{2,98},{4,100},{6,102},{8,104},{10,106},{12,108},{14,110},{... | collective-permute-start | bytes 12296 | tf_op jit(solution)/shard_map/ppermute | solution.py:495
  98.7 2.2 %collective-permute-start.12 = (bf16[16,128]{1,0:T(8,128)(2,1)S(1)}, bf16[16,128]{1,0:T(8,128)(2,1)S(1)}, u32[]{:S(2)}, u32[]{:S(2)}) collective-permute-start(bf16[16,128]{1,0:T(8,128)(2,1)S(1)} %get-tuple-element.87), channel_id=1, source_target_pairs={{0,128},{2,130},{4,132},{6,134},{8,136},{10,138},{12,140},{14,142}... | collective-permute-start | bytes 12296 | tf_op jit(solution)/shard_map/ppermute | solution.py:495
  100.9 3.1 %collective-permute-start.13 = (bf16[16,128]{1,0:T(8,128)(2,1)S(1)}, bf16[16,128]{1,0:T(8,128)(2,1)S(1)}, u32[]{:S(2)}, u32[]{:S(2)}) collective-permute-start(bf16[16,128]{1,0:T(8,128)(2,1)S(1)} %get-tuple-element.88), channel_id=1, source_target_pairs={{0,160},{2,162},{4,164},{6,166},{8,168},{10,170},{12,172},{14,174}... | collective-permute-start | bytes 12296 | tf_op jit(solution)/shard_map/ppermute | solution.py:495
  104.1 1.0 collective-permute-start.14
  105.1 1.2 collective-permute-done.12.refs_4_
  106.2 0.5 collective-permute-start.15
  106.7 0.9 collective-permute-done.13.refs_5_
  107.5 1.0 collective-permute-start.9
  108.6 0.0 collective-permute-done.14.refs_6_
  108.6 1.3 collective-permute-done.15.refs_7_
  109.8 1.3 collective-permute-done.9.refs_1_
  111.2 0.6 shard_map.165
  111.8 0.6 shard_map.166
  112.4 1.7 %shard_map.167 = bf16[1024,640]{1,0:T(8,128)(2,1)} custom-call(s32[1]{0:T(128)} %bitcast.tp_ref, bf16[256,1024]{1,0:T(8,128)(2,1)S(1)} %get-tuple-element.67.refs_0_, bf16[256,1024]{1,0:T(8,128)(2,1)S(1)} %get-tuple-element.70.refs_1_, bf16[256,1152]{1,0:T(8,128)(2,1)S(1)} %collective-permute-done.1.refs_2_, ...), custom_call_target="tpu_custom_call" | custom-call | flops 536870912 | bytes 4194304 | tf_op jit(solution)/shard_map/pallas_call | solution.py:46
  114.1 0.0 copy-start.3
  114.1 0.0 copy-start.7
  114.2 12.3 %all-to-all-start.1 = ((bf16[128,8,640]{2,1,0:T(8,128)(2,1)}), bf16[128,8,640]{2,1,0:T(8,128)(2,1)S(1)}, u32[]{:S(2)}, u32[]{:S(2)}) async-start(bf16[128,8,640]{2,1,0:T(8,128)(2,1)} %bitcast.23), calls=%async_computation.1 | async-start | bytes 2621440 | tf_op jit(solution)/shard_map/all_to_all | solution.py:483
  126.5 0.1 shard_map.168.aux_ref
  126.7 0.0 copy-start.4
  126.7 1.2 copy-done.4
  127.9 1.2 copy-done.5
  129.2 1.2 copy-done.6
  130.4 9.5 %shard_map.170 = (bf16[2048,256]{1,0:T(8,128)(2,1)}, bf16[2048,256]{1,0:T(8,128)(2,1)}, bf16[256,2048]{1,0:T(8,128)(2,1)}, f32[2,2048]{1,0:T(2,128)S(1)}, f32[1,256]{1,0:T(1,128)}) custom-call(bf16[256,2048]{1,0:T(8,128)(2,1)S(1)} %copy-done.3, bf16[256,2048]{1,0:T(8,128)(2,1)S(1)} %copy-done.5, bf16[256,2048]{1,0:T(8,128)(2,1)S(1)} %copy-done.4, ...), custom_call_target="tpu_custom_call" | custom-call | flops 3221225472 | bytes 4194304 | tf_op jit(solution)/shard_map/pallas_call | solution.py:46
  139.9 0.7 shard_map.169
  140.6 0.5 collective-permute-done.16.sqo_ref
  141.1 16.5 %all-to-all-done.1 = bf16[128,8,640]{2,1,0:T(8,128)(2,1)S(1)} async-done(((bf16[128,8,640]{2,1,0:T(8,128)(2,1)}), bf16[128,8,640]{2,1,0:T(8,128)(2,1)S(1)}, u32[]{:S(2)}, u32[]{:S(2)}) %all-to-all-start.1) | async-done | bytes 1310752 | tf_op jit(solution)/shard_map/all_to_all | solution.py:483
  157.6 1.3 shard_map.171
  (28 shorter events, 0.1 us)
Async XLA Ops:
  4.5 68.5 %copy-start = (bf16[1,2048,256]{2,1,0:T(8,128)(2,1)S(1)}, bf16[1,2048,256]{2,1,0:T(8,128)(2,1)}, u32[]{:S(2)}) copy-start(bf16[1,2048,256]{2,1,0:T(8,128)(2,1)} %param.13) | copy-start | bytes 3145732
  73.0 4.9 %collective-permute-start = (bf16[1024,1024]{1,0:T(8,128)(2,1)S(1)}, bf16[1024,1024]{1,0:T(8,128)(2,1)S(1)}, u32[]{:S(2)}, u32[]{:S(2)}) collective-permute-start(bf16[1024,1024]{1,0:T(8,128)(2,1)S(1)} %bitcast.17), channel_id=1, source_target_pairs={{0,1},{1,0},{2,3},{3,2},{4,5},{5,4},{6,7},{7,6},{8,9},{9,8},{10,11... | collective-permute-start | bytes 6291464 | tf_op jit(solution)/shard_map/ppermute | solution.py:487
  77.4 34.4 %collective-permute-start.2 = (bf16[256,1152]{1,0:T(8,128)(2,1)S(1)}, bf16[256,1152]{1,0:T(8,128)(2,1)S(1)}, u32[]{:S(2)}, u32[]{:S(2)}) collective-permute-start(bf16[256,1152]{1,0:T(8,128)(2,1)S(1)} %get-tuple-element.72), channel_id=1, source_target_pairs={{0,1},{1,0},{2,3},{3,2},{4,5},{5,4},{6,7},{7,6},{8,9},{9,8},{10,11... | collective-permute-start | bytes 1769480 | tf_op jit(solution)/shard_map/ppermute | solution.py:487
  81.4 31.0 %collective-permute-start.1 = (bf16[256,1152]{1,0:T(8,128)(2,1)S(1)}, bf16[256,1152]{1,0:T(8,128)(2,1)S(1)}, u32[]{:S(2)}, u32[]{:S(2)}) collective-permute-start(bf16[256,1152]{1,0:T(8,128)(2,1)S(1)} %get-tuple-element.71), channel_id=1, source_target_pairs={{0,1},{1,0},{2,3},{3,2},{4,5},{5,4},{6,7},{7,6},{8,9},{9,8},{10,11... | collective-permute-start | bytes 1769480 | tf_op jit(solution)/shard_map/ppermute | solution.py:487
  82.1 4.9 %collective-permute-start.3 = (bf16[32,128]{1,0:T(8,128)(2,1)S(1)}, bf16[32,128]{1,0:T(8,128)(2,1)S(1)}, u32[]{:S(2)}, u32[]{:S(2)}) collective-permute-start(bf16[32,128]{1,0:T(8,128)(2,1)S(1)} %get-tuple-element.76), channel_id=1, source_target_pairs={{0,2},{2,4},{4,6},{6,0},{8,10},{10,12},{12,14},{14,8},{16,18},{18,... | collective-permute-start | bytes 24584 | tf_op jit(solution)/shard_map/ppermute | solution.py:495
  82.9 5.2 %collective-permute-start.4 = (bf16[32,128]{1,0:T(8,128)(2,1)S(1)}, bf16[32,128]{1,0:T(8,128)(2,1)S(1)}, u32[]{:S(2)}, u32[]{:S(2)}) collective-permute-start(bf16[32,128]{1,0:T(8,128)(2,1)S(1)} %get-tuple-element.77), channel_id=1, source_target_pairs={{0,4},{2,6},{4,0},{6,2},{8,12},{10,14},{12,8},{14,10},{16,20},{18,... | collective-permute-start | bytes 24584 | tf_op jit(solution)/shard_map/ppermute | solution.py:495
  83.7 4.3 %collective-permute-start.5 = (bf16[32,128]{1,0:T(8,128)(2,1)S(1)}, bf16[32,128]{1,0:T(8,128)(2,1)S(1)}, u32[]{:S(2)}, u32[]{:S(2)}) collective-permute-start(bf16[32,128]{1,0:T(8,128)(2,1)S(1)} %get-tuple-element.78), channel_id=1, source_target_pairs={{0,6},{2,0},{4,2},{6,4},{8,14},{10,8},{12,10},{14,12},{16,22},{18,... | collective-permute-start | bytes 24584 | tf_op jit(solution)/shard_map/ppermute | solution.py:495
  88.2 4.9 %collective-permute-start.6 = (bf16[32,128]{1,0:T(8,128)(2,1)S(1)}, bf16[32,128]{1,0:T(8,128)(2,1)S(1)}, u32[]{:S(2)}, u32[]{:S(2)}) collective-permute-start(bf16[32,128]{1,0:T(8,128)(2,1)S(1)} %get-tuple-element.80), channel_id=1, source_target_pairs={{0,8},{2,10},{4,12},{6,14},{8,16},{10,18},{12,20},{14,22},{16,24},... | collective-permute-start | bytes 24584 | tf_op jit(solution)/shard_map/ppermute | solution.py:495
  88.2 5.2 %collective-permute-start.7 = (bf16[32,128]{1,0:T(8,128)(2,1)S(1)}, bf16[32,128]{1,0:T(8,128)(2,1)S(1)}, u32[]{:S(2)}, u32[]{:S(2)}) collective-permute-start(bf16[32,128]{1,0:T(8,128)(2,1)S(1)} %get-tuple-element.81), channel_id=1, source_target_pairs={{0,16},{2,18},{4,20},{6,22},{8,24},{10,26},{12,28},{14,30},{16,0},... | collective-permute-start | bytes 24584 | tf_op jit(solution)/shard_map/ppermute | solution.py:495
  90.2 3.8 %collective-permute-start.8 = (bf16[32,128]{1,0:T(8,128)(2,1)S(1)}, bf16[32,128]{1,0:T(8,128)(2,1)S(1)}, u32[]{:S(2)}, u32[]{:S(2)}) collective-permute-start(bf16[32,128]{1,0:T(8,128)(2,1)S(1)} %get-tuple-element.82), channel_id=1, source_target_pairs={{0,24},{2,26},{4,28},{6,30},{8,0},{10,2},{12,4},{14,6},{16,8},{18,... | collective-permute-start | bytes 24584 | tf_op jit(solution)/shard_map/ppermute | solution.py:495
  94.1 6.8 %collective-permute-start.10 = (bf16[16,128]{1,0:T(8,128)(2,1)S(1)}, bf16[16,128]{1,0:T(8,128)(2,1)S(1)}, u32[]{:S(2)}, u32[]{:S(2)}) collective-permute-start(bf16[16,128]{1,0:T(8,128)(2,1)S(1)} %get-tuple-element.85), channel_id=1, source_target_pairs={{0,64},{2,66},{4,68},{6,70},{8,72},{10,74},{12,76},{14,78},{16,80}... | collective-permute-start | bytes 12296 | tf_op jit(solution)/shard_map/ppermute | solution.py:495
  95.4 8.6 %collective-permute-start.11 = (bf16[16,128]{1,0:T(8,128)(2,1)S(1)}, bf16[16,128]{1,0:T(8,128)(2,1)S(1)}, u32[]{:S(2)}, u32[]{:S(2)}) collective-permute-start(bf16[16,128]{1,0:T(8,128)(2,1)S(1)} %get-tuple-element.86), channel_id=1, source_target_pairs={{0,96},{2,98},{4,100},{6,102},{8,104},{10,106},{12,108},{14,110},{... | collective-permute-start | bytes 12296 | tf_op jit(solution)/shard_map/ppermute | solution.py:495
  98.7 7.5 %collective-permute-start.12 = (bf16[16,128]{1,0:T(8,128)(2,1)S(1)}, bf16[16,128]{1,0:T(8,128)(2,1)S(1)}, u32[]{:S(2)}, u32[]{:S(2)}) collective-permute-start(bf16[16,128]{1,0:T(8,128)(2,1)S(1)} %get-tuple-element.87), channel_id=1, source_target_pairs={{0,128},{2,130},{4,132},{6,134},{8,136},{10,138},{12,140},{14,142}... | collective-permute-start | bytes 12296 | tf_op jit(solution)/shard_map/ppermute | solution.py:495
  100.9 6.6 %collective-permute-start.13 = (bf16[16,128]{1,0:T(8,128)(2,1)S(1)}, bf16[16,128]{1,0:T(8,128)(2,1)S(1)}, u32[]{:S(2)}, u32[]{:S(2)}) collective-permute-start(bf16[16,128]{1,0:T(8,128)(2,1)S(1)} %get-tuple-element.88), channel_id=1, source_target_pairs={{0,160},{2,162},{4,164},{6,166},{8,168},{10,170},{12,172},{14,174}... | collective-permute-start | bytes 12296 | tf_op jit(solution)/shard_map/ppermute | solution.py:495
  104.1 4.5 %collective-permute-start.14 = (bf16[16,128]{1,0:T(8,128)(2,1)S(1)}, bf16[16,128]{1,0:T(8,128)(2,1)S(1)}, u32[]{:S(2)}, u32[]{:S(2)}) collective-permute-start(bf16[16,128]{1,0:T(8,128)(2,1)S(1)} %get-tuple-element.89), channel_id=1, source_target_pairs={{0,192},{2,194},{4,196},{6,198},{8,200},{10,202},{12,204},{14,206}... | collective-permute-start | bytes 12296 | tf_op jit(solution)/shard_map/ppermute | solution.py:495
  106.2 3.6 %collective-permute-start.15 = (bf16[16,128]{1,0:T(8,128)(2,1)S(1)}, bf16[16,128]{1,0:T(8,128)(2,1)S(1)}, u32[]{:S(2)}, u32[]{:S(2)}) collective-permute-start(bf16[16,128]{1,0:T(8,128)(2,1)S(1)} %get-tuple-element.90), channel_id=1, source_target_pairs={{0,224},{2,226},{4,228},{6,230},{8,232},{10,234},{12,236},{14,238}... | collective-permute-start | bytes 12296 | tf_op jit(solution)/shard_map/ppermute | solution.py:495
  107.5 3.6 %collective-permute-start.9 = (bf16[16,128]{1,0:T(8,128)(2,1)S(1)}, bf16[16,128]{1,0:T(8,128)(2,1)S(1)}, u32[]{:S(2)}, u32[]{:S(2)}) collective-permute-start(bf16[16,128]{1,0:T(8,128)(2,1)S(1)} %get-tuple-element.84), channel_id=1, source_target_pairs={{0,32},{2,34},{4,36},{6,38},{8,40},{10,42},{12,44},{14,46},{16,48}... | collective-permute-start | bytes 12296 | tf_op jit(solution)/shard_map/ppermute | solution.py:495
  114.1 12.5 %copy-start.3 = (bf16[256,2048]{1,0:T(8,128)(2,1)S(1)}, bf16[256,2048]{1,0:T(8,128)(2,1)}, u32[]{:S(2)}) copy-start(bf16[256,2048]{1,0:T(8,128)(2,1)} %get-tuple-element.101.refs_0_) | copy-start | bytes 3145732
  114.1 12.5 %copy-start.7 = (bf16[256,256]{1,0:T(8,128)(2,1)S(1)}, bf16[256,256]{1,0:T(8,128)(2,1)}, u32[]{:S(2)}) copy-start(bf16[256,256]{1,0:T(8,128)(2,1)} %get-tuple-element.105.refs_4_) | copy-start | bytes 393220
  114.2 12.5 %copy-start.8 = (bf16[256,256]{1,0:T(8,128)(2,1)S(1)}, bf16[256,256]{1,0:T(8,128)(2,1)}, u32[]{:S(2)}) copy-start(bf16[256,256]{1,0:T(8,128)(2,1)} %get-tuple-element.107.refs_6_) | copy-start | bytes 393220
  114.2 12.5 %copy-start.9 = (bf16[256,256]{1,0:T(8,128)(2,1)S(1)}, bf16[256,256]{1,0:T(8,128)(2,1)}, u32[]{:S(2)}) copy-start(bf16[256,256]{1,0:T(8,128)(2,1)} %get-tuple-element.109.refs_8_) | copy-start | bytes 393220
  114.2 12.5 %copy-start.10 = (bf16[256,256]{1,0:T(8,128)(2,1)S(1)}, bf16[256,256]{1,0:T(8,128)(2,1)}, u32[]{:S(2)}) copy-start(bf16[256,256]{1,0:T(8,128)(2,1)} %get-tuple-element.106.refs_5_) | copy-start | bytes 393220
  114.2 12.5 %copy-start.11 = (bf16[256,256]{1,0:T(8,128)(2,1)S(1)}, bf16[256,256]{1,0:T(8,128)(2,1)}, u32[]{:S(2)}) copy-start(bf16[256,256]{1,0:T(8,128)(2,1)} %get-tuple-element.108.refs_7_) | copy-start | bytes 393220
  114.2 12.5 %copy-start.12 = (bf16[256,256]{1,0:T(8,128)(2,1)S(1)}, bf16[256,256]{1,0:T(8,128)(2,1)}, u32[]{:S(2)}) copy-start(bf16[256,256]{1,0:T(8,128)(2,1)} %get-tuple-element.110.refs_9_) | copy-start | bytes 393220
  114.2 43.4 %all-to-all-start.1 = ((bf16[128,8,640]{2,1,0:T(8,128)(2,1)}), bf16[128,8,640]{2,1,0:T(8,128)(2,1)S(1)}, u32[]{:S(2)}, u32[]{:S(2)}) async-start(bf16[128,8,640]{2,1,0:T(8,128)(2,1)} %bitcast.23), calls=%async_computation.1 | async-start | bytes 2621440 | tf_op jit(solution)/shard_map/all_to_all | solution.py:483
  126.7 1.2 copy-start.4
  127.9 1.2 copy-start.5
  129.2 1.2 copy-start.6
  130.4 9.5 %copy-start.1 = (bf16[2048,128]{1,0:T(8,128)(2,1)S(1)}, bf16[2048,128]{1,0:T(8,128)(2,1)}, u32[]{:S(2)}) copy-start(bf16[2048,128]{1,0:T(8,128)(2,1)} %rex_ref.1) | copy-start | bytes 1572868
  130.4 9.6 %copy-start.2 = (bf16[2048,4]{0,1:T(4,128)(2,1)S(1)}, bf16[2048,4]{0,1:T(4,128)(2,1)}, u32[]{:S(2)}) copy-start(bf16[2048,4]{0,1:T(4,128)(2,1)} %param.11) | copy-start | bytes 49156
  139.9 1.2 collective-permute-start.16

commit v6 on v5

--- a/solution.py
+++ b/solution.py
@@ -63,7 +63,7 @@
 
 def pre_kernel(
     ep_ref, tp_ref, rt_hbm, rgt_hbm, tok_hbm, cot_hbm, rex_hbm,
-    send_out, aux_ref, send_ref, sel_ref, rt_ref, rgt_ref, tok_ref, cot_ref, rex_ref, one_ref, sems,
+    send_out, aux_ref, send_ref, rt_ref, rgt_ref, tok_ref, cot_ref, rex_ref, one_ref, sems,
 ):
     tp = tp_ref[0]
     tok, dm = tok_ref.shape
@@ -82,41 +82,25 @@
     loads[0].wait()
     r0, r1 = rt_ref[0:1, :], rt_ref[1:2, :]
     before = ones_where(iota((tok, tok), 0) < iota((tok, tok), 1))
-    blk = min(256, experts * 8)
-    blocks = experts * 8 // blk
-    row = iota((blk, tok), 0)
-    sub = row & 7
-    want = (2 * tp + (sub & 1)).astype(F32)
-    part = sub >> 1
-    for b in range(blocks):
-        rows = slice(b * blk, (b + 1) * blk)
-        expert = b * (blk // 8) + (row >> 3)
-        hit0 = r0 == expert
-        hit1 = r1 == expert
-        match = mm(ones_where(hit0 | hit1), before) == want
-        one_ref[0, rows, :] = ones_where(hit0 & match)
-        one_ref[1, rows, :] = ones_where(hit1 & match)
-
-    def spread(sel):
-        return jnp.concatenate([jnp.where(part == c, sel, 0.0).astype(BF) for c in range(4)], axis=1)
-
-    def stacked(ref):
-        return jnp.concatenate([ref[:, c * width : (c + 1) * width] for c in range(4)], axis=0)
-
+    n = experts * 2
+    row = iota((n, tok), 0)
+    hit0 = r0 == (row >> 1)
+    hit1 = r1 == (row >> 1)
+    match = mm(ones_where(hit0 | hit1), before) == (2 * tp + (row & 1)).astype(F32)
+    one0 = jnp.where(hit0 & match, 1.0, 0.0)
+    one1 = jnp.where(hit1 & match, 1.0, 0.0)
+    one_ref[...] = (one0 + one1).astype(BF)
     saves = []
 
-    def save(k, rows, cols):
-        saves.append(pltpu.make_async_copy(send_ref.at[rows, cols], send_out.at[rows, cols], sems.at[5 + k]))
+    def place(k, first, rows):
+        cols = pl.ds(first + k * width, width)
+        send_ref[:, :, cols] = rows.astype(BF).reshape(experts, 2, width)
+        saves.append(pltpu.make_async_copy(send_ref.at[:, :, cols], send_out.at[:, :, cols], sems.at[5 + len(saves)]))
         saves[-1].start()
 
     loads[1].wait()
-    stack = stacked(tok_ref)
-    for b in range(blocks):
-        rows = slice(b * blk, (b + 1) * blk)
-        one = one_ref[0, rows, :].astype(F32) + one_ref[1, rows, :].astype(F32)
-        sel_ref[rows, :] = spread(one)
-        send_ref[rows, 0:width] = mm(sel_ref[rows, :], stack).astype(BF)
-        save(2 * b, rows, slice(0, width))
+    for c in range(4):
+        place(c, 0, mm(one_ref[...], tok_ref[:, c * width : (c + 1) * width]))
     loads[2].wait()
     loads[3].wait()
     group_exp = jnp.exp(nt(rgt_ref[...], tok_ref[...]))
@@ -139,13 +123,9 @@
     aux = jnp.where(arow == 6, r0.astype(F32), jnp.where(arow == 7, r1.astype(F32), aux))
     aux_ref[...] = aux
     loads[4].wait()
-    stack = stacked(cot_ref)
-    for b in range(blocks):
-        rows = slice(b * blk, (b + 1) * blk)
-        one0, one1 = one_ref[0, rows, :].astype(F32), one_ref[1, rows, :].astype(F32)
-        scale = jnp.sum(one0 * w0 + one1 * w1, axis=1, keepdims=True)
-        send_ref[rows, width : 2 * width] = (mm(sel_ref[rows, :], stack) * scale).astype(BF)
-        save(2 * b + 1, rows, slice(width, 2 * width))
+    scale = jnp.sum(one0 * w0 + one1 * w1, axis=1, keepdims=True)
+    for c in range(4):
+        place(c, dm, mm(one_ref[...], cot_ref[:, c * width : (c + 1) * width]) * scale)
     for copy in saves:
         copy.wait()
 
@@ -244,30 +224,20 @@
             pltpu.make_async_copy(src, dst, sems.at[5 + k])
             for k, (src, dst) in enumerate(zip(weights[1:], (up_ref, down_ref)))
         ]
-        for copy in loads:
-            copy.start()
+        loads[0].start()
     dm = gate_ref.shape[0]
-    width, half = dm // 4, dm // 2
-    blk = min(256, got_ref.shape[0])
-    n4 = blk // 4
-    shift = n4.bit_length() - 1
-    o, i = iota((blk, blk), 0), iota((blk, blk), 1)
-    perm = ones_where(i == ((o & (n4 - 1)) >> 1) * 8 + (o >> shift) * 2 + (o & 1))
-    for b in range(got_ref.shape[0] // blk):
-        block = slice(b * blk, (b + 1) * blk)
-        rows = slice(b * n4, (b + 1) * n4)
-        y = mm(perm, got_ref[block, 0 : 2 * width]).astype(BF)
-        for c in range(4):
-            cols = slice(c * width, (c + 1) * width)
-            x_ref[rows, cols] = y[c * n4 : (c + 1) * n4, 0:width]
-            sc_ref[rows, cols] = y[c * n4 : (c + 1) * n4, width:]
+    half = dm // 2
+    x_ref[...] = got_ref[:, :, 0:dm].reshape(x_ref.shape)
+    sc_ref[...] = got_ref[:, :, dm:].reshape(sc_ref.shape)
     saves = [
         pltpu.make_async_copy(src, dst, sems.at[k])
         for k, (src, dst) in enumerate(
             ((x_ref, x_out), (sc_ref, sc_out), (gd_ref, gd_out), (ud_ref, ud_out), (hid_ref, hid_out))
         )
     ]
-    if not load:
+    if load:
+        loads[1].start()
+    else:
         saves[0].start()
         saves[1].start()
     gp = mm(x_ref[...], gate_ref[...])
@@ -311,7 +281,8 @@
 def router_terms(tp, x_ref, y_ref, b, bs):
     cols = slice(b * 16 * bs, (b + 1) * 16 * bs)
     rc = tn(x_ref[:, cols], y_ref[...]).reshape(bs, 16, EXTRA)
-    return jnp.where(tp == 0, rc[:, 0:8, :], rc[:, 8:16, :]).reshape(bs * 8, EXTRA)
+    rc = jnp.where(tp == 0, rc[:, 0:8, :], rc[:, 8:16, :])
+    return jnp.where(iota((bs, 4, EXTRA), 2) < LOW_LANE, rc[:, 0:4, :], rc[:, 4:8, :])
 
 
 def early_kernel(tp_ref, came_ref, u_ref, z_ref, x_ref, rc_ref, ul_ref, y_ref):
@@ -319,10 +290,10 @@
     n = u_ref.shape[0]
     u = summed(u_ref, came_ref)
     y_ref[...] = (u * z_ref[...].astype(F32)).astype(BF)
-    ul_ref[...] = jnp.where(iota((n, EXTRA), 1) == U_LANE, u, 0.0).astype(BF)
+    ul_ref[...] = jnp.where(iota((n, EXTRA), 1) == U_LANE, u, 0.0)
     bs = min(32, n // 2)
     for b in range(n // (2 * bs)):
-        rc_ref[b * bs * 8 : (b + 1) * bs * 8, :] = router_terms(tp, x_ref, y_ref, b, bs)
+        rc_ref[b * bs : (b + 1) * bs] = router_terms(tp, x_ref, y_ref, b, bs)
 
 
 def pack_kernel(tp_ref, *refs):
@@ -331,29 +302,20 @@
     u_ref, z_ref, x_ref, rc1_ref, ul1_ref, ret_out, ret_ref, y_ref, ul_ref, sems = refs[4:14]
     saves = []
     n, half = mine[0].shape
-    width = half // 2
     u = summed(u_ref, came[0])
     y_ref[...] = (u * z_ref[...].astype(F32)).astype(BF)
-    ul_ref[...] = jnp.where(iota((n, EXTRA), 1) == U_LANE, u, 0.0).astype(BF)
-    blk = min(256, n * 4)
-    bs = blk // 8
-    o, i = iota((blk, blk), 0), iota((blk, blk), 1)
-    perm = ones_where(i == ((o >> 2) & 1) * (4 * bs) + ((o >> 1) & 1) * (2 * bs) + (o >> 3) * 2 + (o & 1))
-    wide = iota((blk, EXTRA), 1) < LOW_LANE
+    ul_ref[...] = jnp.where(iota((n, EXTRA), 1) == U_LANE, u, 0.0)
+    bs = min(32, n // 2)
     for b in range(n // (2 * bs)):
         rows = slice(b * 2 * bs, (b + 1) * 2 * bs)
-        out = slice(b * blk, (b + 1) * blk)
-        sums = [(mine[p][rows, :].astype(F32) + came[p][rows, 0:half].astype(F32)).astype(BF) for p in range(2)]
-        stack = jnp.concatenate(
-            [sums[0][:, 0:width], sums[1][:, 0:width], sums[0][:, width:], sums[1][:, width:]], axis=0
-        )
-        ret_ref[out, 0:width] = mm(perm, stack).astype(BF)
-        ulane = jnp.concatenate([ul_ref[rows, :], ul1_ref[rows, :]], axis=0)
-        base = mm(perm[:, 0 : 4 * bs], ulane)
-        rc = router_terms(tp, x_ref, y_ref, b, bs) + rc1_ref[out, :]
-        high = rc.astype(BF).astype(F32)
-        ret_ref[out, width:] = (base + jnp.where(wide, high, rc - high)).astype(BF)
-        saves.append(pltpu.make_async_copy(ret_ref.at[out, :], ret_out.at[out, :], sems.at[b]))
+        out = slice(b * bs, (b + 1) * bs)
+        rc = router_terms(tp, x_ref, y_ref, b, bs) + rc1_ref[out]
+        for p, lanes in ((0, ul_ref), (1, ul1_ref)):
+            total = (mine[p][rows, :].astype(F32) + came[p][rows, 0:half].astype(F32)).astype(BF)
+            at = slice(2 * p, 2 * p + 2)
+            ret_ref[out, at, 0:half] = total.reshape(bs, 2, half)
+            ret_ref[out, at, half:] = (rc[:, at, :] + lanes[rows, :].reshape(bs, 2, EXTRA)).astype(BF)
+        saves.append(pltpu.make_async_copy(ret_ref.at[out], ret_out.at[out], sems.at[b]))
         saves[-1].start()
     for save in saves:
         save.wait()
@@ -399,20 +361,15 @@
     experts = rex_ref.shape[1]
     gw = experts // groups
     r0, r1 = aux_ref[:, 6:7].astype(jnp.int32), aux_ref[:, 7:8].astype(jnp.int32)
-    n = experts * 8
+    n = experts * 4
     col = iota((tok, n), 1)
-    hit0 = r0 == (col >> 3)
-    hit1 = r1 == (col >> 3)
+    hit0 = r0 == (col >> 2)
+    hit1 = r1 == (col >> 2)
     earlier = ones_where(iota((tok, tok), 1) < iota((tok, tok), 0))
     rank = mm(earlier, ones_where(hit0 | hit1))
     match = rank == ((2 * tp + (col & 3)) & 3).astype(F32)
-    lower = (col & 4) == 0
-    one0 = jnp.where(hit0 & match, 1.0, 0.0)
-    one1 = jnp.where(hit1 & match, 1.0, 0.0)
-    sel_ref[0] = jnp.where(lower, one0, 0.0).astype(BF)
-    sel_ref[1] = jnp.where(lower, one1, 0.0).astype(BF)
-    sel_ref[2] = jnp.where(lower, one0 + one1, 0.0).astype(BF)
-    sel_ref[3] = jnp.where(lower, 0.0, one0 + one1).astype(BF)
+    sel_ref[0] = ones_where(hit0 & match)
+    sel_ref[1] = ones_where(hit1 & match)
     ei = iota((tok, experts), 1)
     pick = (jnp.where(ei == r0, 1.0, 0.0) - jnp.where(ei == r1, 1.0, 0.0)).astype(BF)
     near = pl.ds(pl.multiple_of(tp * half, half), half)
@@ -431,26 +388,30 @@
 ):
     gate_sq_ref[...] = sq_ref[0:1, :] + sqo_ref[0:1, :]
     up_sq_ref[...] = sq_ref[1:2, :] + sqo_ref[1:2, :]
-    width = back_ref.shape[1] - EXTRA
+    half = tg_ref.shape[1]
+    width = half // 2
     experts = rex_ref.shape[1]
     groups = rg_ref.shape[0]
     gw = experts // groups
-    extra = back_ref[:, width:]
+    slots = experts * 4
+    extra3 = back_ref[:, :, half:]
+    extra = extra3.reshape(slots, EXTRA)
     u0 = mm(sel_ref[0], extra)[:, U_LANE : U_LANE + 1]
     u1 = mm(sel_ref[1], extra)[:, U_LANE : U_LANE + 1]
     lean = aux_ref[:, 1:2] * u0 - aux_ref[:, 0:1] * u1
     both = u0 + u1
+    sel = (sel_ref[0].astype(F32) + sel_ref[1].astype(F32)).astype(BF)
     for c in range(2):
         cols = slice(c * width, (c + 1) * width)
-        part = mm(sel_ref[2 + c], back_ref[:, 0:width])
+        part = mm(sel, back_ref[:, :, cols].reshape(slots, width))
         tg_ref[:, cols] = (part + (both * h_ref[:, cols] + lean * q_ref[:, cols])).astype(BF)
-    sums = jnp.sum(extra.astype(F32).reshape(groups, gw, 8, EXTRA), axis=1)
+    sums = jnp.sum(extra3.astype(F32).reshape(groups, gw, 4, EXTRA), axis=1)
     rg = None
     square = None
     lane = iota((8, EXTRA), 1)
     for g in range(groups):
         s = sums[g]
-        s = s + jnp.concatenate([s[:, LOW_LANE:], s[:, 0:LOW_LANE]], axis=1)
+        s = jnp.concatenate([s, jnp.concatenate([s[:, LOW_LANE:], s[:, 0:LOW_LANE]], axis=1)], axis=0)
         rex = s[:, 0:gw]
         rex_ref[:, g * gw : (g + 1) * gw] = rex
         rg = s if g == 0 else rg + s
@@ -467,7 +428,7 @@
     tok, dm = tokens.shape
     experts = router_expert.shape[1]
     groups = router_group.shape[1]
-    width, half = dm // 4, dm // 2
+    half = dm // 2
     ff = gate_proj.shape[2]
     n = experts * 2
     tp = lax.axis_index("tp").reshape(1)
@@ -479,9 +440,7 @@
     gate, up, down = gate_proj[0], up_proj[0], down_proj[0]
 
     def exchange(x):
-        m = x.shape[1]
-        y = lax.all_to_all(x.reshape(experts, 8, m), "ep", split_axis=0, concat_axis=0, tiled=True)
-        return y.reshape(experts * 8, m)
+        return lax.all_to_all(x, "ep", split_axis=0, concat_axis=0, tiled=True)
 
     def partner(x):
         return lax.ppermute(x, "tp", swap)
@@ -496,13 +455,13 @@
 
     send, aux = call(
         pre_kernel, 1 << 30, 20,
-        [((experts * 8, 2 * width), BF), ((EXTRA, tok), F32)],
+        [((experts, 2, 2 * dm), BF), ((EXTRA, tok), F32)],
         idx, [far(routes.T), far(rgt), far(tokens), far(cotangent), far(router_expert)],
         scratch=[
-            pltpu.VMEM((experts * 8, 2 * width), BF), pltpu.VMEM((experts * 8, 4 * tok), BF),
+            pltpu.VMEM((experts, 2, 2 * dm), BF),
             pltpu.VMEM((2, tok), jnp.int32), pltpu.VMEM((groups, dm), BF),
             pltpu.VMEM((tok, dm), BF), pltpu.VMEM((tok, dm), BF), pltpu.VMEM((dm, experts), BF),
-            pltpu.VMEM((2, experts * 8, tok), BF), pltpu.SemaphoreType.DMA((13,)),
+            pltpu.VMEM((n, tok), BF), pltpu.SemaphoreType.DMA((13,)),
         ],
         spaces=[HB] * 5,
         out_spaces=[HB, VM],
@@ -538,14 +497,14 @@
     u, mine, theirs, xv, x, sc, gd, ud, hid = [list(v) for v in zip(first[:9], second)]
     came = [partner(theirs[1]), partner(theirs[0])]
     rc1, ul1 = call(
-        early_kernel, 1 << 28, 8, [((experts * 8, EXTRA), F32), ((n, EXTRA), BF)],
+        early_kernel, 1 << 28, 8, [((experts, 4, EXTRA), F32), ((n, EXTRA), F32)],
         [tp], [came[1], u[1], z[1], xv[1]], scratch=[pltpu.VMEM((n, EXTRA), BF)],
     )
     (ret,) = call(
-        pack_kernel, 1 << 29, 16, [((experts * 8, width + EXTRA), BF)],
+        pack_kernel, 1 << 29, 16, [((experts, 4, half + EXTRA), BF)],
         [tp], [*mine, *came, u[0], z[0], xv[0], rc1, ul1],
         scratch=[
-            pltpu.VMEM((experts * 8, width + EXTRA), BF), pltpu.VMEM((n, EXTRA), BF), pltpu.VMEM((n, EXTRA), BF),
+            pltpu.VMEM((experts, 4, half + EXTRA), BF), pltpu.VMEM((n, EXTRA), BF), pltpu.VMEM((n, EXTRA), F32),
             pltpu.SemaphoreType.DMA((4,)),
         ],
         out_spaces=[HB],
@@ -559,7 +518,7 @@
     sq_other = partner(sq)
     sel, q, h = call(
         home_kernel, 1 << 29, 8,
-        [((4, tok, experts * 8), BF), ((tok, half), F32), ((tok, half), F32)],
+        [((2, tok, experts * 4), BF), ((tok, half), F32), ((tok, half), F32)],
         [tp], [aux_cols, rgt, router_expert],
     )
     token_grad, rex_grad, rg_grad, rows, gate_sq, up_sq = call(

time: 159 us -> 156 us (0.981)
  waiting for transfers between devices: 26.5 us -> 24 us
    all_to_all x1, waiting for transfers between devices: 16.5 us -> 13.7 us  [exchange(): return lax.all_to_all(x, 'ep', split_axis=0, concat_axis=0, tiled=True)]
where the time goes in v6:
time: 156 us
  blocking collectives  68.5 us (44%)
  starting transfers between devices  32.3 us (21%)
  Pallas kernels  26.2 us (17%)
  waiting for transfers between devices  24 us (15%)
  local copies, waits for them, and re-layouts  3.72 us (2%)
    all_to_all x1, blocking collectives, exchange(): return lax.all_to_all(x, 'ep', split_axis=0, concat_axis=0, tiled=True)  68.5 us
    pallas_call x13, Pallas kernels, call(): pl.pallas_call(kernel, out_shape=[pltpu.HBM(shape, dtype) if out_spaces a...  26.2 us
    ppermute x13, starting transfers between devices, shift(): return lax.ppermute(v, 'ep', pairs)  19.3 us
    all_to_all x1, waiting for transfers between devices, exchange(): return lax.all_to_all(x, 'ep', split_axis=0, concat_axis=0, tiled=True)  13.7 us
    all_to_all x1, starting transfers between devices, exchange(): return lax.all_to_all(x, 'ep', split_axis=0, concat_axis=0, tiled=True)  12.3 us
    ppermute x13, waiting for transfers between devices, shift(): return lax.ppermute(v, 'ep', pairs)  9.63 us
    unnamed x26, local copies, waits for them, and re-layouts  3.72 us
  transfers between devices with their start and end apart: 18, of which 11 were waited for; matrix products, arithmetic and copies ran while one was open for 0% of the time, Pallas kernels for 13%

profile of v6, /device:TPU:32, one launch (start us, length us, event | category | flops | bytes accessed | tf_op | source)
XLA Modules:
  0.0 155.5 jit_solution(7342336974289684722)
XLA Ops:
  0.6 3.5 %shard_map.159 = (bf16[128,2,4096]{2,1,0:T(2,128)(2,1)}, f32[128,128]{1,0:T(8,128)S(1)}) custom-call(s32[1]{0:T(128)} %bitcast.1.ep_ref, s32[1]{0:T(128)} %bitcast.tp_ref, s32[2,128]{1,0:T(2,128)} %bitcast.19, bf16[4,2048]{1,0:T(4,128)(2,1)} %bitcast.14, bf16[128,2048]{1,0:T(8,128)(2,1)} %tok_hbm.1, bf16[128,2048]{1,0:T(8,128)(2,1)} %cot_hbm.1, ...), custom_call_target="tpu_custom_call" | custom-call | flops 1073741824 | bytes 4194304 | tf_op jit(solution)/shard_map/pallas_call | solution.py:46
  4.1 0.0 copy-start
  4.1 68.5 %all_to_all.10.got_ref = bf16[128,2,4096]{2,1,0:T(2,128)(2,1)S(1)} all-to-all(bf16[128,2,4096]{2,1,0:T(2,128)(2,1)} %get-tuple-element.66), channel_id=1, replica_groups=mesh['ep'=128,'tp'=2] {'ep'}, dimensions={0} | all-to-all | bytes 4194304 | tf_op jit(solution)/shard_map/all_to_all | solution.py:443
  72.6 4.3 %shard_map.160 = (f32[256,128]{1,0:T(8,128)S(1)}, bf16[256,1024]{1,0:T(8,128)(2,1)S(1)}, bf16[256,1152]{1,0:T(8,128)(2,1)S(1)}, bf16[256,2048]{1,0:T(8,128)(2,1)...) custom-call(s32[1]{0:T(128)} %bitcast.tp_ref, ...), custom_call_target="tpu_custom_call" | custom-call | flops 3221225472 | bytes 4194304 | tf_op jit(solution)/shard_map/pallas_call | solution.py:46
  76.9 0.6 collective-permute-start.2
  77.5 3.0 %shard_map.161 = (f32[256,128]{1,0:T(8,128)S(1)}, bf16[256,1024]{1,0:T(8,128)(2,1)S(1)}, bf16[256,1152]{1,0:T(8,128)(2,1)S(1)}, bf16[256,2048]{1,0:T(8,128)(2,1)...) custom-call(s32[1]{0:T(128)} %bitcast.tp_ref, ...), custom_call_target="tpu_custom_call" | custom-call | flops 3221225472 | bytes 4194304 | tf_op jit(solution)/shard_map/pallas_call | solution.py:46
  80.6 0.1 collective-permute-start.1
  80.7 0.6 shard_map.162
  81.2 0.8 collective-permute-start.3
  82.0 0.8 collective-permute-start.4
  82.9 1.9 %collective-permute-start.5 = (bf16[32,128]{1,0:T(8,128)(2,1)S(1)}, bf16[32,128]{1,0:T(8,128)(2,1)S(1)}, u32[]{:S(2)}, u32[]{:S(2)}) collective-permute-start(bf16[32,128]{1,0:T(8,128)(2,1)S(1)} %get-tuple-element.78), channel_id=1, source_target_pairs={{0,6},{2,0},{4,2},{6,4},{8,14},{10,8},{12,10},{14,12},{16,22},{18,... | collective-permute-start | bytes 24584 | tf_op jit(solution)/shard_map/ppermute | solution.py:454
  84.8 1.4 collective-permute-done.3.b_ref
  86.2 1.0 collective-permute-done.4.c_ref
  87.2 0.1 shard_map.163
  87.3 0.2 collective-permute-start.6
  87.5 2.0 %collective-permute-start.7 = (bf16[32,128]{1,0:T(8,128)(2,1)S(1)}, bf16[32,128]{1,0:T(8,128)(2,1)S(1)}, u32[]{:S(2)}, u32[]{:S(2)}) collective-permute-start(bf16[32,128]{1,0:T(8,128)(2,1)S(1)} %get-tuple-element.81), channel_id=1, source_target_pairs={{0,16},{2,18},{4,20},{6,22},{8,24},{10,26},{12,28},{14,30},{16,0},... | collective-permute-start | bytes 24584 | tf_op jit(solution)/shard_map/ppermute | solution.py:454
  89.5 1.3 collective-permute-start.8
  90.7 1.6 %collective-permute-done.6.b_ref = bf16[32,128]{1,0:T(8,128)(2,1)S(1)} collective-permute-done((bf16[32,128]{1,0:T(8,128)(2,1)S(1)}, bf16[32,128]{1,0:T(8,128)(2,1)S(1)}, u32[]{:S(2)}, u32[]{:S(2)}) %collective-permute-start.6) | collective-permute-done | bytes 8224 | tf_op jit(solution)/shard_map/ppermute | solution.py:454
  92.4 0.4 collective-permute-done.7.c_ref
  92.8 0.6 collective-permute-done.8.d_ref
  93.3 0.2 shard_map.164
  93.5 1.3 collective-permute-start.10
  94.7 3.3 %collective-permute-start.11 = (bf16[16,128]{1,0:T(8,128)(2,1)S(1)}, bf16[16,128]{1,0:T(8,128)(2,1)S(1)}, u32[]{:S(2)}, u32[]{:S(2)}) collective-permute-start(bf16[16,128]{1,0:T(8,128)(2,1)S(1)} %get-tuple-element.86), channel_id=1, source_target_pairs={{0,96},{2,98},{4,100},{6,102},{8,104},{10,106},{12,108},{14,110},{... | collective-permute-start | bytes 12296 | tf_op jit(solution)/shard_map/ppermute | solution.py:454
  98.0 2.2 %collective-permute-start.12 = (bf16[16,128]{1,0:T(8,128)(2,1)S(1)}, bf16[16,128]{1,0:T(8,128)(2,1)S(1)}, u32[]{:S(2)}, u32[]{:S(2)}) collective-permute-start(bf16[16,128]{1,0:T(8,128)(2,1)S(1)} %get-tuple-element.87), channel_id=1, source_target_pairs={{0,128},{2,130},{4,132},{6,134},{8,136},{10,138},{12,140},{14,142}... | collective-permute-start | bytes 12296 | tf_op jit(solution)/shard_map/ppermute | solution.py:454
  100.2 3.1 %collective-permute-start.13 = (bf16[16,128]{1,0:T(8,128)(2,1)S(1)}, bf16[16,128]{1,0:T(8,128)(2,1)S(1)}, u32[]{:S(2)}, u32[]{:S(2)}) collective-permute-start(bf16[16,128]{1,0:T(8,128)(2,1)S(1)} %get-tuple-element.88), channel_id=1, source_target_pairs={{0,160},{2,162},{4,164},{6,166},{8,168},{10,170},{12,172},{14,174}... | collective-permute-start | bytes 12296 | tf_op jit(solution)/shard_map/ppermute | solution.py:454
  103.4 1.0 collective-permute-start.14
  104.4 1.2 collective-permute-done.12.refs_4_
  105.5 0.4 collective-permute-start.15
  106.0 0.9 collective-permute-done.13.refs_5_
  106.9 1.0 collective-permute-start.9
  107.9 0.0 collective-permute-done.14.refs_6_
  107.9 1.3 collective-permute-done.15.refs_7_
  109.1 1.3 collective-permute-done.9.refs_1_
  110.5 0.6 shard_map.165
  111.1 0.6 shard_map.166
  111.7 1.9 %shard_map.167 = bf16[128,4,1152]{2,1,0:T(4,128)(2,1)} custom-call(s32[1]{0:T(128)} %bitcast.tp_ref, bf16[256,1024]{1,0:T(8,128)(2,1)S(1)} %get-tuple-element.67.refs_0_, bf16[256,1024]{1,0:T(8,128)(2,1)S(1)} %get-tuple-element.70.refs_1_, bf16[256,1152]{1,0:T(8,128)(2,1)S(1)} %collective-permute-done.1.refs_2_, ...), custom_call_target="tpu_custom_call" | custom-call | flops 536870912 | bytes 4194304 | tf_op jit(solution)/shard_map/pallas_call | solution.py:46
  113.6 0.0 copy-start.3
  113.6 12.3 %all-to-all-start.1 = ((bf16[128,4,1152]{2,1,0:T(4,128)(2,1)}), bf16[128,4,1152]{2,1,0:T(4,128)(2,1)S(1)}, u32[]{:S(2)}, u32[]{:S(2)}) async-start(bf16[128,4,1152]{2,1,0:T(4,128)(2,1)} %shard_map.167), calls=%async_computation.1 | async-start | bytes 2359296 | tf_op jit(solution)/shard_map/all_to_all | solution.py:443
  126.0 0.1 shard_map.168.aux_ref
  126.1 0.0 copy-start.4
  126.1 1.2 copy-done.4
  127.4 1.2 copy-done.5
  128.6 1.2 copy-done.6
  129.8 9.5 %shard_map.170 = (bf16[2048,256]{1,0:T(8,128)(2,1)}, bf16[2048,256]{1,0:T(8,128)(2,1)}, bf16[256,2048]{1,0:T(8,128)(2,1)}, f32[2,2048]{1,0:T(2,128)S(1)}, f32[1,256]{1,0:T(1,128)}) custom-call(bf16[256,2048]{1,0:T(8,128)(2,1)S(1)} %copy-done.3, bf16[256,2048]{1,0:T(8,128)(2,1)S(1)} %copy-done.5, bf16[256,2048]{1,0:T(8,128)(2,1)S(1)} %copy-done.4, ...), custom_call_target="tpu_custom_call" | custom-call | flops 3221225472 | bytes 4194304 | tf_op jit(solution)/shard_map/pallas_call | solution.py:46
  139.4 0.5 shard_map.169
  139.9 0.6 collective-permute-done.16.sqo_ref
  140.5 13.7 %all-to-all-done.1.back_ref = bf16[128,4,1152]{2,1,0:T(4,128)(2,1)S(1)} async-done(((bf16[128,4,1152]{2,1,0:T(4,128)(2,1)}), bf16[128,4,1152]{2,1,0:T(4,128)(2,1)S(1)}, u32[]{:S(2)}, u32[]{:S(2)}) %all-to-all-start.1) | async-done | bytes 1179680 | tf_op jit(solution)/shard_map/all_to_all | solution.py:443
  154.3 1.3 shard_map.171
  (28 shorter events, 0.1 us)
Async XLA Ops:
  4.1 68.5 %copy-start = (bf16[1,2048,256]{2,1,0:T(8,128)(2,1)S(1)}, bf16[1,2048,256]{2,1,0:T(8,128)(2,1)}, u32[]{:S(2)}) copy-start(bf16[1,2048,256]{2,1,0:T(8,128)(2,1)} %param.13) | copy-start | bytes 3145732
  72.6 4.9 %collective-permute-start = (bf16[128,2,4096]{2,1,0:T(2,128)(2,1)S(1)}, bf16[128,2,4096]{2,1,0:T(2,128)(2,1)S(1)}, u32[]{:S(2)}, u32[]{:S(2)}) collective-permute-start(bf16[128,2,4096]{2,1,0:T(2,128)(2,1)S(1)} %all_to_all.10.got_ref), channel_id=1, source_target_pairs={{0,1},{1,0},{2,3},{3,2},{4,5},{5,4},{6,7},{7,6},{8,9},{9,8},{10,11... | collective-permute-start | bytes 6291464 | tf_op jit(solution)/shard_map/ppermute | solution.py:446
  76.9 34.2 %collective-permute-start.2 = (bf16[256,1152]{1,0:T(8,128)(2,1)S(1)}, bf16[256,1152]{1,0:T(8,128)(2,1)S(1)}, u32[]{:S(2)}, u32[]{:S(2)}) collective-permute-start(bf16[256,1152]{1,0:T(8,128)(2,1)S(1)} %get-tuple-element.72), channel_id=1, source_target_pairs={{0,1},{1,0},{2,3},{3,2},{4,5},{5,4},{6,7},{7,6},{8,9},{9,8},{10,11... | collective-permute-start | bytes 1769480 | tf_op jit(solution)/shard_map/ppermute | solution.py:446
  80.6 31.1 %collective-permute-start.1 = (bf16[256,1152]{1,0:T(8,128)(2,1)S(1)}, bf16[256,1152]{1,0:T(8,128)(2,1)S(1)}, u32[]{:S(2)}, u32[]{:S(2)}) collective-permute-start(bf16[256,1152]{1,0:T(8,128)(2,1)S(1)} %get-tuple-element.71), channel_id=1, source_target_pairs={{0,1},{1,0},{2,3},{3,2},{4,5},{5,4},{6,7},{7,6},{8,9},{9,8},{10,11... | collective-permute-start | bytes 1769480 | tf_op jit(solution)/shard_map/ppermute | solution.py:446
  81.2 4.9 %collective-permute-start.3 = (bf16[32,128]{1,0:T(8,128)(2,1)S(1)}, bf16[32,128]{1,0:T(8,128)(2,1)S(1)}, u32[]{:S(2)}, u32[]{:S(2)}) collective-permute-start(bf16[32,128]{1,0:T(8,128)(2,1)S(1)} %get-tuple-element.76), channel_id=1, source_target_pairs={{0,2},{2,4},{4,6},{6,0},{8,10},{10,12},{12,14},{14,8},{16,18},{18,... | collective-permute-start | bytes 24584 | tf_op jit(solution)/shard_map/ppermute | solution.py:454
  82.0 5.2 %collective-permute-start.4 = (bf16[32,128]{1,0:T(8,128)(2,1)S(1)}, bf16[32,128]{1,0:T(8,128)(2,1)S(1)}, u32[]{:S(2)}, u32[]{:S(2)}) collective-permute-start(bf16[32,128]{1,0:T(8,128)(2,1)S(1)} %get-tuple-element.77), channel_id=1, source_target_pairs={{0,4},{2,6},{4,0},{6,2},{8,12},{10,14},{12,8},{14,10},{16,20},{18,... | collective-permute-start | bytes 24584 | tf_op jit(solution)/shard_map/ppermute | solution.py:454
  82.9 4.3 %collective-permute-start.5 = (bf16[32,128]{1,0:T(8,128)(2,1)S(1)}, bf16[32,128]{1,0:T(8,128)(2,1)S(1)}, u32[]{:S(2)}, u32[]{:S(2)}) collective-permute-start(bf16[32,128]{1,0:T(8,128)(2,1)S(1)} %get-tuple-element.78), channel_id=1, source_target_pairs={{0,6},{2,0},{4,2},{6,4},{8,14},{10,8},{12,10},{14,12},{16,22},{18,... | collective-permute-start | bytes 24584 | tf_op jit(solution)/shard_map/ppermute | solution.py:454
  87.3 5.0 %collective-permute-start.6 = (bf16[32,128]{1,0:T(8,128)(2,1)S(1)}, bf16[32,128]{1,0:T(8,128)(2,1)S(1)}, u32[]{:S(2)}, u32[]{:S(2)}) collective-permute-start(bf16[32,128]{1,0:T(8,128)(2,1)S(1)} %get-tuple-element.80), channel_id=1, source_target_pairs={{0,8},{2,10},{4,12},{6,14},{8,16},{10,18},{12,20},{14,22},{16,24},... | collective-permute-start | bytes 24584 | tf_op jit(solution)/shard_map/ppermute | solution.py:454
  87.5 5.2 %collective-permute-start.7 = (bf16[32,128]{1,0:T(8,128)(2,1)S(1)}, bf16[32,128]{1,0:T(8,128)(2,1)S(1)}, u32[]{:S(2)}, u32[]{:S(2)}) collective-permute-start(bf16[32,128]{1,0:T(8,128)(2,1)S(1)} %get-tuple-element.81), channel_id=1, source_target_pairs={{0,16},{2,18},{4,20},{6,22},{8,24},{10,26},{12,28},{14,30},{16,0},... | collective-permute-start | bytes 24584 | tf_op jit(solution)/shard_map/ppermute | solution.py:454
  89.5 3.8 %collective-permute-start.8 = (bf16[32,128]{1,0:T(8,128)(2,1)S(1)}, bf16[32,128]{1,0:T(8,128)(2,1)S(1)}, u32[]{:S(2)}, u32[]{:S(2)}) collective-permute-start(bf16[32,128]{1,0:T(8,128)(2,1)S(1)} %get-tuple-element.82), channel_id=1, source_target_pairs={{0,24},{2,26},{4,28},{6,30},{8,0},{10,2},{12,4},{14,6},{16,8},{18,... | collective-permute-start | bytes 24584 | tf_op jit(solution)/shard_map/ppermute | solution.py:454
  93.5 6.8 %collective-permute-start.10 = (bf16[16,128]{1,0:T(8,128)(2,1)S(1)}, bf16[16,128]{1,0:T(8,128)(2,1)S(1)}, u32[]{:S(2)}, u32[]{:S(2)}) collective-permute-start(bf16[16,128]{1,0:T(8,128)(2,1)S(1)} %get-tuple-element.85), channel_id=1, source_target_pairs={{0,64},{2,66},{4,68},{6,70},{8,72},{10,74},{12,76},{14,78},{16,80}... | collective-permute-start | bytes 12296 | tf_op jit(solution)/shard_map/ppermute | solution.py:454
  94.7 8.6 %collective-permute-start.11 = (bf16[16,128]{1,0:T(8,128)(2,1)S(1)}, bf16[16,128]{1,0:T(8,128)(2,1)S(1)}, u32[]{:S(2)}, u32[]{:S(2)}) collective-permute-start(bf16[16,128]{1,0:T(8,128)(2,1)S(1)} %get-tuple-element.86), channel_id=1, source_target_pairs={{0,96},{2,98},{4,100},{6,102},{8,104},{10,106},{12,108},{14,110},{... | collective-permute-start | bytes 12296 | tf_op jit(solution)/shard_map/ppermute | solution.py:454
  98.0 7.5 %collective-permute-start.12 = (bf16[16,128]{1,0:T(8,128)(2,1)S(1)}, bf16[16,128]{1,0:T(8,128)(2,1)S(1)}, u32[]{:S(2)}, u32[]{:S(2)}) collective-permute-start(bf16[16,128]{1,0:T(8,128)(2,1)S(1)} %get-tuple-element.87), channel_id=1, source_target_pairs={{0,128},{2,130},{4,132},{6,134},{8,136},{10,138},{12,140},{14,142}... | collective-permute-start | bytes 12296 | tf_op jit(solution)/shard_map/ppermute | solution.py:454
  100.2 6.6 %collective-permute-start.13 = (bf16[16,128]{1,0:T(8,128)(2,1)S(1)}, bf16[16,128]{1,0:T(8,128)(2,1)S(1)}, u32[]{:S(2)}, u32[]{:S(2)}) collective-permute-start(bf16[16,128]{1,0:T(8,128)(2,1)S(1)} %get-tuple-element.88), channel_id=1, source_target_pairs={{0,160},{2,162},{4,164},{6,166},{8,168},{10,170},{12,172},{14,174}... | collective-permute-start | bytes 12296 | tf_op jit(solution)/shard_map/ppermute | solution.py:454
  103.4 4.5 %collective-permute-start.14 = (bf16[16,128]{1,0:T(8,128)(2,1)S(1)}, bf16[16,128]{1,0:T(8,128)(2,1)S(1)}, u32[]{:S(2)}, u32[]{:S(2)}) collective-permute-start(bf16[16,128]{1,0:T(8,128)(2,1)S(1)} %get-tuple-element.89), channel_id=1, source_target_pairs={{0,192},{2,194},{4,196},{6,198},{8,200},{10,202},{12,204},{14,206}... | collective-permute-start | bytes 12296 | tf_op jit(solution)/shard_map/ppermute | solution.py:454
  105.5 3.6 %collective-permute-start.15 = (bf16[16,128]{1,0:T(8,128)(2,1)S(1)}, bf16[16,128]{1,0:T(8,128)(2,1)S(1)}, u32[]{:S(2)}, u32[]{:S(2)}) collective-permute-start(bf16[16,128]{1,0:T(8,128)(2,1)S(1)} %get-tuple-element.90), channel_id=1, source_target_pairs={{0,224},{2,226},{4,228},{6,230},{8,232},{10,234},{12,236},{14,238}... | collective-permute-start | bytes 12296 | tf_op jit(solution)/shard_map/ppermute | solution.py:454
  106.9 3.6 %collective-permute-start.9 = (bf16[16,128]{1,0:T(8,128)(2,1)S(1)}, bf16[16,128]{1,0:T(8,128)(2,1)S(1)}, u32[]{:S(2)}, u32[]{:S(2)}) collective-permute-start(bf16[16,128]{1,0:T(8,128)(2,1)S(1)} %get-tuple-element.84), channel_id=1, source_target_pairs={{0,32},{2,34},{4,36},{6,38},{8,40},{10,42},{12,44},{14,46},{16,48}... | collective-permute-start | bytes 12296 | tf_op jit(solution)/shard_map/ppermute | solution.py:454
  113.6 12.5 %copy-start.3 = (bf16[256,2048]{1,0:T(8,128)(2,1)S(1)}, bf16[256,2048]{1,0:T(8,128)(2,1)}, u32[]{:S(2)}) copy-start(bf16[256,2048]{1,0:T(8,128)(2,1)} %get-tuple-element.101.refs_0_) | copy-start | bytes 3145732
  113.6 12.5 %copy-start.7 = (bf16[256,256]{1,0:T(8,128)(2,1)S(1)}, bf16[256,256]{1,0:T(8,128)(2,1)}, u32[]{:S(2)}) copy-start(bf16[256,256]{1,0:T(8,128)(2,1)} %get-tuple-element.105.refs_4_) | copy-start | bytes 393220
  113.6 12.5 %copy-start.8 = (bf16[256,256]{1,0:T(8,128)(2,1)S(1)}, bf16[256,256]{1,0:T(8,128)(2,1)}, u32[]{:S(2)}) copy-start(bf16[256,256]{1,0:T(8,128)(2,1)} %get-tuple-element.107.refs_6_) | copy-start | bytes 393220
  113.6 12.5 %copy-start.9 = (bf16[256,256]{1,0:T(8,128)(2,1)S(1)}, bf16[256,256]{1,0:T(8,128)(2,1)}, u32[]{:S(2)}) copy-start(bf16[256,256]{1,0:T(8,128)(2,1)} %get-tuple-element.109.refs_8_) | copy-start | bytes 393220
  113.6 12.5 %copy-start.10 = (bf16[256,256]{1,0:T(8,128)(2,1)S(1)}, bf16[256,256]{1,0:T(8,128)(2,1)}, u32[]{:S(2)}) copy-start(bf16[256,256]{1,0:T(8,128)(2,1)} %get-tuple-element.106.refs_5_) | copy-start | bytes 393220
  113.6 12.5 %copy-start.11 = (bf16[256,256]{1,0:T(8,128)(2,1)S(1)}, bf16[256,256]{1,0:T(8,128)(2,1)}, u32[]{:S(2)}) copy-start(bf16[256,256]{1,0:T(8,128)(2,1)} %get-tuple-element.108.refs_7_) | copy-start | bytes 393220
  113.6 12.5 %copy-start.12 = (bf16[256,256]{1,0:T(8,128)(2,1)S(1)}, bf16[256,256]{1,0:T(8,128)(2,1)}, u32[]{:S(2)}) copy-start(bf16[256,256]{1,0:T(8,128)(2,1)} %get-tuple-element.110.refs_9_) | copy-start | bytes 393220
  113.6 40.6 %all-to-all-start.1 = ((bf16[128,4,1152]{2,1,0:T(4,128)(2,1)}), bf16[128,4,1152]{2,1,0:T(4,128)(2,1)S(1)}, u32[]{:S(2)}, u32[]{:S(2)}) async-start(bf16[128,4,1152]{2,1,0:T(4,128)(2,1)} %shard_map.167), calls=%async_computation.1 | async-start | bytes 2359296 | tf_op jit(solution)/shard_map/all_to_all | solution.py:443
  126.1 1.2 copy-start.4
  127.4 1.2 copy-start.5
  128.6 1.2 copy-start.6
  129.8 9.6 %copy-start.1 = (bf16[2048,128]{1,0:T(8,128)(2,1)S(1)}, bf16[2048,128]{1,0:T(8,128)(2,1)}, u32[]{:S(2)}) copy-start(bf16[2048,128]{1,0:T(8,128)(2,1)} %rex_ref.1) | copy-start | bytes 1572868
  129.8 9.6 %copy-start.2 = (bf16[2048,4]{0,1:T(4,128)(2,1)S(1)}, bf16[2048,4]{0,1:T(4,128)(2,1)}, u32[]{:S(2)}) copy-start(bf16[2048,4]{0,1:T(4,128)(2,1)} %param.11) | copy-start | bytes 49156
  139.3 1.2 collective-permute-start.16

commit v7 on v6

--- a/solution.py
+++ b/solution.py
@@ -214,40 +214,46 @@
 def expert_kernel(load, tp_ref, got_ref, *refs):
     tp = tp_ref[0]
     weights, refs = refs[:3], refs[3:]
-    u_ref, mine_ref, theirs_ref, x_ref, x_out, sc_out, gd_out, ud_out, hid_out = refs[:9]
-    sc_ref, gd_ref, ud_ref, hid_ref, sems = refs[-5:]
-    gate_ref = weights[0]
-    up_ref, down_ref = refs[9:11] if load else weights[1:]
-    loads = []
     if load:
+        gate_ref, up_ref, down_ref = refs[8:11]
+        u_ref, mine_ref, theirs_ref, x_ref, sc_ref, gd_out, ud_out, hid_out = refs[:8]
+        gd_ref, ud_ref, hid_ref, sems = refs[11:]
         loads = [
-            pltpu.make_async_copy(src, dst, sems.at[5 + k])
-            for k, (src, dst) in enumerate(zip(weights[1:], (up_ref, down_ref)))
+            pltpu.make_async_copy(src, dst, sems.at[3 + k])
+            for k, (src, dst) in enumerate(zip(weights, (gate_ref, up_ref, down_ref)))
         ]
         loads[0].start()
+        pairs = []
+    else:
+        gate_ref, up_ref, down_ref = weights
+        x0_ref, sc0_ref = refs[:2]
+        u_ref, mine_ref, theirs_ref, x_ref, gd_out, ud_out, hid_out, x0_out, sc0_out, x_out, sc_out = refs[2:13]
+        sc_ref, gd_ref, ud_ref, hid_ref, sems = refs[13:]
+        pairs = [(x0_ref, x0_out), (sc0_ref, sc0_out), (x_ref, x_out), (sc_ref, sc_out)]
+    pairs = [(gd_ref, gd_out), (ud_ref, ud_out), (hid_ref, hid_out)] + pairs
+    base = 6 if load else 0
+    saves = [pltpu.make_async_copy(src, dst, sems.at[base + k]) for k, (src, dst) in enumerate(pairs)]
     dm = gate_ref.shape[0]
     half = dm // 2
+    if not load:
+        saves[3].start()
+        saves[4].start()
     x_ref[...] = got_ref[:, :, 0:dm].reshape(x_ref.shape)
-    sc_ref[...] = got_ref[:, :, dm:].reshape(sc_ref.shape)
-    saves = [
-        pltpu.make_async_copy(src, dst, sems.at[k])
-        for k, (src, dst) in enumerate(
-            ((x_ref, x_out), (sc_ref, sc_out), (gd_ref, gd_out), (ud_ref, ud_out), (hid_ref, hid_out))
-        )
-    ]
     if load:
         loads[1].start()
+    sc_ref[...] = got_ref[:, :, dm:].reshape(sc_ref.shape)
+    if load:
+        loads[2].start()
+        loads[0].wait()
     else:
-        saves[0].start()
-        saves[1].start()
+        saves[5].start()
+        saves[6].start()
     gp = mm(x_ref[...], gate_ref[...])
     if load:
-        loads[0].wait()
+        loads[1].wait()
     upre = mm(x_ref[...], up_ref[...])
     if load:
-        loads[1].wait()
-        saves[0].start()
-        saves[1].start()
+        loads[2].wait()
     pulled = nt(sc_ref[...], down_ref[...])
     sig = 1.0 / (1.0 + jnp.exp(-gp))
     act = gp * sig
@@ -258,7 +264,7 @@
     ud = (pulled * act).astype(BF)
     gd_ref[...] = gd
     ud_ref[...] = ud
-    for save in saves[2:]:
+    for save in saves[:3]:
         save.start()
     n = x_ref.shape[0]
     u_ref[...] = jnp.broadcast_to(u, (n, EXTRA))
@@ -480,21 +486,28 @@
     z = call(functools.partial(side_end_kernel, groups), 1 << 24, 6, [((n, EXTRA), BF)] * 2, idx, sides)
     other = partner(got)
 
-    def expert(g, weights, load):
-        held = [((dm, ff), BF), ((ff, dm), BF)] if load else []
+    def expert(g, weights, load, saved):
+        shared = [((n, EXTRA), F32), ((n, half), BF), ((n, half + EXTRA), BF), ((n, dm), BF)]
+        deltas = [((n, ff), BF)] * 3
+        if load:
+            outs = shared + [((n, dm), BF)] + deltas + [((dm, ff), BF), ((dm, ff), BF), ((ff, dm), BF)]
+            places = [VM] * 5 + [HB] * 3 + [VM] * 3
+        else:
+            outs = shared + deltas + [((n, dm), BF)] * 4
+            places = [VM] * 4 + [HB] * 7
         return call(
-            functools.partial(expert_kernel, load), 3 << 30, 18,
-            [((n, EXTRA), F32), ((n, half), BF), ((n, half + EXTRA), BF), ((n, dm), BF),
-             ((n, dm), BF), ((n, dm), BF), ((n, ff), BF), ((n, ff), BF), ((n, ff), BF)] + held,
-            [tp], [g, *weights],
-            scratch=[pltpu.VMEM((n, w), BF) for w in (dm, ff, ff, ff)] + [pltpu.SemaphoreType.DMA((8,))],
-            spaces=[VM] * 2 + [HB if load else VM] * 2,
-            out_spaces=[VM] * 4 + [HB] * 5 + [VM] * len(held),
+            functools.partial(expert_kernel, load), 3 << 30, 18, outs, [tp], [g, *weights, *saved],
+            scratch=[pltpu.VMEM((n, w), BF) for w in ((ff, ff, ff) if load else (dm, ff, ff, ff))]
+            + [pltpu.SemaphoreType.DMA((9,))],
+            spaces=[VM] + [HB if load else VM] * 3 + [VM] * len(saved),
+            out_spaces=places,
         )
 
-    first = expert(got, [gate, far(up), far(down)], True)
-    second = expert(other, [gate, *first[9:]], False)
-    u, mine, theirs, xv, x, sc, gd, ud, hid = [list(v) for v in zip(first[:9], second)]
+    u0, mine0, theirs0, x0, sc0, gd0, ud0, hid0, *held = expert(got, [far(gate), far(up), far(down)], True, [])
+    u1, mine1, theirs1, x1, gd1, ud1, hid1, *stored = expert(other, held, False, [x0, sc0])
+    u, mine, theirs, xv = [u0, u1], [mine0, mine1], [theirs0, theirs1], [x0, x1]
+    gd, ud, hid = [gd0, gd1], [ud0, ud1], [hid0, hid1]
+    x, sc = [stored[0], stored[2]], [stored[1], stored[3]]
     came = [partner(theirs[1]), partner(theirs[0])]
     rc1, ul1 = call(
         early_kernel, 1 << 28, 8, [((experts, 4, EXTRA), F32), ((n, EXTRA), F32)],

time: 156 us -> 156 us (level)
    unnamed x26 -> x24, local copies, waits for them, and re-layouts: 3.72 us -> 3.71 us
where the time goes in v7:
time: 156 us; the launch traced here: 155 us
  blocking collectives  68.4 us (44%)
  starting transfers between devices  32.2 us (21%)
  Pallas kernels  26 us (17%)
  waiting for transfers between devices  24 us (15%)
  local copies, waits for them, and re-layouts  3.71 us (2%)
    all_to_all x1, blocking collectives, exchange(): return lax.all_to_all(x, 'ep', split_axis=0, concat_axis=0, tiled=True)  68.4 us
    pallas_call x13, Pallas kernels, call(): pl.pallas_call(kernel, out_shape=[pltpu.HBM(shape, dtype) if out_spaces a...  26 us
    ppermute x13, starting transfers between devices, shift(): return lax.ppermute(v, 'ep', pairs)  19.3 us
    all_to_all x1, waiting for transfers between devices, exchange(): return lax.all_to_all(x, 'ep', split_axis=0, concat_axis=0, tiled=True)  13.7 us
    all_to_all x1, starting transfers between devices, exchange(): return lax.all_to_all(x, 'ep', split_axis=0, concat_axis=0, tiled=True)  12.3 us
    ppermute x13, waiting for transfers between devices, shift(): return lax.ppermute(v, 'ep', pairs)  9.65 us
    unnamed x24, local copies, waits for them, and re-layouts  3.71 us
  transfers between devices with their start and end apart: 18, of which 11 were waited for; matrix products, arithmetic and copies ran while one was open for 0% of the time, Pallas kernels for 13%

profile of v7, /device:TPU:32, one launch (start us, length us, event | category | flops | bytes accessed | tf_op | source)
XLA Modules:
  0.0 155.2 jit_solution(8233159707961616446)
XLA Ops:
  0.6 3.5 %shard_map.159 = (bf16[128,2,4096]{2,1,0:T(2,128)(2,1)}, f32[128,128]{1,0:T(8,128)S(1)}) custom-call(s32[1]{0:T(128)} %bitcast.1.ep_ref, s32[1]{0:T(128)} %bitcast.tp_ref, s32[2,128]{1,0:T(2,128)} %bitcast.18, bf16[4,2048]{1,0:T(4,128)(2,1)} %bitcast.12, bf16[128,2048]{1,0:T(8,128)(2,1)} %tok_hbm.1, bf16[128,2048]{1,0:T(8,128)(2,1)} %cot_hbm.1, ...), custom_call_target="tpu_custom_call" | custom-call | flops 1073741824 | bytes 4194304 | tf_op jit(solution)/shard_map/pallas_call | solution.py:46
  4.1 68.4 %all_to_all.10.got_ref = bf16[128,2,4096]{2,1,0:T(2,128)(2,1)S(1)} all-to-all(bf16[128,2,4096]{2,1,0:T(2,128)(2,1)} %get-tuple-element.68), channel_id=1, replica_groups=mesh['ep'=128,'tp'=2] {'ep'}, dimensions={0} | all-to-all | bytes 4194304 | tf_op jit(solution)/shard_map/all_to_all | solution.py:449
  72.5 4.4 %shard_map.160 = (f32[256,128]{1,0:T(8,128)S(1)}, bf16[256,1024]{1,0:T(8,128)(2,1)S(1)}, bf16[256,1152]{1,0:T(8,128)(2,1)S(1)}, bf16[256,2048]{1,0:T(8,128)(2,1)...) custom-call(s32[1]{0:T(128)} %bitcast.tp_ref, ...), custom_call_target="tpu_custom_call" | custom-call | flops 3221225472 | bytes 4194304 | tf_op jit(solution)/shard_map/pallas_call | solution.py:46
  76.9 0.6 collective-permute-start.2
  77.5 2.8 %shard_map.161 = (f32[256,128]{1,0:T(8,128)S(1)}, bf16[256,1024]{1,0:T(8,128)(2,1)S(1)}, bf16[256,1152]{1,0:T(8,128)(2,1)S(1)}, bf16[256,2048]{1,0:T(8,128)(2,1)...) custom-call(s32[1]{0:T(128)} %bitcast.tp_ref, ...), custom_call_target="tpu_custom_call" | custom-call | flops 3221225472 | bytes 4194304 | tf_op jit(solution)/shard_map/pallas_call | solution.py:46
  80.3 0.1 collective-permute-start.1
  80.4 0.6 shard_map.162
  81.0 0.8 collective-permute-start.3
  81.8 0.8 collective-permute-start.4
  82.6 1.9 %collective-permute-start.5 = (bf16[32,128]{1,0:T(8,128)(2,1)S(1)}, bf16[32,128]{1,0:T(8,128)(2,1)S(1)}, u32[]{:S(2)}, u32[]{:S(2)}) collective-permute-start(bf16[32,128]{1,0:T(8,128)(2,1)S(1)} %get-tuple-element.83), channel_id=1, source_target_pairs={{0,6},{2,0},{4,2},{6,4},{8,14},{10,8},{12,10},{14,12},{16,22},{18,... | collective-permute-start | bytes 24584 | tf_op jit(solution)/shard_map/ppermute | solution.py:460
  84.5 1.4 collective-permute-done.3.b_ref
  85.9 1.0 collective-permute-done.4.c_ref
  86.9 0.1 shard_map.163
  87.0 0.2 collective-permute-start.6
  87.2 2.0 %collective-permute-start.7 = (bf16[32,128]{1,0:T(8,128)(2,1)S(1)}, bf16[32,128]{1,0:T(8,128)(2,1)S(1)}, u32[]{:S(2)}, u32[]{:S(2)}) collective-permute-start(bf16[32,128]{1,0:T(8,128)(2,1)S(1)} %get-tuple-element.86), channel_id=1, source_target_pairs={{0,16},{2,18},{4,20},{6,22},{8,24},{10,26},{12,28},{14,30},{16,0},... | collective-permute-start | bytes 24584 | tf_op jit(solution)/shard_map/ppermute | solution.py:460
  89.2 1.3 collective-permute-start.8
  90.5 1.6 %collective-permute-done.6.b_ref = bf16[32,128]{1,0:T(8,128)(2,1)S(1)} collective-permute-done((bf16[32,128]{1,0:T(8,128)(2,1)S(1)}, bf16[32,128]{1,0:T(8,128)(2,1)S(1)}, u32[]{:S(2)}, u32[]{:S(2)}) %collective-permute-start.6) | collective-permute-done | bytes 8224 | tf_op jit(solution)/shard_map/ppermute | solution.py:460
  92.1 0.4 collective-permute-done.7.c_ref
  92.5 0.6 collective-permute-done.8.d_ref
  93.0 0.2 shard_map.164
  93.2 1.2 collective-permute-start.10
  94.4 3.3 %collective-permute-start.11 = (bf16[16,128]{1,0:T(8,128)(2,1)S(1)}, bf16[16,128]{1,0:T(8,128)(2,1)S(1)}, u32[]{:S(2)}, u32[]{:S(2)}) collective-permute-start(bf16[16,128]{1,0:T(8,128)(2,1)S(1)} %get-tuple-element.91), channel_id=1, source_target_pairs={{0,96},{2,98},{4,100},{6,102},{8,104},{10,106},{12,108},{14,110},{... | collective-permute-start | bytes 12296 | tf_op jit(solution)/shard_map/ppermute | solution.py:460
  97.7 2.2 %collective-permute-start.12 = (bf16[16,128]{1,0:T(8,128)(2,1)S(1)}, bf16[16,128]{1,0:T(8,128)(2,1)S(1)}, u32[]{:S(2)}, u32[]{:S(2)}) collective-permute-start(bf16[16,128]{1,0:T(8,128)(2,1)S(1)} %get-tuple-element.92), channel_id=1, source_target_pairs={{0,128},{2,130},{4,132},{6,134},{8,136},{10,138},{12,140},{14,142}... | collective-permute-start | bytes 12296 | tf_op jit(solution)/shard_map/ppermute | solution.py:460
  100.0 3.1 %collective-permute-start.13 = (bf16[16,128]{1,0:T(8,128)(2,1)S(1)}, bf16[16,128]{1,0:T(8,128)(2,1)S(1)}, u32[]{:S(2)}, u32[]{:S(2)}) collective-permute-start(bf16[16,128]{1,0:T(8,128)(2,1)S(1)} %get-tuple-element.93), channel_id=1, source_target_pairs={{0,160},{2,162},{4,164},{6,166},{8,168},{10,170},{12,172},{14,174}... | collective-permute-start | bytes 12296 | tf_op jit(solution)/shard_map/ppermute | solution.py:460
  103.1 1.0 collective-permute-start.14
  104.1 1.2 collective-permute-done.12.refs_4_
  105.2 0.4 collective-permute-start.15
  105.7 0.9 collective-permute-done.13.refs_5_
  106.6 1.0 collective-permute-start.9
  107.6 0.0 collective-permute-done.14.refs_6_
  107.6 1.3 collective-permute-done.15.refs_7_
  108.8 1.3 collective-permute-done.9.refs_1_
  110.2 0.6 shard_map.165
  110.8 0.6 shard_map.166
  111.4 1.9 %shard_map.167 = bf16[128,4,1152]{2,1,0:T(4,128)(2,1)} custom-call(s32[1]{0:T(128)} %bitcast.tp_ref, bf16[256,1024]{1,0:T(8,128)(2,1)S(1)} %get-tuple-element.69.refs_0_, bf16[256,1024]{1,0:T(8,128)(2,1)S(1)} %get-tuple-element.75.refs_1_, bf16[256,1152]{1,0:T(8,128)(2,1)S(1)} %collective-permute-done.1.refs_2_, ...), custom_call_target="tpu_custom_call" | custom-call | flops 536870912 | bytes 4194304 | tf_op jit(solution)/shard_map/pallas_call | solution.py:46
  113.3 0.0 copy-start.2
  113.3 0.0 copy-start.9
  113.4 12.3 %all-to-all-start.1 = ((bf16[128,4,1152]{2,1,0:T(4,128)(2,1)}), bf16[128,4,1152]{2,1,0:T(4,128)(2,1)S(1)}, u32[]{:S(2)}, u32[]{:S(2)}) async-start(bf16[128,4,1152]{2,1,0:T(4,128)(2,1)} %shard_map.167), calls=%async_computation.1 | async-start | bytes 2359296 | tf_op jit(solution)/shard_map/all_to_all | solution.py:449
  125.7 0.1 shard_map.168.aux_ref
  125.8 0.0 copy-start.3
  125.8 1.2 copy-done.3
  127.1 1.2 copy-done.4
  128.3 1.2 copy-done.5
  129.5 9.5 %shard_map.170 = (bf16[2048,256]{1,0:T(8,128)(2,1)}, bf16[2048,256]{1,0:T(8,128)(2,1)}, bf16[256,2048]{1,0:T(8,128)(2,1)}, f32[2,2048]{1,0:T(2,128)S(1)}, f32[1,256]{1,0:T(1,128)}) custom-call(bf16[256,2048]{1,0:T(8,128)(2,1)S(1)} %copy-done.2, bf16[256,2048]{1,0:T(8,128)(2,1)S(1)} %copy-done.4, bf16[256,2048]{1,0:T(8,128)(2,1)S(1)} %copy-done.3, ...), custom_call_target="tpu_custom_call" | custom-call | flops 3221225472 | bytes 4194304 | tf_op jit(solution)/shard_map/pallas_call | solution.py:46
  139.1 0.5 shard_map.169
  139.6 0.6 collective-permute-done.16.sqo_ref
  140.2 13.7 %all-to-all-done.1.back_ref = bf16[128,4,1152]{2,1,0:T(4,128)(2,1)S(1)} async-done(((bf16[128,4,1152]{2,1,0:T(4,128)(2,1)}), bf16[128,4,1152]{2,1,0:T(4,128)(2,1)S(1)}, u32[]{:S(2)}, u32[]{:S(2)}) %all-to-all-start.1) | async-done | bytes 1179680 | tf_op jit(solution)/shard_map/all_to_all | solution.py:449
  153.9 1.3 shard_map.171
  (26 shorter events, 0.1 us)
Async XLA Ops:
  72.5 5.0 %collective-permute-start = (bf16[128,2,4096]{2,1,0:T(2,128)(2,1)S(1)}, bf16[128,2,4096]{2,1,0:T(2,128)(2,1)S(1)}, u32[]{:S(2)}, u32[]{:S(2)}) collective-permute-start(bf16[128,2,4096]{2,1,0:T(2,128)(2,1)S(1)} %all_to_all.10.got_ref), channel_id=1, source_target_pairs={{0,1},{1,0},{2,3},{3,2},{4,5},{5,4},{6,7},{7,6},{8,9},{9,8},{10,11... | collective-permute-start | bytes 6291464 | tf_op jit(solution)/shard_map/ppermute | solution.py:452
  76.9 34.0 %collective-permute-start.2 = (bf16[256,1152]{1,0:T(8,128)(2,1)S(1)}, bf16[256,1152]{1,0:T(8,128)(2,1)S(1)}, u32[]{:S(2)}, u32[]{:S(2)}) collective-permute-start(bf16[256,1152]{1,0:T(8,128)(2,1)S(1)} %get-tuple-element.77), channel_id=1, source_target_pairs={{0,1},{1,0},{2,3},{3,2},{4,5},{5,4},{6,7},{7,6},{8,9},{9,8},{10,11... | collective-permute-start | bytes 1769480 | tf_op jit(solution)/shard_map/ppermute | solution.py:452
  80.3 31.1 %collective-permute-start.1 = (bf16[256,1152]{1,0:T(8,128)(2,1)S(1)}, bf16[256,1152]{1,0:T(8,128)(2,1)S(1)}, u32[]{:S(2)}, u32[]{:S(2)}) collective-permute-start(bf16[256,1152]{1,0:T(8,128)(2,1)S(1)} %get-tuple-element.76), channel_id=1, source_target_pairs={{0,1},{1,0},{2,3},{3,2},{4,5},{5,4},{6,7},{7,6},{8,9},{9,8},{10,11... | collective-permute-start | bytes 1769480 | tf_op jit(solution)/shard_map/ppermute | solution.py:452
  81.0 4.9 %collective-permute-start.3 = (bf16[32,128]{1,0:T(8,128)(2,1)S(1)}, bf16[32,128]{1,0:T(8,128)(2,1)S(1)}, u32[]{:S(2)}, u32[]{:S(2)}) collective-permute-start(bf16[32,128]{1,0:T(8,128)(2,1)S(1)} %get-tuple-element.81), channel_id=1, source_target_pairs={{0,2},{2,4},{4,6},{6,0},{8,10},{10,12},{12,14},{14,8},{16,18},{18,... | collective-permute-start | bytes 24584 | tf_op jit(solution)/shard_map/ppermute | solution.py:460
  81.8 5.2 %collective-permute-start.4 = (bf16[32,128]{1,0:T(8,128)(2,1)S(1)}, bf16[32,128]{1,0:T(8,128)(2,1)S(1)}, u32[]{:S(2)}, u32[]{:S(2)}) collective-permute-start(bf16[32,128]{1,0:T(8,128)(2,1)S(1)} %get-tuple-element.82), channel_id=1, source_target_pairs={{0,4},{2,6},{4,0},{6,2},{8,12},{10,14},{12,8},{14,10},{16,20},{18,... | collective-permute-start | bytes 24584 | tf_op jit(solution)/shard_map/ppermute | solution.py:460
  82.6 4.3 %collective-permute-start.5 = (bf16[32,128]{1,0:T(8,128)(2,1)S(1)}, bf16[32,128]{1,0:T(8,128)(2,1)S(1)}, u32[]{:S(2)}, u32[]{:S(2)}) collective-permute-start(bf16[32,128]{1,0:T(8,128)(2,1)S(1)} %get-tuple-element.83), channel_id=1, source_target_pairs={{0,6},{2,0},{4,2},{6,4},{8,14},{10,8},{12,10},{14,12},{16,22},{18,... | collective-permute-start | bytes 24584 | tf_op jit(solution)/shard_map/ppermute | solution.py:460
  87.0 5.0 %collective-permute-start.6 = (bf16[32,128]{1,0:T(8,128)(2,1)S(1)}, bf16[32,128]{1,0:T(8,128)(2,1)S(1)}, u32[]{:S(2)}, u32[]{:S(2)}) collective-permute-start(bf16[32,128]{1,0:T(8,128)(2,1)S(1)} %get-tuple-element.85), channel_id=1, source_target_pairs={{0,8},{2,10},{4,12},{6,14},{8,16},{10,18},{12,20},{14,22},{16,24},... | collective-permute-start | bytes 24584 | tf_op jit(solution)/shard_map/ppermute | solution.py:460
  87.2 5.2 %collective-permute-start.7 = (bf16[32,128]{1,0:T(8,128)(2,1)S(1)}, bf16[32,128]{1,0:T(8,128)(2,1)S(1)}, u32[]{:S(2)}, u32[]{:S(2)}) collective-permute-start(bf16[32,128]{1,0:T(8,128)(2,1)S(1)} %get-tuple-element.86), channel_id=1, source_target_pairs={{0,16},{2,18},{4,20},{6,22},{8,24},{10,26},{12,28},{14,30},{16,0},... | collective-permute-start | bytes 24584 | tf_op jit(solution)/shard_map/ppermute | solution.py:460
  89.2 3.8 %collective-permute-start.8 = (bf16[32,128]{1,0:T(8,128)(2,1)S(1)}, bf16[32,128]{1,0:T(8,128)(2,1)S(1)}, u32[]{:S(2)}, u32[]{:S(2)}) collective-permute-start(bf16[32,128]{1,0:T(8,128)(2,1)S(1)} %get-tuple-element.87), channel_id=1, source_target_pairs={{0,24},{2,26},{4,28},{6,30},{8,0},{10,2},{12,4},{14,6},{16,8},{18,... | collective-permute-start | bytes 24584 | tf_op jit(solution)/shard_map/ppermute | solution.py:460
  93.2 6.8 %collective-permute-start.10 = (bf16[16,128]{1,0:T(8,128)(2,1)S(1)}, bf16[16,128]{1,0:T(8,128)(2,1)S(1)}, u32[]{:S(2)}, u32[]{:S(2)}) collective-permute-start(bf16[16,128]{1,0:T(8,128)(2,1)S(1)} %get-tuple-element.90), channel_id=1, source_target_pairs={{0,64},{2,66},{4,68},{6,70},{8,72},{10,74},{12,76},{14,78},{16,80}... | collective-permute-start | bytes 12296 | tf_op jit(solution)/shard_map/ppermute | solution.py:460
  94.4 8.6 %collective-permute-start.11 = (bf16[16,128]{1,0:T(8,128)(2,1)S(1)}, bf16[16,128]{1,0:T(8,128)(2,1)S(1)}, u32[]{:S(2)}, u32[]{:S(2)}) collective-permute-start(bf16[16,128]{1,0:T(8,128)(2,1)S(1)} %get-tuple-element.91), channel_id=1, source_target_pairs={{0,96},{2,98},{4,100},{6,102},{8,104},{10,106},{12,108},{14,110},{... | collective-permute-start | bytes 12296 | tf_op jit(solution)/shard_map/ppermute | solution.py:460
  97.7 7.5 %collective-permute-start.12 = (bf16[16,128]{1,0:T(8,128)(2,1)S(1)}, bf16[16,128]{1,0:T(8,128)(2,1)S(1)}, u32[]{:S(2)}, u32[]{:S(2)}) collective-permute-start(bf16[16,128]{1,0:T(8,128)(2,1)S(1)} %get-tuple-element.92), channel_id=1, source_target_pairs={{0,128},{2,130},{4,132},{6,134},{8,136},{10,138},{12,140},{14,142}... | collective-permute-start | bytes 12296 | tf_op jit(solution)/shard_map/ppermute | solution.py:460
  100.0 6.6 %collective-permute-start.13 = (bf16[16,128]{1,0:T(8,128)(2,1)S(1)}, bf16[16,128]{1,0:T(8,128)(2,1)S(1)}, u32[]{:S(2)}, u32[]{:S(2)}) collective-permute-start(bf16[16,128]{1,0:T(8,128)(2,1)S(1)} %get-tuple-element.93), channel_id=1, source_target_pairs={{0,160},{2,162},{4,164},{6,166},{8,168},{10,170},{12,172},{14,174}... | collective-permute-start | bytes 12296 | tf_op jit(solution)/shard_map/ppermute | solution.py:460
  103.1 4.5 %collective-permute-start.14 = (bf16[16,128]{1,0:T(8,128)(2,1)S(1)}, bf16[16,128]{1,0:T(8,128)(2,1)S(1)}, u32[]{:S(2)}, u32[]{:S(2)}) collective-permute-start(bf16[16,128]{1,0:T(8,128)(2,1)S(1)} %get-tuple-element.94), channel_id=1, source_target_pairs={{0,192},{2,194},{4,196},{6,198},{8,200},{10,202},{12,204},{14,206}... | collective-permute-start | bytes 12296 | tf_op jit(solution)/shard_map/ppermute | solution.py:460
  105.2 3.6 %collective-permute-start.15 = (bf16[16,128]{1,0:T(8,128)(2,1)S(1)}, bf16[16,128]{1,0:T(8,128)(2,1)S(1)}, u32[]{:S(2)}, u32[]{:S(2)}) collective-permute-start(bf16[16,128]{1,0:T(8,128)(2,1)S(1)} %get-tuple-element.95), channel_id=1, source_target_pairs={{0,224},{2,226},{4,228},{6,230},{8,232},{10,234},{12,236},{14,238}... | collective-permute-start | bytes 12296 | tf_op jit(solution)/shard_map/ppermute | solution.py:460
  106.6 3.6 %collective-permute-start.9 = (bf16[16,128]{1,0:T(8,128)(2,1)S(1)}, bf16[16,128]{1,0:T(8,128)(2,1)S(1)}, u32[]{:S(2)}, u32[]{:S(2)}) collective-permute-start(bf16[16,128]{1,0:T(8,128)(2,1)S(1)} %get-tuple-element.89), channel_id=1, source_target_pairs={{0,32},{2,34},{4,36},{6,38},{8,40},{10,42},{12,44},{14,46},{16,48}... | collective-permute-start | bytes 12296 | tf_op jit(solution)/shard_map/ppermute | solution.py:460
  113.3 12.5 %copy-start.2 = (bf16[256,2048]{1,0:T(8,128)(2,1)S(1)}, bf16[256,2048]{1,0:T(8,128)(2,1)}, u32[]{:S(2)}) copy-start(bf16[256,2048]{1,0:T(8,128)(2,1)} %get-tuple-element.105.refs_0_) | copy-start | bytes 3145732
  113.3 12.5 %copy-start.6 = (bf16[256,256]{1,0:T(8,128)(2,1)S(1)}, bf16[256,256]{1,0:T(8,128)(2,1)}, u32[]{:S(2)}) copy-start(bf16[256,256]{1,0:T(8,128)(2,1)} %get-tuple-element.110.refs_5_) | copy-start | bytes 393220
  113.3 12.5 %copy-start.7 = (bf16[256,256]{1,0:T(8,128)(2,1)S(1)}, bf16[256,256]{1,0:T(8,128)(2,1)}, u32[]{:S(2)}) copy-start(bf16[256,256]{1,0:T(8,128)(2,1)} %get-tuple-element.112.refs_7_) | copy-start | bytes 393220
  113.3 12.5 %copy-start.8 = (bf16[256,256]{1,0:T(8,128)(2,1)S(1)}, bf16[256,256]{1,0:T(8,128)(2,1)}, u32[]{:S(2)}) copy-start(bf16[256,256]{1,0:T(8,128)(2,1)} %get-tuple-element.114.refs_9_) | copy-start | bytes 393220
  113.3 12.5 %copy-start.9 = (bf16[256,256]{1,0:T(8,128)(2,1)S(1)}, bf16[256,256]{1,0:T(8,128)(2,1)}, u32[]{:S(2)}) copy-start(bf16[256,256]{1,0:T(8,128)(2,1)} %get-tuple-element.109.refs_4_) | copy-start | bytes 393220
  113.3 12.5 %copy-start.10 = (bf16[256,256]{1,0:T(8,128)(2,1)S(1)}, bf16[256,256]{1,0:T(8,128)(2,1)}, u32[]{:S(2)}) copy-start(bf16[256,256]{1,0:T(8,128)(2,1)} %get-tuple-element.111.refs_6_) | copy-start | bytes 393220
  113.4 12.5 %copy-start.11 = (bf16[256,256]{1,0:T(8,128)(2,1)S(1)}, bf16[256,256]{1,0:T(8,128)(2,1)}, u32[]{:S(2)}) copy-start(bf16[256,256]{1,0:T(8,128)(2,1)} %get-tuple-element.113.refs_8_) | copy-start | bytes 393220
  113.4 40.6 %all-to-all-start.1 = ((bf16[128,4,1152]{2,1,0:T(4,128)(2,1)}), bf16[128,4,1152]{2,1,0:T(4,128)(2,1)S(1)}, u32[]{:S(2)}, u32[]{:S(2)}) async-start(bf16[128,4,1152]{2,1,0:T(4,128)(2,1)} %shard_map.167), calls=%async_computation.1 | async-start | bytes 2359296 | tf_op jit(solution)/shard_map/all_to_all | solution.py:449
  125.8 1.2 copy-start.3
  127.1 1.2 copy-start.4
  128.3 1.2 copy-start.5
  129.5 9.6 %copy-start = (bf16[2048,128]{1,0:T(8,128)(2,1)S(1)}, bf16[2048,128]{1,0:T(8,128)(2,1)}, u32[]{:S(2)}) copy-start(bf16[2048,128]{1,0:T(8,128)(2,1)} %rex_ref.1) | copy-start | bytes 1572868
  129.5 9.6 %copy-start.1 = (bf16[2048,4]{0,1:T(4,128)(2,1)S(1)}, bf16[2048,4]{0,1:T(4,128)(2,1)}, u32[]{:S(2)}) copy-start(bf16[2048,4]{0,1:T(4,128)(2,1)} %param.11) | copy-start | bytes 49156
  139.1 1.2 collective-permute-start.16

commit v8 on v7

--- a/solution.py
+++ b/solution.py
@@ -222,7 +222,8 @@
             pltpu.make_async_copy(src, dst, sems.at[3 + k])
             for k, (src, dst) in enumerate(zip(weights, (gate_ref, up_ref, down_ref)))
         ]
-        loads[0].start()
+        for copy in loads:
+            copy.start()
         pairs = []
     else:
         gate_ref, up_ref, down_ref = weights
@@ -239,11 +240,8 @@
         saves[3].start()
         saves[4].start()
     x_ref[...] = got_ref[:, :, 0:dm].reshape(x_ref.shape)
-    if load:
-        loads[1].start()
     sc_ref[...] = got_ref[:, :, dm:].reshape(sc_ref.shape)
     if load:
-        loads[2].start()
         loads[0].wait()
     else:
         saves[5].start()

time: 156 us -> 156 us (level)
  no operation moved by 1% of the time
where the time goes in v8:
time: 156 us; the launch traced here: 155 us
  blocking collectives  68.4 us (44%)
  starting transfers between devices  32.2 us (21%)
  Pallas kernels  26 us (17%)
  waiting for transfers between devices  24 us (15%)
  local copies, waits for them, and re-layouts  3.71 us (2%)
    all_to_all x1, blocking collectives, exchange(): return lax.all_to_all(x, 'ep', split_axis=0, concat_axis=0, tiled=True)  68.4 us
    pallas_call x13, Pallas kernels, call(): pl.pallas_call(kernel, out_shape=[pltpu.HBM(shape, dtype) if out_spaces a...  26 us
    ppermute x13, starting transfers between devices, shift(): return lax.ppermute(v, 'ep', pairs)  19.3 us
    all_to_all x1, waiting for transfers between devices, exchange(): return lax.all_to_all(x, 'ep', split_axis=0, concat_axis=0, tiled=True)  13.7 us
    all_to_all x1, starting transfers between devices, exchange(): return lax.all_to_all(x, 'ep', split_axis=0, concat_axis=0, tiled=True)  12.3 us
    ppermute x13, waiting for transfers between devices, shift(): return lax.ppermute(v, 'ep', pairs)  9.65 us
    unnamed x24, local copies, waits for them, and re-layouts  3.71 us
  transfers between devices with their start and end apart: 18, of which 11 were waited for; matrix products, arithmetic and copies ran while one was open for 0% of the time, Pallas kernels for 13%

profile of v8, /device:TPU:32, one launch (start us, length us, event | category | flops | bytes accessed | tf_op | source)
XLA Modules:
  0.0 155.2 jit_solution(11454345982220130656)
XLA Ops:
  0.6 3.5 %shard_map.159 = (bf16[128,2,4096]{2,1,0:T(2,128)(2,1)}, f32[128,128]{1,0:T(8,128)S(1)}) custom-call(s32[1]{0:T(128)} %bitcast.1.ep_ref, s32[1]{0:T(128)} %bitcast.tp_ref, s32[2,128]{1,0:T(2,128)} %bitcast.18, bf16[4,2048]{1,0:T(4,128)(2,1)} %bitcast.12, bf16[128,2048]{1,0:T(8,128)(2,1)} %tok_hbm.1, bf16[128,2048]{1,0:T(8,128)(2,1)} %cot_hbm.1, ...), custom_call_target="tpu_custom_call" | custom-call | flops 1073741824 | bytes 4194304 | tf_op jit(solution)/shard_map/pallas_call | solution.py:46
  4.1 68.4 %all_to_all.10.got_ref = bf16[128,2,4096]{2,1,0:T(2,128)(2,1)S(1)} all-to-all(bf16[128,2,4096]{2,1,0:T(2,128)(2,1)} %get-tuple-element.68), channel_id=1, replica_groups=mesh['ep'=128,'tp'=2] {'ep'}, dimensions={0} | all-to-all | bytes 4194304 | tf_op jit(solution)/shard_map/all_to_all | solution.py:447
  72.5 4.4 %shard_map.160 = (f32[256,128]{1,0:T(8,128)S(1)}, bf16[256,1024]{1,0:T(8,128)(2,1)S(1)}, bf16[256,1152]{1,0:T(8,128)(2,1)S(1)}, bf16[256,2048]{1,0:T(8,128)(2,1)...) custom-call(s32[1]{0:T(128)} %bitcast.tp_ref, ...), custom_call_target="tpu_custom_call" | custom-call | flops 3221225472 | bytes 4194304 | tf_op jit(solution)/shard_map/pallas_call | solution.py:46
  76.9 0.6 collective-permute-start.2
  77.5 2.8 %shard_map.161 = (f32[256,128]{1,0:T(8,128)S(1)}, bf16[256,1024]{1,0:T(8,128)(2,1)S(1)}, bf16[256,1152]{1,0:T(8,128)(2,1)S(1)}, bf16[256,2048]{1,0:T(8,128)(2,1)...) custom-call(s32[1]{0:T(128)} %bitcast.tp_ref, ...), custom_call_target="tpu_custom_call" | custom-call | flops 3221225472 | bytes 4194304 | tf_op jit(solution)/shard_map/pallas_call | solution.py:46
  80.3 0.1 collective-permute-start.1
  80.4 0.6 shard_map.162
  81.0 0.8 collective-permute-start.3
  81.8 0.8 collective-permute-start.4
  82.6 1.9 %collective-permute-start.5 = (bf16[32,128]{1,0:T(8,128)(2,1)S(1)}, bf16[32,128]{1,0:T(8,128)(2,1)S(1)}, u32[]{:S(2)}, u32[]{:S(2)}) collective-permute-start(bf16[32,128]{1,0:T(8,128)(2,1)S(1)} %get-tuple-element.83), channel_id=1, source_target_pairs={{0,6},{2,0},{4,2},{6,4},{8,14},{10,8},{12,10},{14,12},{16,22},{18,... | collective-permute-start | bytes 24584 | tf_op jit(solution)/shard_map/ppermute | solution.py:458
  84.5 1.4 collective-permute-done.3.b_ref
  85.9 1.0 collective-permute-done.4.c_ref
  86.9 0.1 shard_map.163
  87.0 0.2 collective-permute-start.6
  87.2 2.0 %collective-permute-start.7 = (bf16[32,128]{1,0:T(8,128)(2,1)S(1)}, bf16[32,128]{1,0:T(8,128)(2,1)S(1)}, u32[]{:S(2)}, u32[]{:S(2)}) collective-permute-start(bf16[32,128]{1,0:T(8,128)(2,1)S(1)} %get-tuple-element.86), channel_id=1, source_target_pairs={{0,16},{2,18},{4,20},{6,22},{8,24},{10,26},{12,28},{14,30},{16,0},... | collective-permute-start | bytes 24584 | tf_op jit(solution)/shard_map/ppermute | solution.py:458
  89.2 1.3 collective-permute-start.8
  90.5 1.6 %collective-permute-done.6.b_ref = bf16[32,128]{1,0:T(8,128)(2,1)S(1)} collective-permute-done((bf16[32,128]{1,0:T(8,128)(2,1)S(1)}, bf16[32,128]{1,0:T(8,128)(2,1)S(1)}, u32[]{:S(2)}, u32[]{:S(2)}) %collective-permute-start.6) | collective-permute-done | bytes 8224 | tf_op jit(solution)/shard_map/ppermute | solution.py:458
  92.1 0.4 collective-permute-done.7.c_ref
  92.5 0.6 collective-permute-done.8.d_ref
  93.0 0.2 shard_map.164
  93.2 1.2 collective-permute-start.10
  94.4 3.3 %collective-permute-start.11 = (bf16[16,128]{1,0:T(8,128)(2,1)S(1)}, bf16[16,128]{1,0:T(8,128)(2,1)S(1)}, u32[]{:S(2)}, u32[]{:S(2)}) collective-permute-start(bf16[16,128]{1,0:T(8,128)(2,1)S(1)} %get-tuple-element.91), channel_id=1, source_target_pairs={{0,96},{2,98},{4,100},{6,102},{8,104},{10,106},{12,108},{14,110},{... | collective-permute-start | bytes 12296 | tf_op jit(solution)/shard_map/ppermute | solution.py:458
  97.7 2.2 %collective-permute-start.12 = (bf16[16,128]{1,0:T(8,128)(2,1)S(1)}, bf16[16,128]{1,0:T(8,128)(2,1)S(1)}, u32[]{:S(2)}, u32[]{:S(2)}) collective-permute-start(bf16[16,128]{1,0:T(8,128)(2,1)S(1)} %get-tuple-element.92), channel_id=1, source_target_pairs={{0,128},{2,130},{4,132},{6,134},{8,136},{10,138},{12,140},{14,142}... | collective-permute-start | bytes 12296 | tf_op jit(solution)/shard_map/ppermute | solution.py:458
  100.0 3.1 %collective-permute-start.13 = (bf16[16,128]{1,0:T(8,128)(2,1)S(1)}, bf16[16,128]{1,0:T(8,128)(2,1)S(1)}, u32[]{:S(2)}, u32[]{:S(2)}) collective-permute-start(bf16[16,128]{1,0:T(8,128)(2,1)S(1)} %get-tuple-element.93), channel_id=1, source_target_pairs={{0,160},{2,162},{4,164},{6,166},{8,168},{10,170},{12,172},{14,174}... | collective-permute-start | bytes 12296 | tf_op jit(solution)/shard_map/ppermute | solution.py:458
  103.1 1.0 collective-permute-start.14
  104.1 1.2 collective-permute-done.12.refs_4_
  105.2 0.4 collective-permute-start.15
  105.7 0.9 collective-permute-done.13.refs_5_
  106.6 1.0 collective-permute-start.9
  107.6 0.0 collective-permute-done.14.refs_6_
  107.6 1.3 collective-permute-done.15.refs_7_
  108.8 1.3 collective-permute-done.9.refs_1_
  110.2 0.6 shard_map.165
  110.8 0.6 shard_map.166
  111.4 1.9 %shard_map.167 = bf16[128,4,1152]{2,1,0:T(4,128)(2,1)} custom-call(s32[1]{0:T(128)} %bitcast.tp_ref, bf16[256,1024]{1,0:T(8,128)(2,1)S(1)} %get-tuple-element.69.refs_0_, bf16[256,1024]{1,0:T(8,128)(2,1)S(1)} %get-tuple-element.75.refs_1_, bf16[256,1152]{1,0:T(8,128)(2,1)S(1)} %collective-permute-done.1.refs_2_, ...), custom_call_target="tpu_custom_call" | custom-call | flops 536870912 | bytes 4194304 | tf_op jit(solution)/shard_map/pallas_call | solution.py:46
  113.3 0.0 copy-start.2
  113.3 0.0 copy-start.9
  113.4 12.3 %all-to-all-start.1 = ((bf16[128,4,1152]{2,1,0:T(4,128)(2,1)}), bf16[128,4,1152]{2,1,0:T(4,128)(2,1)S(1)}, u32[]{:S(2)}, u32[]{:S(2)}) async-start(bf16[128,4,1152]{2,1,0:T(4,128)(2,1)} %shard_map.167), calls=%async_computation.1 | async-start | bytes 2359296 | tf_op jit(solution)/shard_map/all_to_all | solution.py:447
  125.7 0.1 shard_map.168.aux_ref
  125.8 0.0 copy-start.3
  125.8 1.2 copy-done.3
  127.1 1.2 copy-done.4
  128.3 1.2 copy-done.5
  129.5 9.5 %shard_map.170 = (bf16[2048,256]{1,0:T(8,128)(2,1)}, bf16[2048,256]{1,0:T(8,128)(2,1)}, bf16[256,2048]{1,0:T(8,128)(2,1)}, f32[2,2048]{1,0:T(2,128)S(1)}, f32[1,256]{1,0:T(1,128)}) custom-call(bf16[256,2048]{1,0:T(8,128)(2,1)S(1)} %copy-done.2, bf16[256,2048]{1,0:T(8,128)(2,1)S(1)} %copy-done.4, bf16[256,2048]{1,0:T(8,128)(2,1)S(1)} %copy-done.3, ...), custom_call_target="tpu_custom_call" | custom-call | flops 3221225472 | bytes 4194304 | tf_op jit(solution)/shard_map/pallas_call | solution.py:46
  139.1 0.5 shard_map.169
  139.6 0.6 collective-permute-done.16.sqo_ref
  140.2 13.7 %all-to-all-done.1.back_ref = bf16[128,4,1152]{2,1,0:T(4,128)(2,1)S(1)} async-done(((bf16[128,4,1152]{2,1,0:T(4,128)(2,1)}), bf16[128,4,1152]{2,1,0:T(4,128)(2,1)S(1)}, u32[]{:S(2)}, u32[]{:S(2)}) %all-to-all-start.1) | async-done | bytes 1179680 | tf_op jit(solution)/shard_map/all_to_all | solution.py:447
  153.9 1.3 shard_map.171
  (26 shorter events, 0.1 us)
Async XLA Ops:
  72.5 5.0 %collective-permute-start = (bf16[128,2,4096]{2,1,0:T(2,128)(2,1)S(1)}, bf16[128,2,4096]{2,1,0:T(2,128)(2,1)S(1)}, u32[]{:S(2)}, u32[]{:S(2)}) collective-permute-start(bf16[128,2,4096]{2,1,0:T(2,128)(2,1)S(1)} %all_to_all.10.got_ref), channel_id=1, source_target_pairs={{0,1},{1,0},{2,3},{3,2},{4,5},{5,4},{6,7},{7,6},{8,9},{9,8},{10,11... | collective-permute-start | bytes 6291464 | tf_op jit(solution)/shard_map/ppermute | solution.py:450
  76.9 34.0 %collective-permute-start.2 = (bf16[256,1152]{1,0:T(8,128)(2,1)S(1)}, bf16[256,1152]{1,0:T(8,128)(2,1)S(1)}, u32[]{:S(2)}, u32[]{:S(2)}) collective-permute-start(bf16[256,1152]{1,0:T(8,128)(2,1)S(1)} %get-tuple-element.77), channel_id=1, source_target_pairs={{0,1},{1,0},{2,3},{3,2},{4,5},{5,4},{6,7},{7,6},{8,9},{9,8},{10,11... | collective-permute-start | bytes 1769480 | tf_op jit(solution)/shard_map/ppermute | solution.py:450
  80.3 31.1 %collective-permute-start.1 = (bf16[256,1152]{1,0:T(8,128)(2,1)S(1)}, bf16[256,1152]{1,0:T(8,128)(2,1)S(1)}, u32[]{:S(2)}, u32[]{:S(2)}) collective-permute-start(bf16[256,1152]{1,0:T(8,128)(2,1)S(1)} %get-tuple-element.76), channel_id=1, source_target_pairs={{0,1},{1,0},{2,3},{3,2},{4,5},{5,4},{6,7},{7,6},{8,9},{9,8},{10,11... | collective-permute-start | bytes 1769480 | tf_op jit(solution)/shard_map/ppermute | solution.py:450
  81.0 4.9 %collective-permute-start.3 = (bf16[32,128]{1,0:T(8,128)(2,1)S(1)}, bf16[32,128]{1,0:T(8,128)(2,1)S(1)}, u32[]{:S(2)}, u32[]{:S(2)}) collective-permute-start(bf16[32,128]{1,0:T(8,128)(2,1)S(1)} %get-tuple-element.81), channel_id=1, source_target_pairs={{0,2},{2,4},{4,6},{6,0},{8,10},{10,12},{12,14},{14,8},{16,18},{18,... | collective-permute-start | bytes 24584 | tf_op jit(solution)/shard_map/ppermute | solution.py:458
  81.8 5.2 %collective-permute-start.4 = (bf16[32,128]{1,0:T(8,128)(2,1)S(1)}, bf16[32,128]{1,0:T(8,128)(2,1)S(1)}, u32[]{:S(2)}, u32[]{:S(2)}) collective-permute-start(bf16[32,128]{1,0:T(8,128)(2,1)S(1)} %get-tuple-element.82), channel_id=1, source_target_pairs={{0,4},{2,6},{4,0},{6,2},{8,12},{10,14},{12,8},{14,10},{16,20},{18,... | collective-permute-start | bytes 24584 | tf_op jit(solution)/shard_map/ppermute | solution.py:458
  82.6 4.3 %collective-permute-start.5 = (bf16[32,128]{1,0:T(8,128)(2,1)S(1)}, bf16[32,128]{1,0:T(8,128)(2,1)S(1)}, u32[]{:S(2)}, u32[]{:S(2)}) collective-permute-start(bf16[32,128]{1,0:T(8,128)(2,1)S(1)} %get-tuple-element.83), channel_id=1, source_target_pairs={{0,6},{2,0},{4,2},{6,4},{8,14},{10,8},{12,10},{14,12},{16,22},{18,... | collective-permute-start | bytes 24584 | tf_op jit(solution)/shard_map/ppermute | solution.py:458
  87.0 5.0 %collective-permute-start.6 = (bf16[32,128]{1,0:T(8,128)(2,1)S(1)}, bf16[32,128]{1,0:T(8,128)(2,1)S(1)}, u32[]{:S(2)}, u32[]{:S(2)}) collective-permute-start(bf16[32,128]{1,0:T(8,128)(2,1)S(1)} %get-tuple-element.85), channel_id=1, source_target_pairs={{0,8},{2,10},{4,12},{6,14},{8,16},{10,18},{12,20},{14,22},{16,24},... | collective-permute-start | bytes 24584 | tf_op jit(solution)/shard_map/ppermute | solution.py:458
  87.2 5.2 %collective-permute-start.7 = (bf16[32,128]{1,0:T(8,128)(2,1)S(1)}, bf16[32,128]{1,0:T(8,128)(2,1)S(1)}, u32[]{:S(2)}, u32[]{:S(2)}) collective-permute-start(bf16[32,128]{1,0:T(8,128)(2,1)S(1)} %get-tuple-element.86), channel_id=1, source_target_pairs={{0,16},{2,18},{4,20},{6,22},{8,24},{10,26},{12,28},{14,30},{16,0},... | collective-permute-start | bytes 24584 | tf_op jit(solution)/shard_map/ppermute | solution.py:458
  89.2 3.8 %collective-permute-start.8 = (bf16[32,128]{1,0:T(8,128)(2,1)S(1)}, bf16[32,128]{1,0:T(8,128)(2,1)S(1)}, u32[]{:S(2)}, u32[]{:S(2)}) collective-permute-start(bf16[32,128]{1,0:T(8,128)(2,1)S(1)} %get-tuple-element.87), channel_id=1, source_target_pairs={{0,24},{2,26},{4,28},{6,30},{8,0},{10,2},{12,4},{14,6},{16,8},{18,... | collective-permute-start | bytes 24584 | tf_op jit(solution)/shard_map/ppermute | solution.py:458
  93.2 6.8 %collective-permute-start.10 = (bf16[16,128]{1,0:T(8,128)(2,1)S(1)}, bf16[16,128]{1,0:T(8,128)(2,1)S(1)}, u32[]{:S(2)}, u32[]{:S(2)}) collective-permute-start(bf16[16,128]{1,0:T(8,128)(2,1)S(1)} %get-tuple-element.90), channel_id=1, source_target_pairs={{0,64},{2,66},{4,68},{6,70},{8,72},{10,74},{12,76},{14,78},{16,80}... | collective-permute-start | bytes 12296 | tf_op jit(solution)/shard_map/ppermute | solution.py:458
  94.4 8.6 %collective-permute-start.11 = (bf16[16,128]{1,0:T(8,128)(2,1)S(1)}, bf16[16,128]{1,0:T(8,128)(2,1)S(1)}, u32[]{:S(2)}, u32[]{:S(2)}) collective-permute-start(bf16[16,128]{1,0:T(8,128)(2,1)S(1)} %get-tuple-element.91), channel_id=1, source_target_pairs={{0,96},{2,98},{4,100},{6,102},{8,104},{10,106},{12,108},{14,110},{... | collective-permute-start | bytes 12296 | tf_op jit(solution)/shard_map/ppermute | solution.py:458
  97.7 7.5 %collective-permute-start.12 = (bf16[16,128]{1,0:T(8,128)(2,1)S(1)}, bf16[16,128]{1,0:T(8,128)(2,1)S(1)}, u32[]{:S(2)}, u32[]{:S(2)}) collective-permute-start(bf16[16,128]{1,0:T(8,128)(2,1)S(1)} %get-tuple-element.92), channel_id=1, source_target_pairs={{0,128},{2,130},{4,132},{6,134},{8,136},{10,138},{12,140},{14,142}... | collective-permute-start | bytes 12296 | tf_op jit(solution)/shard_map/ppermute | solution.py:458
  100.0 6.6 %collective-permute-start.13 = (bf16[16,128]{1,0:T(8,128)(2,1)S(1)}, bf16[16,128]{1,0:T(8,128)(2,1)S(1)}, u32[]{:S(2)}, u32[]{:S(2)}) collective-permute-start(bf16[16,128]{1,0:T(8,128)(2,1)S(1)} %get-tuple-element.93), channel_id=1, source_target_pairs={{0,160},{2,162},{4,164},{6,166},{8,168},{10,170},{12,172},{14,174}... | collective-permute-start | bytes 12296 | tf_op jit(solution)/shard_map/ppermute | solution.py:458
  103.1 4.5 %collective-permute-start.14 = (bf16[16,128]{1,0:T(8,128)(2,1)S(1)}, bf16[16,128]{1,0:T(8,128)(2,1)S(1)}, u32[]{:S(2)}, u32[]{:S(2)}) collective-permute-start(bf16[16,128]{1,0:T(8,128)(2,1)S(1)} %get-tuple-element.94), channel_id=1, source_target_pairs={{0,192},{2,194},{4,196},{6,198},{8,200},{10,202},{12,204},{14,206}... | collective-permute-start | bytes 12296 | tf_op jit(solution)/shard_map/ppermute | solution.py:458
  105.2 3.6 %collective-permute-start.15 = (bf16[16,128]{1,0:T(8,128)(2,1)S(1)}, bf16[16,128]{1,0:T(8,128)(2,1)S(1)}, u32[]{:S(2)}, u32[]{:S(2)}) collective-permute-start(bf16[16,128]{1,0:T(8,128)(2,1)S(1)} %get-tuple-element.95), channel_id=1, source_target_pairs={{0,224},{2,226},{4,228},{6,230},{8,232},{10,234},{12,236},{14,238}... | collective-permute-start | bytes 12296 | tf_op jit(solution)/shard_map/ppermute | solution.py:458
  106.6 3.6 %collective-permute-start.9 = (bf16[16,128]{1,0:T(8,128)(2,1)S(1)}, bf16[16,128]{1,0:T(8,128)(2,1)S(1)}, u32[]{:S(2)}, u32[]{:S(2)}) collective-permute-start(bf16[16,128]{1,0:T(8,128)(2,1)S(1)} %get-tuple-element.89), channel_id=1, source_target_pairs={{0,32},{2,34},{4,36},{6,38},{8,40},{10,42},{12,44},{14,46},{16,48}... | collective-permute-start | bytes 12296 | tf_op jit(solution)/shard_map/ppermute | solution.py:458
  113.3 12.5 %copy-start.2 = (bf16[256,2048]{1,0:T(8,128)(2,1)S(1)}, bf16[256,2048]{1,0:T(8,128)(2,1)}, u32[]{:S(2)}) copy-start(bf16[256,2048]{1,0:T(8,128)(2,1)} %get-tuple-element.105.refs_0_) | copy-start | bytes 3145732
  113.3 12.5 %copy-start.6 = (bf16[256,256]{1,0:T(8,128)(2,1)S(1)}, bf16[256,256]{1,0:T(8,128)(2,1)}, u32[]{:S(2)}) copy-start(bf16[256,256]{1,0:T(8,128)(2,1)} %get-tuple-element.110.refs_5_) | copy-start | bytes 393220
  113.3 12.5 %copy-start.7 = (bf16[256,256]{1,0:T(8,128)(2,1)S(1)}, bf16[256,256]{1,0:T(8,128)(2,1)}, u32[]{:S(2)}) copy-start(bf16[256,256]{1,0:T(8,128)(2,1)} %get-tuple-element.112.refs_7_) | copy-start | bytes 393220
  113.3 12.5 %copy-start.8 = (bf16[256,256]{1,0:T(8,128)(2,1)S(1)}, bf16[256,256]{1,0:T(8,128)(2,1)}, u32[]{:S(2)}) copy-start(bf16[256,256]{1,0:T(8,128)(2,1)} %get-tuple-element.114.refs_9_) | copy-start | bytes 393220
  113.3 12.5 %copy-start.9 = (bf16[256,256]{1,0:T(8,128)(2,1)S(1)}, bf16[256,256]{1,0:T(8,128)(2,1)}, u32[]{:S(2)}) copy-start(bf16[256,256]{1,0:T(8,128)(2,1)} %get-tuple-element.109.refs_4_) | copy-start | bytes 393220
  113.3 12.5 %copy-start.10 = (bf16[256,256]{1,0:T(8,128)(2,1)S(1)}, bf16[256,256]{1,0:T(8,128)(2,1)}, u32[]{:S(2)}) copy-start(bf16[256,256]{1,0:T(8,128)(2,1)} %get-tuple-element.111.refs_6_) | copy-start | bytes 393220
  113.4 12.5 %copy-start.11 = (bf16[256,256]{1,0:T(8,128)(2,1)S(1)}, bf16[256,256]{1,0:T(8,128)(2,1)}, u32[]{:S(2)}) copy-start(bf16[256,256]{1,0:T(8,128)(2,1)} %get-tuple-element.113.refs_8_) | copy-start | bytes 393220
  113.4 40.6 %all-to-all-start.1 = ((bf16[128,4,1152]{2,1,0:T(4,128)(2,1)}), bf16[128,4,1152]{2,1,0:T(4,128)(2,1)S(1)}, u32[]{:S(2)}, u32[]{:S(2)}) async-start(bf16[128,4,1152]{2,1,0:T(4,128)(2,1)} %shard_map.167), calls=%async_computation.1 | async-start | bytes 2359296 | tf_op jit(solution)/shard_map/all_to_all | solution.py:447
  125.8 1.2 copy-start.3
  127.1 1.2 copy-start.4
  128.3 1.2 copy-start.5
  129.5 9.6 %copy-start = (bf16[2048,128]{1,0:T(8,128)(2,1)S(1)}, bf16[2048,128]{1,0:T(8,128)(2,1)}, u32[]{:S(2)}) copy-start(bf16[2048,128]{1,0:T(8,128)(2,1)} %rex_ref.1) | copy-start | bytes 1572868
  129.5 9.6 %copy-start.1 = (bf16[2048,4]{0,1:T(4,128)(2,1)S(1)}, bf16[2048,4]{0,1:T(4,128)(2,1)}, u32[]{:S(2)}) copy-start(bf16[2048,4]{0,1:T(4,128)(2,1)} %param.11) | copy-start | bytes 49156
  139.1 1.2 collective-permute-start.16
